TPU v7x, 32 devices: a whole 2x2x4 slice. The times are simulated.
32 devices in a mesh: dp: 4 (over y, x), kv: 4 (over z), tp: 2 (over core).
Axes of the slice: x: 2, y: 2, z: 4, core: 2. Of those that a mesh axis runs over, the one named last changes fastest.
Arguments:
- hidden: bfloat16 [2048, 16], P(('kv', 'tp'), 'dp'), parts along dimension 1, may hold values from -20 to 20
- mixer_gain: float32 [2048], replicated, may hold values from 0.1 to 1.9
- gate_proj: bfloat16 [2048, 64, 64], P(None, 'kv', 'tp'), may hold values from -0.125 to 0.125
- inner_proj: bfloat16 [2048, 64, 64], P(None, 'kv', 'tp'), may hold values from -0.125 to 0.125
- input_proj: bfloat16 [2048, 1024], P(None, 'kv'), may hold values from -0.125 to 0.125
- output_proj: bfloat16 [2048, 1024], P(None, 'kv'), may hold values from -0.125 to 0.125
- step_proj: bfloat16 [2048, 64], replicated, may hold values from -0.125 to 0.125
- step_bias: float32 [64], replicated, may hold values from -3 to -0.5
- decay_log: float32 [64], replicated, may hold values from -3 to 1
- skip_gain: float32 [64], replicated, may hold values from 0.3 to 1.5
- taps_inner: float32 [4, 64, 64], P(None, None, 'tp'), may hold values from -3 to 3
- taps_input: float32 [4, 1024], replicated, may hold values from -3 to 3
- taps_output: float32 [4, 1024], replicated, may hold values from -3 to 3
- recent_inner: bfloat16 [16, 3, 64, 64], P(('dp', 'kv'), None, None, 'tp'), parts along dimension 0, may hold values from -6 to 6
- recent_input: bfloat16 [16, 3, 1024], P(('dp', 'kv')), parts along dimension 0, may hold values from -6 to 6
- recent_output: bfloat16 [16, 3, 1024], P(('dp', 'kv')), parts along dimension 0, may hold values from -6 to 6
- states: float32 [16, 64, 64, 128], P(('dp', 'kv'), None, 'tp'), parts along dimension 0, may hold values from -4 to 4
- block_inner: bfloat16 [16, 128, 64, 64], P(('dp', 'kv'), None, None, 'tp'), parts along dimension 0, may hold values from -6 to 6
- block_input: bfloat16 [16, 128, 1024], P(('dp', 'kv')), parts along dimension 0, may hold values from -4 to 4
- block_decay: float32 [16, 128, 64], P(('dp', 'kv')), parts along dimension 0
- lengths: int32 [16], P(('dp', 'kv')), parts along dimension 0, may hold values from 1 to 128, 170 in all
- norm_gain: float32 [64, 64], P(None, 'tp'), may hold values from 0.1 to 1.9
- mixer_out: bfloat16 [64, 64, 2048], P('kv', 'tp'), may hold values from -0.125 to 0.125
- channel_gain: float32 [2048], replicated, may hold values from 0.1 to 1.9
- expand_gate: bfloat16 [2048, 5632], P(None, ('kv', 'tp')), may hold values from -0.125 to 0.125
- expand_value: bfloat16 [2048, 5632], P(None, ('kv', 'tp')), may hold values from -0.125 to 0.125
- reduce_proj: bfloat16 [5632, 2048], P(('kv', 'tp')), may hold values from -0.109375 to 0.109375
Outputs:
- layer_out: bfloat16 [2048, 16], P(('kv', 'tp'), 'dp'), parts along dimension 1
There are 4 independent parts, one for each index of `dp`. A program takes and returns all parts, laid end to end along the dimension named above; an argument that names none is the same for every part. Nothing has to cross between parts.
All inputs are finite; a program needn't handle non-finite values. No bound on the sum of `lengths` on one device may be relied on, other than what follows from the above.
Results may differ from a plain program's by a relative error of at most 0.01.
Values may be sent and summed in bfloat16 or wider, within the bound.
No kernel may reach another device: no remote copies, remote signals or barrier semaphores. Data moves between devices by JAX's collectives and lax.ppermute only.
A program may use at most 64 MiB of HBM per device.

v0:
```python
import jax
import jax.numpy as jnp
from jax import lax
from jax.sharding import PartitionSpec as P

MIXER_HEADS = 64
HEAD_DIM = 64
GROUPS = 8
STATE = 128
OPEN_BLOCK_SPAN = 128


epsilon = 1e-05


def short_conv(recent, newest, taps):
    window = jnp.concatenate(
        [recent.astype(jnp.float32), newest.astype(jnp.float32)[:, None]], axis=1
    )
    return jax.nn.silu(jnp.sum(window * taps[None], axis=1))


def shards(
    hidden,
    mixer_gain,
    gate_proj,
    inner_proj,
    input_proj,
    output_proj,
    step_proj,
    step_bias,
    decay_log,
    skip_gain,
    taps_inner,
    taps_input,
    taps_output,
    recent_inner,
    recent_input,
    recent_output,
    states,
    block_inner,
    block_input,
    block_decay,
    lengths,
    norm_gain,
    mixer_out,
    channel_gain,
    expand_gate,
    expand_value,
    reduce_proj,
):
    rows_own = hidden.shape[0]
    seq_all = hidden.shape[1]
    seq_dev = states.shape[0]
    half_dim = states.shape[2]
    width = rows_own * lax.axis_size("kv") * lax.axis_size("tp")
    offset = (lax.axis_index("kv") * lax.axis_size("tp") + lax.axis_index("tp")) * rows_own
    own_start = lax.axis_index("kv") * seq_dev
    whole_rows = lax.all_gather(hidden, ("kv", "tp"), axis=0, tiled=True)
    whole_f = whole_rows.astype(jnp.float32)
    rms_in = lax.rsqrt(jnp.mean(whole_f * whole_f, axis=0) + epsilon)
    normed_in = (whole_f * mixer_gain[:, None]).astype(jnp.bfloat16)
    gate_part = (
        rms_in[:, None, None]
        * jnp.einsum("ds,dhp->shp", normed_in, gate_proj, preferred_element_type=jnp.float32)
    ).astype(jnp.bfloat16)
    inner_part = (
        rms_in[:, None, None]
        * jnp.einsum("ds,dhp->shp", normed_in, inner_proj, preferred_element_type=jnp.float32)
    ).astype(jnp.bfloat16)
    input_part = (
        rms_in[:, None]
        * jnp.einsum("ds,dk->sk", normed_in, input_proj, preferred_element_type=jnp.float32)
    ).astype(jnp.bfloat16)
    output_part = (
        rms_in[:, None]
        * jnp.einsum("ds,dk->sk", normed_in, output_proj, preferred_element_type=jnp.float32)
    ).astype(jnp.bfloat16)
    own_cols = lax.dynamic_slice_in_dim(normed_in, own_start, seq_dev, 1)
    own_rms = lax.dynamic_slice_in_dim(rms_in, own_start, seq_dev, 0)
    step_pre = (
        own_rms[:, None]
        * jnp.einsum("ds,dh->sh", own_cols, step_proj, preferred_element_type=jnp.float32)
    ).astype(jnp.bfloat16)
    gate_pre, inner_pre, input_pre, output_pre = (
        lax.all_to_all(gate_part, "kv", split_axis=0, concat_axis=1, tiled=True),
        lax.all_to_all(inner_part, "kv", split_axis=0, concat_axis=1, tiled=True),
        lax.all_to_all(input_part, "kv", split_axis=0, concat_axis=1, tiled=True),
        lax.all_to_all(output_part, "kv", split_axis=0, concat_axis=1, tiled=True),
    )
    conv_inner = short_conv(recent_inner, inner_pre, taps_inner)
    conv_input = short_conv(recent_input, input_pre, taps_input)
    conv_output = short_conv(recent_output, output_pre, taps_output).astype(jnp.bfloat16)
    step = jax.nn.softplus(step_pre.astype(jnp.float32) + step_bias[None, :])
    new_decay = -jnp.exp(decay_log)[None, :] * step
    per_group = MIXER_HEADS // GROUPS
    live = (jnp.arange(OPEN_BLOCK_SPAN, dtype=jnp.int32)[None, :] < lengths[:, None]).astype(
        jnp.float32
    )
    masked = block_decay * live[:, :, None]
    cached = jnp.sum(masked, axis=1)
    tail = new_decay[:, None, :] + cached[:, None, :] - jnp.cumsum(masked, axis=1)
    total = new_decay + cached
    readout = conv_output.reshape(seq_dev, GROUPS, STATE)
    score = jnp.einsum(
        "sgn,sjgn->sgj",
        readout,
        block_input.reshape(seq_dev, OPEN_BLOCK_SPAN, GROUPS, STATE),
        preferred_element_type=jnp.float32,
    )
    score_heads = jnp.repeat(score, per_group, axis=1)
    weight = (live[:, None, :] * jnp.exp(jnp.swapaxes(tail, 1, 2)) * score_heads).astype(
        jnp.bfloat16
    )
    from_block = jnp.einsum(
        "shj,sjhp->shp", weight, block_inner, preferred_element_type=jnp.float32
    )
    readout_f = readout.astype(jnp.float32)
    grouped = states.reshape(seq_dev, GROUPS, per_group, half_dim, STATE)
    from_state = jnp.einsum(
        "sgn,sgrpn->sgrp", readout_f, grouped, precision=lax.Precision.HIGHEST
    ).reshape(seq_dev, MIXER_HEADS, half_dim)
    own_score = jnp.repeat(
        jnp.sum(readout_f * conv_input.reshape(seq_dev, GROUPS, STATE), axis=-1), per_group, axis=1
    )
    mix = (
        from_block
        + jnp.exp(total)[:, :, None] * from_state
        + (own_score * step)[:, :, None] * conv_inner
        + skip_gain[None, :, None] * conv_inner
    )
    gated_raw = mix * jax.nn.silu(gate_pre.astype(jnp.float32))
    part_squares = jnp.sum(gated_raw * gated_raw, axis=(1, 2))
    gated = (gated_raw * norm_gain[None]).astype(jnp.bfloat16)
    placed = lax.dynamic_update_slice_in_dim(
        jnp.zeros((seq_all,), jnp.float32), part_squares, own_start, 0
    )
    gate_squares = lax.psum(placed, ("kv", "tp"))
    rms_gate = lax.rsqrt(gate_squares / (MIXER_HEADS * HEAD_DIM) + epsilon)
    by_head = lax.all_to_all(gated, "kv", split_axis=1, concat_axis=0, tiled=True)
    columns = mixer_out
    mixed_full = rms_gate[None, :] * lax.psum(
        jnp.einsum("hpd,shp->ds", columns, by_head, preferred_element_type=jnp.float32),
        ("kv", "tp"),
    )
    mid_full = (whole_f + mixed_full).astype(jnp.bfloat16)
    mid = lax.dynamic_slice_in_dim(mid_full, offset, rows_own, 0)
    full_f = mid_full.astype(jnp.float32)
    mid_squares = jnp.sum(full_f * full_f, axis=0)
    normed_full = (full_f * channel_gain[:, None]).astype(jnp.bfloat16)
    gate_sum = jnp.einsum("ds,df->sf", normed_full, expand_gate, preferred_element_type=jnp.float32)
    value_sum = jnp.einsum(
        "ds,df->sf", normed_full, expand_value, preferred_element_type=jnp.float32
    )
    rms_mid = lax.rsqrt(mid_squares / width + epsilon)
    act = (jax.nn.silu(rms_mid[:, None] * gate_sum) * (rms_mid[:, None] * value_sum)).astype(
        jnp.bfloat16
    )
    columns = reduce_proj
    channel = lax.psum_scatter(
        jnp.einsum("fd,sf->ds", columns, act, preferred_element_type=jnp.float32),
        ("kv", "tp"),
        scatter_dimension=0,
        tiled=True,
    )
    return (mid.astype(jnp.float32) + channel).astype(jnp.bfloat16)


def solution(mesh):
    return jax.shard_map(
        shards,
        mesh=mesh,
        in_specs=(
            P(("kv", "tp"), "dp"),
            P(),
            P(None, "kv", "tp"),
            P(None, "kv", "tp"),
            P(None, "kv"),
            P(None, "kv"),
            P(),
            P(),
            P(),
            P(),
            P(None, None, "tp"),
            P(),
            P(),
            P(("dp", "kv"), None, None, "tp"),
            P(("dp", "kv"), None, None),
            P(("dp", "kv"), None, None),
            P(("dp", "kv"), None, "tp", None),
            P(("dp", "kv"), None, None, "tp"),
            P(("dp", "kv"), None, None),
            P(("dp", "kv"), None, None),
            P(("dp", "kv")),
            P(None, "tp"),
            P("kv", "tp", None),
            P(),
            P(None, ("kv", "tp")),
            P(None, ("kv", "tp")),
            P(("kv", "tp"), None),
        ),
        out_specs=P(("kv", "tp"), "dp"),
        check_vma=False,
    )
```

profile of v0, /device:TPU:0, one launch (start us, length us, event | category | flops | bytes accessed | tf_op | source)
XLA Modules:
  0.0 156.3 jit_solution(15144254045306652727)
XLA Ops:
  6.5 14.7 %all_gather.3 = bf16[2048,4]{0,1:T(4,128)(2,1)S(1)} all-gather(bf16[256,4]{0,1:T(4,128)(2,1)} %param.27), channel_id=1, replica_groups=mesh['dp'=4,'kv'=4,'tp'=2] {'kv','tp'}, dimensions={0}, use_global_device_ids=true | all-gather | bytes 18432 | tf_op jit(solution)/shard_map/all_gather | solution.py:59
  21.3 0.8 fusion.15
  22.1 1.4 fusion.7
  25.4 3.4 %all-to-all-start = ((bf16[4,2,128]{2,1,0:T(2,128)(2,1)}), bf16[4,2,128]{2,1,0:T(2,128)(2,1)S(1)}, u32[]{:S(2)}, u32[]{:S(2)}) async-start(bf16[4,2,128]{2,1,0:T(2,128)(2,1)} %reshape.385), calls=%async_computation | async-start | bytes 4096 | tf_op jit(solution)/shard_map/all_to_all | solution.py:89
  29.5 1.4 fusion.6
  31.0 3.1 %fusion.1 = bf16[4,16,32]{2,0,1:T(4,128)(2,1)S(1)} fusion(bf16[2048,16,32]{0,2,1:T(8,128)(2,1)} %param.29, bf16[2048,4]{0,1:T(4,128)(2,1)S(1)} %get-tuple-element.16, f32[4]{0:T(128)S(1)} %add_rsqrt_fusion.2), kind=kOutput, calls=%fused_computation.5 | convolution fusion | flops 8392704 | bytes 2117648 | tf_op jit(solution)/shard_map/ds,dhp->shp/dot_general | solution.py:65
  34.1 1.5 fusion
  36.9 5.1 %all-to-all-start.1 = ((bf16[4,2,128]{2,1,0:T(2,128)(2,1)}), bf16[4,2,128]{2,1,0:T(2,128)(2,1)S(1)}, u32[]{:S(2)}, u32[]{:S(2)}) async-start(bf16[4,2,128]{2,1,0:T(2,128)(2,1)} %reshape.387), calls=%async_computation.1 | async-start | bytes 4096 | tf_op jit(solution)/shard_map/all_to_all | solution.py:88
  43.3 0.7 reshape.381
  44.0 0.7 reshape.383
  45.0 2.5 %all-to-all-done.1 = bf16[4,2,128]{2,1,0:T(2,128)(2,1)S(1)} async-done(((bf16[4,2,128]{2,1,0:T(2,128)(2,1)}), bf16[4,2,128]{2,1,0:T(2,128)(2,1)S(1)}, u32[]{:S(2)}, u32[]{:S(2)}) %all-to-all-start.1) | async-done | bytes 2080 | tf_op jit(solution)/shard_map/all_to_all | solution.py:88
  47.5 3.2 %all-to-all-start.2 = ((bf16[4,2,256]{2,1,0:T(2,128)(2,1)}), bf16[4,2,256]{2,1,0:T(2,128)(2,1)S(1)}, u32[]{:S(2)}, u32[]{:S(2)}) async-start(bf16[4,2,256]{2,1,0:T(2,128)(2,1)} %reshape.383), calls=%async_computation.2 | async-start | bytes 8192 | tf_op jit(solution)/shard_map/all_to_all | solution.py:87
  50.8 0.8 multiply_reduce_fusion.3
  52.2 3.4 %fusion.43 = f32[8,1,8,32]{3,1,2,0:T(1,128)S(1)} fusion(f32[8,8,32,128]{3,2,1,0:T(8,128)} %bitcast.136, bf16[8,128,1,1]{1,0,2,3:T(8,128)(2,1)S(1)} %get-tuple-element.17), kind=kOutput, calls=%fused_computation.72 | convolution fusion | flops 3145728 | bytes 1058816 | tf_op jit(solution)/shard_map/sgn,sgrpn->sgrp/dot_general | solution.py:120
  55.6 1.8 %fusion.57 = (f32[64]{0:T(128)S(1)}, f32[64]{0:T(128)S(1)}, f32[64]{0:T(128)S(1)}) fusion(f32[64]{0:T(128)} %get-tuple-element.13, f32[64]{0:T(128)} %param.35, f32[64]{0:T(128)S(1)} %broadcast_in_dim.11, f32[64]{0:T(128)} %param.34, bf16[2048,64]{0,1:T(8,128)(2,1)} %param.33, bf16[2048,4]{0,1:T(4,128)(2,1)S(1)} %get-tuple-element.16, s32[]{:T(128)S(6)} %select_n.13, ...), kind=kOutput, calls=%fused_computation.90 | convolution fusion | flops 263040 | bytes 272392 | tf_op jit(solution)/shard_map/ds,dh->sh/dot_general | solution.py:83
  57.4 0.8 fusion.19
  58.2 5.1 %all-to-all-start.3 = ((bf16[4,2,256]{2,1,0:T(2,128)(2,1)}), bf16[4,2,256]{2,1,0:T(2,128)(2,1)S(1)}, u32[]{:S(2)}, u32[]{:S(2)}) async-start(bf16[4,2,256]{2,1,0:T(2,128)(2,1)} %reshape.381), calls=%async_computation.3 | async-start | bytes 8192 | tf_op jit(solution)/shard_map/all_to_all | solution.py:86
  63.3 1.4 multiply_reduce_fusion
  65.0 3.9 %all-to-all-done.3 = bf16[4,2,256]{2,1,0:T(2,128)(2,1)S(1)} async-done(((bf16[4,2,256]{2,1,0:T(2,128)(2,1)}), bf16[4,2,256]{2,1,0:T(2,128)(2,1)S(1)}, u32[]{:S(2)}, u32[]{:S(2)}) %all-to-all-start.3) | async-done | bytes 4128 | tf_op jit(solution)/shard_map/all_to_all | solution.py:86
  69.0 1.3 multiply_reduce_fusion.2
  70.5 0.7 reduce.14
  71.2 0.7 reshape.389
  71.9 3.2 %all-to-all-start.4 = ((bf16[4,2,256]{2,1,0:T(2,128)(2,1)}), bf16[4,2,256]{2,1,0:T(2,128)(2,1)S(1)}, u32[]{:S(2)}, u32[]{:S(2)}) async-start(bf16[4,2,256]{2,1,0:T(2,128)(2,1)} %reshape.389), calls=%async_computation.4 | async-start | bytes 8192 | tf_op jit(solution)/shard_map/all_to_all | solution.py:140
  75.2 0.8 dynamic_update_slice.3
  75.9 4.7 %all-to-all-done.4 = bf16[4,2,256]{2,1,0:T(2,128)(2,1)S(1)} async-done(((bf16[4,2,256]{2,1,0:T(2,128)(2,1)}), bf16[4,2,256]{2,1,0:T(2,128)(2,1)S(1)}, u32[]{:S(2)}, u32[]{:S(2)}) %all-to-all-start.4) | async-done | bytes 4128 | tf_op jit(solution)/shard_map/all_to_all | solution.py:140
  80.8 2.0 %convolution_bitcast_fusion.1 = f32[2048,4]{0,1:T(4,128)S(1)} fusion(bf16[16,32,2048]{2,1,0:T(8,128)(2,1)} %param.49, bf16[4,16,32]{2,1,0:T(8,128)(2,1)S(1)} %bitcast.141), kind=kOutput, calls=%fused_computation.1 | convolution fusion | flops 8388608 | bytes 2134016 | tf_op jit(solution)/shard_map/hpd,shp->ds/dot_general | solution.py:143
  82.8 26.3 %all-reduce = (f32[2048,4]{0,1:T(4,128)S(1)}, f32[4]{0:T(128)S(1)}) all-reduce(f32[2048,4]{0,1:T(4,128)S(1)} %convolution_bitcast_fusion.1, f32[4]{0:T(128)S(1)} %dynamic_update_slice.3), channel_id=1, replica_groups=mesh['dp'=4,'kv'=4,'tp'=2] {'kv','tp'}, use_global_device_ids=true, to_apply=%region_9.10 | all-reduce | flops 8196 | bytes 65568 | tf_op jit(solution)/shard_map/psum | solution.py:142
  109.3 2.7 %convolution_multiply_fusion.3 = f32[4,704]{1,0:T(4,128)S(1)} fusion(bf16[2048,704]{0,1:T(8,128)(2,1)} %param.51, bf16[2048,4]{0,1:T(4,128)(2,1)S(1)} %get-tuple-element.8, f32[2048]{0:T(1024)S(1)} %copy-done.4, f32[4]{0:T(128)S(1)} %add_rsqrt_fusion), kind=kOutput, calls=%fused_computation.8 | convolution fusion | flops 11561728 | bytes 2919440 | tf_op jit(solution)/shard_map/ds,df->sf/dot_general | solution.py:151
  112.0 3.5 %convolution_bitcast_fusion = f32[2048,4]{0,1:T(4,128)S(1)} fusion(bf16[704,2048]{1,0:T(8,128)(2,1)S(1)} %copy-done, bf16[2048,704]{0,1:T(8,128)(2,1)} %param.52, f32[4,704]{1,0:T(4,128)S(1)} %convolution_multiply_fusion.3, bf16[2048,4]{0,1:T(4,128)(2,1)S(1)} %get-tuple-element.8, f32[2048]{0:T(1024)S(1)} %copy-done.4, f32[4]{0:T(128)S(1)} %add_rsqrt_fusion), kind=kOutput, calls=%fused_computation | convolution fusion | flops 23112960 | bytes 5835792 | tf_op jit(solution)/shard_map/fd,sf->ds/dot_general | solution.py:161
  115.5 1.4 copy.71
  116.9 31.0 %reduce-scatter.4.cloned.1.call-done = f32[256,4]{1,0:T(8,128)} async-done(((f32[2048,4]{1,0:T(8,128)}), f32[256,4]{1,0:T(8,128)}) %reduce-scatter.4.cloned.1.call-update) | async-done | bytes 4112
  147.8 1.0 copy.72
  (63 shorter events, 7.1 us)
Async XLA Ops:
  6.5 105.4 %copy-start = (bf16[704,2048]{1,0:T(8,128)(2,1)S(1)}, bf16[704,2048]{1,0:T(8,128)(2,1)}, u32[]{:S(2)}) copy-start(bf16[704,2048]{1,0:T(8,128)(2,1)} %param.53) | copy-start | bytes 8650756
  23.5 13.3 %copy-start.5 = (f32[1,128,64]{1,2,0:T(8,128)S(1)}, f32[1,128,64]{1,2,0:T(8,128)}, u32[]{:S(2)}) copy-start(f32[1,128,64]{1,2,0:T(8,128)} %param.46) | copy-start | bytes 98308
  23.5 21.1 %copy-start.2 = (bf16[1,128,1024]{2,1,0:T(8,128)(2,1)S(1)}, bf16[1,128,1024]{2,1,0:T(8,128)(2,1)}, u32[]{:S(2)}) copy-start(bf16[1,128,1024]{2,1,0:T(8,128)(2,1)} %param.45) | copy-start | bytes 786436
  25.4 11.5 %all-to-all-start = ((bf16[4,2,128]{2,1,0:T(2,128)(2,1)}), bf16[4,2,128]{2,1,0:T(2,128)(2,1)S(1)}, u32[]{:S(2)}, u32[]{:S(2)}) async-start(bf16[4,2,128]{2,1,0:T(2,128)(2,1)} %reshape.385), calls=%async_computation | async-start | bytes 4096 | tf_op jit(solution)/shard_map/all_to_all | solution.py:89
  28.7 5.3 %copy-start.1 = (bf16[2048,16,32]{0,2,1:T(8,128)(2,1)S(1)}, bf16[2048,16,32]{0,2,1:T(8,128)(2,1)}, u32[]{:S(2)}) copy-start(bf16[2048,16,32]{0,2,1:T(8,128)(2,1)} %param.30) | copy-start | bytes 6291460
  34.1 34.9 %copy-start.6 = (bf16[1,3,64,32]{2,3,1,0:T(8,128)(2,1)S(1)}, bf16[1,3,64,32]{2,3,1,0:T(8,128)(2,1)}, u32[]{:S(2)}) copy-start(bf16[1,3,64,32]{2,3,1,0:T(8,128)(2,1)} %param.40) | copy-start | bytes 36868
  34.1 36.2 %copy-start.7 = (f32[64,32]{0,1:T(8,128)S(1)}, f32[64,32]{0,1:T(8,128)}, u32[]{:S(2)}) copy-start(f32[64,32]{0,1:T(8,128)} %param.48) | copy-start | bytes 24580
  35.6 8.4 %copy-start.8 = (f32[128]{0:T(128)}, f32[128]{0:T(128)S(1)}, u32[]{:S(2)}) copy-start(f32[128]{0:T(128)S(1)} %compare_convert_fusion) | copy-start | bytes 1540
  36.9 10.6 %all-to-all-start.1 = ((bf16[4,2,128]{2,1,0:T(2,128)(2,1)}), bf16[4,2,128]{2,1,0:T(2,128)(2,1)S(1)}, u32[]{:S(2)}, u32[]{:S(2)}) async-start(bf16[4,2,128]{2,1,0:T(2,128)(2,1)} %reshape.387), calls=%async_computation.1 | async-start | bytes 4096 | tf_op jit(solution)/shard_map/all_to_all | solution.py:88
  44.8 24.2 %copy-start.3 = (f32[4,64,32]{1,2,0:T(8,128)S(1)}, f32[4,64,32]{1,2,0:T(8,128)}, u32[]{:S(2)}) copy-start(f32[4,64,32]{1,2,0:T(8,128)} %param.37) | copy-start | bytes 98308
  47.5 10.7 %all-to-all-start.2 = ((bf16[4,2,256]{2,1,0:T(2,128)(2,1)}), bf16[4,2,256]{2,1,0:T(2,128)(2,1)S(1)}, u32[]{:S(2)}, u32[]{:S(2)}) async-start(bf16[4,2,256]{2,1,0:T(2,128)(2,1)} %reshape.383), calls=%async_computation.2 | async-start | bytes 8192 | tf_op jit(solution)/shard_map/all_to_all | solution.py:87
  50.8 58.5 %copy-start.4 = (f32[2048]{0:T(1024)S(1)}, f32[2048]{0:T(1024)}, u32[]{:S(2)}) copy-start(f32[2048]{0:T(1024)} %param.50) | copy-start | bytes 24580
  58.2 10.6 %all-to-all-start.3 = ((bf16[4,2,256]{2,1,0:T(2,128)(2,1)}), bf16[4,2,256]{2,1,0:T(2,128)(2,1)S(1)}, u32[]{:S(2)}, u32[]{:S(2)}) async-start(bf16[4,2,256]{2,1,0:T(2,128)(2,1)} %reshape.381), calls=%async_computation.3 | async-start | bytes 8192 | tf_op jit(solution)/shard_map/all_to_all | solution.py:86
  71.9 8.8 %all-to-all-start.4 = ((bf16[4,2,256]{2,1,0:T(2,128)(2,1)}), bf16[4,2,256]{2,1,0:T(2,128)(2,1)S(1)}, u32[]{:S(2)}, u32[]{:S(2)}) async-start(bf16[4,2,256]{2,1,0:T(2,128)(2,1)} %reshape.389), calls=%async_computation.4 | async-start | bytes 8192 | tf_op jit(solution)/shard_map/all_to_all | solution.py:140
  75.1 72.7 %reduce-scatter.4.cloned.1.call-start = ((), (), s32[]{:S(2)}) async-start(), calls=%async_computation.6 | async-start | bytes 1179648
Sparse Core Ops, SparseCore 0:
  117.0 30.8 reduce-scatter.3
where the time goes:
time: 157 us; the launch traced here: 156 us
  waiting for transfers between devices  42.1 us (27%)
  blocking collectives  41 us (26%)
  matrix products  20.9 us (13%)
  starting transfers between devices  20 us (13%)
  between operations  14.4 us (9%)
  other arithmetic  8.9 us (6%)
  local copies, waits for them, and re-layouts  8.85 us (6%)
    unnamed x2, waiting for transfers between devices  31 us
    psum x1, blocking collectives, shards(): lax.psum(jnp.einsum('hpd,shp->ds', columns, by_head, preferred_element_ty...  26.3 us
    all_gather x1, blocking collectives, shards(): whole_rows = lax.all_gather(hidden, ('kv', 'tp'), axis=0, tiled=True)  14.7 us
    unnamed x33, local copies, waits for them, and re-layouts  6.14 us
    all_to_all x1, starting transfers between devices, shards(): lax.all_to_all(input_part, 'kv', split_axis=0, concat_axis=1, tiled=True)  5.1 us
    all_to_all x1, starting transfers between devices, shards(): lax.all_to_all(gate_part, 'kv', split_axis=0, concat_axis=1, tiled=True)  5.06 us
    all_to_all x1, waiting for transfers between devices, shards(): lax.all_to_all(gated, 'kv', split_axis=1, concat_axis=0, tiled=True)  4.73 us
    all_to_all x1, waiting for transfers between devices, shards(): lax.all_to_all(gate_part, 'kv', split_axis=0, concat_axis=1, tiled=True)  3.87 us
  transfers between devices with their start and end apart: 6, of which 4 were waited for; matrix products, arithmetic and copies ran while one was open for 13% of the time, Pallas kernels for 0%

commit v1 on v0

--- a/solution.py
+++ b/solution.py
@@ -1,6 +1,10 @@
+import functools
+
 import jax
 import jax.numpy as jnp
 from jax import lax
+from jax.experimental import pallas as pl
+from jax.experimental.pallas import tpu as pltpu
 from jax.sharding import PartitionSpec as P
 
 MIXER_HEADS = 64
@@ -20,7 +24,7 @@
     return jax.nn.silu(jnp.sum(window * taps[None], axis=1))
 
 
-def shards(
+def general(
     hidden,
     mixer_gain,
     gate_proj,
@@ -166,9 +170,336 @@
     return (mid.astype(jnp.float32) + channel).astype(jnp.bfloat16)
 
 
+NT = (((1,), (1,)), ((), ()))
+NN = (((1,), (0,)), ((), ()))
+LANES = 128
+
+
+def dot(a, b, dims, precision=None):
+    return lax.dot_general(a, b, dims, precision=precision, preferred_element_type=jnp.float32)
+
+
+def silu(v):
+    return v / (1.0 + jnp.exp(-v))
+
+
+def tree(values):
+    values = list(values)
+    while len(values) > 1:
+        values = [a + b for a, b in zip(values[::2], values[1::2])]
+    return values[0]
+
+
+def call(body, outs, args, scratch=(), scalars=(), flops=0):
+    args = [
+        a if i in scalars else pltpu.with_memory_space_constraint(a, pltpu.VMEM)
+        for i, a in enumerate(args)
+    ]
+    return pl.pallas_call(
+        body,
+        out_shape=[pltpu.VMEM(s, d) for s, d in outs],
+        in_specs=[
+            pl.BlockSpec(memory_space=pltpu.SMEM if i in scalars else pltpu.VMEM)
+            for i in range(len(args))
+        ],
+        out_specs=[pl.BlockSpec(memory_space=pltpu.VMEM) for _ in outs],
+        scratch_shapes=[pltpu.VMEM(s, d) for s, d in scratch],
+        compiler_params=pltpu.CompilerParams(vmem_limit_bytes=8 << 20),
+        cost_estimate=pl.CostEstimate(flops=flops, bytes_accessed=0, transcendentals=0),
+    )(*args)
+
+
+def lane(start, size):
+    return pl.ds(pl.multiple_of(start, LANES), size)
+
+
+def project(n, *refs):
+    pieces, refs = refs[:n], refs[n:]
+    mixer_gain, gate_w, inner_w, input_w, output_w, step_w = refs[:6]
+    x_out, step_out = refs[6:8]
+    sends = refs[8:]
+    kv, tp = lax.axis_index("kv"), lax.axis_index("tp")
+    width = x_out.shape[1]
+    part = pieces[0].shape[1] // 2
+    for k, ref in enumerate(pieces):
+        base = (kv ^ k) * (2 * part)
+        x_out[:, lane(base + tp * part, part)] = ref[:, :part]
+        x_out[:, lane(base + (1 - tp) * part, part)] = ref[:, part:]
+    x = x_out[...].astype(jnp.float32)
+    rms = lax.rsqrt(jnp.sum(x * x, axis=1, keepdims=True) / width + epsilon)
+    normed = (x * mixer_gain[...]).astype(jnp.bfloat16)
+    at = 0
+    for weight, dims in ((gate_w, NT), (inner_w, NT), (input_w, NN), (output_w, NN)):
+        value = rms * dot(normed, weight[...], dims)
+        value = value.astype(jnp.bfloat16).astype(jnp.float32)
+        row = lax.broadcasted_iota(jnp.int32, value.shape, 0)
+        for k, ref in enumerate(sends):
+            picked = jnp.sum(jnp.where(row == (kv ^ k), value, 0.0), axis=0, keepdims=True)
+            ref[:, at : at + value.shape[1]] = picked
+        at += value.shape[1]
+    steps = (rms * dot(normed, step_w[...], NT)).astype(jnp.bfloat16).astype(jnp.float32)
+    row = lax.broadcasted_iota(jnp.int32, steps.shape, 0)
+    step_out[...] = jnp.sum(jnp.where(row == kv, steps, 0.0), axis=0, keepdims=True)
+
+
+def mixer(n, length, *refs):
+    pieces, refs = refs[:n], refs[n:]
+    step_pre, step_bias, decay_log, skip_gain = refs[:4]
+    taps_inner, taps_input, taps_output = refs[4:7]
+    recent_inner, recent_input, recent_output = refs[7:10]
+    states, block_inner, block_input, block_decay, norm_gain = refs[10:15]
+    sends, (gate_row, inner_row, input_row, output_row, gated_row) = refs[15:-5], refs[-5:]
+    kv = lax.axis_index("kv")
+    heads, span = block_decay.shape
+    channels = gate_row.shape[1]
+    half = channels // heads
+    size = states.shape[1]
+    groups = block_input.shape[1] // size
+    per_group = heads // groups
+    chunk = per_group * half
+    cols, maps = channels // n, input_row.shape[1] // n
+    for k, ref in enumerate(pieces):
+        src = kv ^ k
+        gate_row[:, lane(src * cols, cols)] = ref[:, :cols]
+        inner_row[:, lane(src * cols, cols)] = ref[:, cols : 2 * cols]
+        input_row[:, lane(src * maps, maps)] = ref[:, 2 * cols : 2 * cols + maps]
+        output_row[:, lane(src * maps, maps)] = ref[:, 2 * cols + maps :]
+
+    def conv(recent, newest, taps):
+        weights = taps[...]
+        past = jnp.sum(recent[...].astype(jnp.float32) * weights[:-1], axis=0, keepdims=True)
+        return silu(past + weights[-1:] * newest)
+
+    conv_output = conv(recent_output, output_row[...], taps_output).astype(jnp.bfloat16)
+    conv_input = conv(recent_input, input_row[...], taps_input)
+    conv_inner = conv(recent_inner, inner_row[...], taps_inner)
+    readout = conv_output.astype(jnp.float32)
+
+    eye = lax.broadcasted_iota(jnp.int32, (heads, heads), 0) == lax.broadcasted_iota(
+        jnp.int32, (heads, heads), 1
+    )
+
+    def column(row):
+        return jnp.sum(jnp.where(eye, row, 0.0), axis=1, keepdims=True)
+
+    pre = step_pre[...] + step_bias[...]
+    step_row = jnp.maximum(pre, 0.0) + jnp.log1p(jnp.exp(-jnp.abs(pre)))
+    step = column(step_row)
+    new_decay = column(-jnp.exp(decay_log[...]) * step_row)
+    skip = column(skip_gain[...])
+
+    live = (lax.broadcasted_iota(jnp.int32, (1, span), 1) < length[0]).astype(jnp.float32)
+    masked = block_decay[...] * live
+    later = (
+        lax.broadcasted_iota(jnp.int32, (span, span), 0)
+        > lax.broadcasted_iota(jnp.int32, (span, span), 1)
+    ).astype(jnp.float32)
+    suffix = dot(masked, later, NN, lax.Precision.HIGHEST)
+    grown = jnp.exp(new_decay + jnp.sum(masked, axis=1, keepdims=True))
+    decayed = live * jnp.exp(new_decay + suffix)
+
+    wide = (groups, groups * size)
+    diagonal = lax.broadcasted_iota(jnp.int32, wide, 1) // size == lax.broadcasted_iota(
+        jnp.int32, wide, 0
+    )
+    spread = jnp.where(diagonal, readout, 0.0)
+    score = dot(spread.astype(jnp.bfloat16), block_input[...], NT)
+    own_score = jnp.sum(spread * conv_input, axis=1, keepdims=True)
+
+    narrow = (per_group, chunk)
+    mine = lax.broadcasted_iota(jnp.int32, narrow, 1) // half == lax.broadcasted_iota(
+        jnp.int32, narrow, 0
+    )
+    squares = jnp.zeros((1, chunk), jnp.float32)
+    for g in range(groups):
+        head = slice(g * per_group, (g + 1) * per_group)
+        rows = slice(g * chunk, (g + 1) * chunk)
+        weight = (decayed[head] * score[g : g + 1]).astype(jnp.bfloat16)
+        from_block = dot(weight, block_inner[rows, :], NT)
+        state = states[rows, :]
+        high = state.astype(jnp.bfloat16)
+        low = (state - high.astype(jnp.float32)).astype(jnp.bfloat16)
+        out_map = jnp.broadcast_to(
+            readout[:, g * size : (g + 1) * size], (per_group, size)
+        ).astype(jnp.bfloat16)
+        from_state = dot(out_map, high, NT) + dot(out_map, low, NT)
+        direct = own_score[g : g + 1] * step[head] + skip[head]
+        both = from_block + grown[head] * from_state + direct * conv_inner[:, rows]
+        mix = jnp.sum(jnp.where(mine, both, 0.0), axis=0, keepdims=True)
+        raw = mix * silu(gate_row[:, rows])
+        squares = squares + raw * raw
+        gated_row[:, rows] = (raw * norm_gain[:, rows]).astype(jnp.bfloat16).astype(jnp.float32)
+    square = jnp.sum(squares, axis=1, keepdims=True)
+    for k, ref in enumerate(sends):
+        ref[:, :cols] = gated_row[:, lane((kv ^ k) * cols, cols)]
+        ref[:, cols:] = jnp.broadcast_to(square, (1, LANES))
+
+
+def out_project(n, *refs):
+    pieces, (mixer_out, out, rows) = refs[:n], refs[n:]
+    kv = lax.axis_index("kv")
+    cols, width = mixer_out.shape
+    for k, ref in enumerate(pieces):
+        rows[pl.ds(kv ^ k, 1), :] = ref[...]
+    out[:, :width] = dot(rows[:, :cols].astype(jnp.bfloat16), mixer_out[...], NN)
+    out[:, width:] = rows[:, cols:]
+
+
+def add_pair(a, b, out):
+    out[...] = a[...] + b[...]
+
+
+def channel_mix(n, channels, *refs):
+    pieces, (x, gain, gate_w, value_w, reduce_w) = refs[:n], refs[n : n + 5]
+    mid_out, keep, send, moved = refs[n + 5 :]
+    kv, tp = lax.axis_index("kv"), lax.axis_index("tp")
+    width = x.shape[1]
+    part = mid_out.shape[1]
+    whole = tree(ref[:, :width] for ref in pieces)
+    rms_gate = lax.rsqrt(pieces[0][:, width : width + 1] / channels + epsilon)
+    mid = (x[...].astype(jnp.float32) + rms_gate * whole).astype(jnp.bfloat16)
+    mid = mid.astype(jnp.float32)
+    rms = lax.rsqrt(jnp.sum(mid * mid, axis=1, keepdims=True) / width + epsilon)
+    normed = (mid * gain[...]).astype(jnp.bfloat16)
+    moved[...] = mid
+    mid_out[...] = moved[:, lane((kv * 2 + tp) * part, part)]
+    act = silu(rms * dot(normed, gate_w[...], NT)) * (rms * dot(normed, value_w[...], NT))
+    moved[...] = dot(act.astype(jnp.bfloat16), reduce_w[...], NN)
+    for i in range(n):
+        at = slice(i * part, (i + 1) * part)
+        keep[:, at] = moved[:, lane((2 * i + tp) * part, part)]
+        send[:, at] = moved[:, lane((2 * i + 1 - tp) * part, part)]
+
+
+def split_pair(n, a, b, *outs):
+    *outs, moved = outs
+    kv = lax.axis_index("kv")
+    part = outs[0].shape[1]
+    moved[...] = a[...] + b[...]
+    for k, ref in enumerate(outs):
+        ref[...] = moved[:, lane((kv ^ k) * part, part)]
+
+
+def finish(n, *refs):
+    pieces, (mid, out) = refs[:n], refs[n:]
+    out[...] = (mid[...] + tree(ref[...] for ref in pieces)).astype(jnp.bfloat16)
+
+
+def across(label, values):
+    n = len(values)
+    got = [values[0]] + [None] * (n - 1)
+    for k in reversed(range(1, n)):
+        with jax.named_scope(f"{label}_{k}"):
+            got[k] = lax.ppermute(values[k], "kv", [(i, i ^ k) for i in range(n)])
+    return got
+
+
+def beside(label, value):
+    with jax.named_scope(label):
+        return lax.ppermute(value, "tp", [(0, 1), (1, 0)])
+
+
+def layer(*args):
+    (
+        hidden, mixer_gain, gate_proj, inner_proj, input_proj, output_proj, step_proj, step_bias,
+        decay_log, skip_gain, taps_inner, taps_input, taps_output, recent_inner, recent_input,
+        recent_output, states, block_inner, block_input, block_decay, lengths, norm_gain, mixer_out,
+        channel_gain, expand_gate, expand_value, reduce_proj,
+    ) = args
+    n = lax.axis_size("kv")
+    part, seqs = hidden.shape
+    width = part * n * 2
+    heads, half, size = states.shape[1:]
+    channels = heads * half
+    cols, maps = channels // n, input_proj.shape[1]
+    aligned = all(v % LANES == 0 for v in (part, cols, maps, width, size, block_decay.shape[1]))
+    if not (
+        n & (n - 1) == 0
+        and lax.axis_size("tp") == 2
+        and states.shape[0] == 1
+        and seqs == n
+        and aligned
+    ):
+        return general(*args)
+    f32, bf16 = jnp.float32, jnp.bfloat16
+    x = hidden.T
+    pair = jnp.concatenate([x, beside("in_tp", x)], axis=1)
+    pieces = across("in", [pair] * n)
+    whole, step_pre, *sends = call(
+        functools.partial(project, n),
+        [((seqs, width), bf16), ((1, heads), f32)] + [((1, 2 * cols + 2 * maps), f32)] * n,
+        pieces
+        + [
+            mixer_gain.reshape(1, width),
+            gate_proj.transpose(1, 2, 0).reshape(cols, width),
+            inner_proj.transpose(1, 2, 0).reshape(cols, width),
+            input_proj,
+            output_proj,
+            step_proj.T,
+        ],
+        flops=2 * seqs * width * (2 * cols + 2 * maps),
+    )
+    pieces = across("pre", sends)
+    sends = call(
+        functools.partial(mixer, n),
+        [((1, cols + LANES), f32)] * n,
+        [lengths]
+        + pieces
+        + [
+            step_pre,
+            step_bias.reshape(1, heads),
+            decay_log.reshape(1, heads),
+            skip_gain.reshape(1, heads),
+            taps_inner.reshape(-1, channels),
+            taps_input,
+            taps_output,
+            recent_inner.reshape(-1, channels),
+            recent_input[0],
+            recent_output[0],
+            states.reshape(channels, size),
+            block_inner.transpose(0, 2, 3, 1).reshape(channels, -1),
+            block_input[0],
+            block_decay[0].T,
+            norm_gain.reshape(1, channels),
+        ],
+        scratch=[((1, channels), f32)] * 2 + [((1, n * maps), f32)] * 2 + [((1, channels), f32)],
+        scalars=(0,),
+        flops=1 << 24,
+    )
+    pieces = across("gated", sends)
+    (mixed,) = call(
+        functools.partial(out_project, n),
+        [((seqs, width + LANES), f32)],
+        pieces + [mixer_out.reshape(cols, width)],
+        scratch=[((seqs, cols + LANES), f32)],
+        flops=2 * seqs * width * cols,
+    )
+    (mixed,) = call(
+        add_pair, [((seqs, width + LANES), f32)], [mixed, beside("mixed_tp", mixed)]
+    )
+    pieces = across("mixed", [mixed] * n)
+    mid, keep, send = call(
+        functools.partial(channel_mix, n, 2 * channels),
+        [((seqs, part), f32)] + [((seqs, width // 2), f32)] * 2,
+        pieces
+        + [whole, channel_gain.reshape(1, width), expand_gate.T, expand_value.T, reduce_proj],
+        scratch=[((seqs, width), f32)],
+        flops=6 * seqs * width * reduce_proj.shape[0],
+    )
+    sends = call(
+        functools.partial(split_pair, n),
+        [((seqs, part), f32)] * n,
+        [keep, beside("down_tp", send)],
+        scratch=[((seqs, width // 2), f32)],
+    )
+    pieces = across("down", sends)
+    (out,) = call(functools.partial(finish, n), [((seqs, part), bf16)], pieces + [mid])
+    return out.T
+
+
 def solution(mesh):
     return jax.shard_map(
-        shards,
+        layer,
         mesh=mesh,
         in_specs=(
             P(("kv", "tp"), "dp"),

time: 157 us -> 77.9 us (0.50)
  blocking collectives: 41 us -> 0 us
  waiting for transfers between devices: 42.1 us -> 18.1 us
  matrix products: 20.9 us -> 0 us
  local copies, waits for them, and re-layouts: 8.85 us -> 27.6 us
  between operations: 14.4 us -> 0.81 us
  other arithmetic: 8.9 us -> 0.69 us
  Pallas kernels: 0 us -> 6.16 us
  starting transfers between devices: 20 us -> 23.6 us
    unnamed x2 -> x0, waiting for transfers between devices: 31 us -> none
    psum x1 -> x0, blocking collectives: 26.3 us -> none  [shards(): lax.psum(jnp.einsum('hpd,shp->ds', columns, by_head, preferred_element_ty...]
    ppermute x0 -> x18, starting transfers between devices: none -> 23.6 us  [the longest x15 23.1 us: across(): got[k] = lax.ppermute(values[k], 'kv', [(i, i ^ k) for i in range(n)])]
    dot_general x10 -> x0, matrix products: 20.9 us -> none  [the longest x1 3.49 us: shards(): jnp.einsum('fd,sf->ds', columns, act, preferred_element_type=jnp.float32)]
    all_to_all x5 -> x0, starting transfers between devices: 20 us -> none  [the longest x1 5.1 us: shards(): lax.all_to_all(input_part, 'kv', split_axis=0, concat_axis=1, tiled=True)]
    unnamed x33 -> x58, local copies, waits for them, and re-layouts: 6.14 us -> 24.8 us
    ppermute x0 -> x18, waiting for transfers between devices: none -> 18.1 us  [the longest x15 14.7 us: across(): got[k] = lax.ppermute(values[k], 'kv', [(i, i ^ k) for i in range(n)])]
    all_gather x1 -> x0, blocking collectives: 14.7 us -> none  [shards(): whole_rows = lax.all_gather(hidden, ('kv', 'tp'), axis=0, tiled=True)]
  transfers between devices with their start and end apart: 6 -> 18, of which waited for: 4 -> 11; matrix products, arithmetic and copies ran while one was open for 13% -> 8% of each run, Pallas kernels for 0% -> 0%
where the time goes in v1:
time: 77.9 us; the launch traced here: 76.9 us
  local copies, waits for them, and re-layouts  27.6 us (35%)
  starting transfers between devices  23.6 us (30%)
  waiting for transfers between devices  18.1 us (23%)
  Pallas kernels  6.16 us (8%)
  between operations  0.81 us (1%)
    unnamed x58, local copies, waits for them, and re-layouts  24.8 us
    ppermute x15, starting transfers between devices, across(): got[k] = lax.ppermute(values[k], 'kv', [(i, i ^ k) for i in range(n)])  23.1 us
    ppermute x15, waiting for transfers between devices, across(): got[k] = lax.ppermute(values[k], 'kv', [(i, i ^ k) for i in range(n)])  14.7 us
    pallas_call x7, Pallas kernels, call(): pl.pallas_call(body, out_shape=[pltpu.VMEM(s, d) for s, d in outs], in_sp...  6.16 us
    ppermute x3, waiting for transfers between devices, beside(): return lax.ppermute(value, 'tp', [(0, 1), (1, 0)])  3.45 us
  transfers between devices with their start and end apart: 18, of which 11 were waited for; matrix products, arithmetic and copies ran while one was open for 8% of the time, Pallas kernels for 0%

profile of v1, /device:TPU:0, one launch (start us, length us, event | category | flops | bytes accessed | tf_op | source)
XLA Modules:
  0.0 76.9 jit_solution(9371095932874673811)
XLA Ops:
  0.5 1.0 %collective-permute-done = bf16[4,256]{1,0:T(4,128)(2,1)S(1)} collective-permute-done((bf16[4,256]{1,0:T(4,128)(2,1)}, bf16[4,256]{1,0:T(4,128)(2,1)S(1)}, u32[]{:S(2)}, u32[]{:S(2)}) %collective-permute-start) | collective-permute-done | bytes 2080 | tf_op jit(solution)/shard_map/in_tp/ppermute | solution.py:399
  2.2 2.9 %collective-permute-start.1 = (bf16[4,512]{1,0:T(4,128)(2,1)S(1)}, bf16[4,512]{1,0:T(4,128)(2,1)S(1)}, u32[]{:S(2)}, u32[]{:S(2)}) collective-permute-start(bf16[4,512]{1,0:T(4,128)(2,1)S(1)} %pad_maximum_fusion.refs_0_), channel_id=1, source_target_pairs={{0,2},{2,0},{4,6},{6,4},{1,3},{3,1},{5,7},{7,5},{8,10},{10,8},{12,... | collective-permute-start | bytes 12296 | tf_op jit(solution)/shard_map/in_1/ppermute | solution.py:393
  5.1 2.6 %collective-permute-start.2 = (bf16[4,512]{1,0:T(4,128)(2,1)S(1)}, bf16[4,512]{1,0:T(4,128)(2,1)S(1)}, u32[]{:S(2)}, u32[]{:S(2)}) collective-permute-start(bf16[4,512]{1,0:T(4,128)(2,1)S(1)} %pad_maximum_fusion.refs_0_), channel_id=1, source_target_pairs={{0,4},{2,6},{4,0},{6,2},{1,5},{3,7},{5,1},{7,3},{8,12},{10,14},{12... | collective-permute-start | bytes 12296 | tf_op jit(solution)/shard_map/in_2/ppermute | solution.py:393
  7.7 1.9 %collective-permute-done.2.refs_2_ = bf16[4,512]{1,0:T(4,128)(2,1)S(1)} collective-permute-done((bf16[4,512]{1,0:T(4,128)(2,1)S(1)}, bf16[4,512]{1,0:T(4,128)(2,1)S(1)}, u32[]{:S(2)}, u32[]{:S(2)}) %collective-permute-start.2) | collective-permute-done | bytes 4128 | tf_op jit(solution)/shard_map/in_2/ppermute | solution.py:393
  9.6 3.5 %collective-permute-done.3.refs_3_ = bf16[4,512]{1,0:T(4,128)(2,1)S(1)} collective-permute-done((bf16[4,512]{1,0:T(4,128)(2,1)S(1)}, bf16[4,512]{1,0:T(4,128)(2,1)S(1)}, u32[]{:S(2)}, u32[]{:S(2)}) %collective-permute-start.3) | collective-permute-done | bytes 4128 | tf_op jit(solution)/shard_map/in_3/ppermute | solution.py:393
  13.1 1.6 %copy-done.3 = bf16[2048,16,32]{0,2,1:T(8,128)(2,1)S(1)} copy-done((bf16[2048,16,32]{0,2,1:T(8,128)(2,1)S(1)}, bf16[2048,16,32]{0,2,1:T(8,128)(2,1)}, u32[]{:S(2)}) %copy-start.3) | copy-done | bytes 2097176
  14.7 1.6 %copy-done.4 = bf16[2048,16,32]{0,2,1:T(8,128)(2,1)S(1)} copy-done((bf16[2048,16,32]{0,2,1:T(8,128)(2,1)S(1)}, bf16[2048,16,32]{0,2,1:T(8,128)(2,1)}, u32[]{:S(2)}) %copy-start.4) | copy-done | bytes 2097176
  16.3 1.2 %copy-done.6 = bf16[2048,256]{1,0:T(8,128)(2,1)S(1)} copy-done((bf16[2048,256]{1,0:T(8,128)(2,1)S(1)}, bf16[2048,256]{1,0:T(8,128)(2,1)}, u32[]{:S(2)}) %copy-start.6) | copy-done | bytes 1048600
  17.5 1.2 %copy-done.7 = bf16[2048,256]{1,0:T(8,128)(2,1)S(1)} copy-done((bf16[2048,256]{1,0:T(8,128)(2,1)S(1)}, bf16[2048,256]{1,0:T(8,128)(2,1)}, u32[]{:S(2)}) %copy-start.7) | copy-done | bytes 1048600
  18.7 0.9 %copy-done.10 = bf16[2048,64]{0,1:T(8,128)(2,1)S(1)} copy-done((bf16[2048,64]{0,1:T(8,128)(2,1)S(1)}, bf16[2048,64]{0,1:T(8,128)(2,1)}, u32[]{:S(2)}) %copy-start.10) | copy-done | bytes 262168
  20.4 2.2 %shard_map.253 = (bf16[4,2048]{1,0:T(4,128)(2,1)S(1)}, f32[1,64]{1,0:T(1,128)S(1)}, f32[1,1536]{1,0:T(1,128)S(1)}, f32[1,1536]{1,0:T(1,128)}, f32[1,1536]{1,0:T(1,128)}, /*index=5*/f32[1,1536]{1,0:T(1,128)}) custom-call(bf16[4,512]{1,0:T(4,128)(2,1)S(1)} %pad_maximum_fusion.refs_0_, bf16[4,512]{1,0:T(4,128)(2,1)S(1)} %collective-permute-done.1.refs_1_, ...), custom_call_target="tpu_custom_call" | custom-call | flops 25165824 | tf_op jit(solution)/shard_map/pallas_call | solution.py:198
  24.3 3.8 %collective-permute-start.6 = (f32[1,1536]{1,0:T(1,128)}, f32[1,1536]{1,0:T(1,128)}, u32[]{:S(2)}, u32[]{:S(2)}) collective-permute-start(f32[1,1536]{1,0:T(1,128)} %get-tuple-element.25), channel_id=1, source_target_pairs={{0,6},{2,4},{4,2},{6,0},{1,7},{3,5},{5,3},{7,1},{8,14},{10,12},{12... | collective-permute-start | bytes 18440 | tf_op jit(solution)/shard_map/pre_3/ppermute | solution.py:393
  28.1 1.6 %copy.31 = f32[4,64,32]{2,1,0:T(8,128)} copy(f32[4,64,32]{1,2,0:T(8,128)} %param.37) | data formatting | bytes 65536 | tf_op args[10]
  29.7 1.0 %reshape.45.refs_8_ = f32[4,2048]{1,0:T(4,128)S(1)} reshape(f32[4,64,32]{2,1,0:T(8,128)} %copy.31) | data formatting | bytes 65536 | tf_op jit(solution)/shard_map/reshape | solution.py:453
  32.3 1.4 %copy.33 = f32[64,32]{1,0:T(8,128)} copy(f32[64,32]{0,1:T(8,128)} %param.48) | data formatting | bytes 16384 | tf_op args[21]
  35.3 1.2 %copy-done.8 = f32[1,64,32,128]{3,2,1,0:T(8,128)S(1)} copy-done((f32[1,64,32,128]{3,2,1,0:T(8,128)S(1)}, f32[1,64,32,128]{3,2,1,0:T(8,128)}, u32[]{:S(2)}) %copy-start.8) | copy-done | bytes 1048600
  36.5 0.9 %copy-done.11 = bf16[1,128,1024]{2,1,0:T(8,128)(2,1)S(1)} copy-done((bf16[1,128,1024]{2,1,0:T(8,128)(2,1)S(1)}, bf16[1,128,1024]{2,1,0:T(8,128)(2,1)}, u32[]{:S(2)}) %copy-start.11) | copy-done | bytes 262168
  41.5 1.6 %shard_map.254 = (f32[1,640]{1,0:T(1,128)S(1)}, f32[1,640]{1,0:T(1,128)S(1)}, f32[1,640]{1,0:T(1,128)S(1)}, f32[1,640]{1,0:T(1,128)S(1)}) custom-call(s32[1]{0:T(128)S(6)} %copy.35.length, f32[1,1536]{1,0:T(1,128)S(1)} %copy-done.20, f32[1,1536]{1,0:T(1,128)} %collective-permute-done.4.refs_1_, f32[1,1536]{1,0:T(1,128)} %collective-permute-done.5.refs_2_, ...), custom_call_target="tpu_custom_call" | custom-call | flops 16777216 | tf_op jit(solution)/shard_map/pallas_call | solution.py:198
  43.7 3.8 %collective-permute-start.9 = (f32[1,640]{1,0:T(1,128)S(1)}, f32[1,640]{1,0:T(1,128)S(1)}, u32[]{:S(2)}, u32[]{:S(2)}) collective-permute-start(f32[1,640]{1,0:T(1,128)S(1)} %get-tuple-element.30), channel_id=1, source_target_pairs={{0,6},{2,4},{4,2},{6,0},{1,7},{3,5},{5,3},{7,1},{8,14},{10,12},{12... | collective-permute-start | bytes 7688 | tf_op jit(solution)/shard_map/gated_3/ppermute | solution.py:393
  47.6 1.4 %collective-permute-done.9.refs_3_ = f32[1,640]{1,0:T(1,128)S(1)} collective-permute-done((f32[1,640]{1,0:T(1,128)S(1)}, f32[1,640]{1,0:T(1,128)S(1)}, u32[]{:S(2)}, u32[]{:S(2)}) %collective-permute-start.9) | collective-permute-done | bytes 2592 | tf_op jit(solution)/shard_map/gated_3/ppermute | solution.py:393
  49.1 1.6 %copy-done.5 = bf16[16,32,2048]{2,1,0:T(8,128)(2,1)S(1)} copy-done((bf16[16,32,2048]{2,1,0:T(8,128)(2,1)S(1)}, bf16[16,32,2048]{2,1,0:T(8,128)(2,1)}, u32[]{:S(2)}) %copy-start.5) | copy-done | bytes 2097176
  51.0 1.2 %collective-permute-done.10.b = f32[4,2176]{1,0:T(4,128)S(1)} collective-permute-done((f32[4,2176]{1,0:T(4,128)S(1)}, f32[4,2176]{1,0:T(4,128)S(1)}, u32[]{:S(2)}, u32[]{:S(2)}) %collective-permute-start.10) | collective-permute-done | bytes 34848 | tf_op jit(solution)/shard_map/mixed_tp/ppermute | solution.py:399
  52.8 3.8 %collective-permute-start.12 = (f32[4,2176]{1,0:T(4,128)S(1)}, f32[4,2176]{1,0:T(4,128)S(1)}, u32[]{:S(2)}, u32[]{:S(2)}) collective-permute-start(f32[4,2176]{1,0:T(4,128)S(1)} %shard_map.256.refs_0_), channel_id=1, source_target_pairs={{0,4},{2,6},{4,0},{6,2},{1,5},{3,7},{5,1},{7,3},{8,12},{10,14},{12... | collective-permute-start | bytes 104456 | tf_op jit(solution)/shard_map/mixed_2/ppermute | solution.py:393
  56.7 2.5 %collective-permute-done.12.refs_2_ = f32[4,2176]{1,0:T(4,128)S(1)} collective-permute-done((f32[4,2176]{1,0:T(4,128)S(1)}, f32[4,2176]{1,0:T(4,128)S(1)}, u32[]{:S(2)}, u32[]{:S(2)}) %collective-permute-start.12) | collective-permute-done | bytes 34848 | tf_op jit(solution)/shard_map/mixed_2/ppermute | solution.py:393
  59.2 3.1 %collective-permute-done.13.refs_3_ = f32[4,2176]{1,0:T(4,128)S(1)} collective-permute-done((f32[4,2176]{1,0:T(4,128)S(1)}, f32[4,2176]{1,0:T(4,128)S(1)}, u32[]{:S(2)}, u32[]{:S(2)}) %collective-permute-start.13) | collective-permute-done | bytes 34848 | tf_op jit(solution)/shard_map/mixed_3/ppermute | solution.py:393
  62.3 1.8 %copy-done.1 = bf16[2048,704]{0,1:T(8,128)(2,1)S(1)} copy-done((bf16[2048,704]{0,1:T(8,128)(2,1)S(1)}, bf16[2048,704]{0,1:T(8,128)(2,1)}, u32[]{:S(2)}) %copy-start.1) | copy-done | bytes 2883608
  64.2 1.8 %copy-done.2 = bf16[704,2048]{1,0:T(8,128)(2,1)S(1)} copy-done((bf16[704,2048]{1,0:T(8,128)(2,1)S(1)}, bf16[704,2048]{1,0:T(8,128)(2,1)}, u32[]{:S(2)}) %copy-start.2) | copy-done | bytes 2883608
  66.7 2.0 %shard_map.257 = (f32[4,256]{1,0:T(4,128)S(1)}, f32[4,1024]{1,0:T(4,128)S(1)}, f32[4,1024]{1,0:T(4,128)S(1)}) custom-call(f32[4,2176]{1,0:T(4,128)S(1)} %shard_map.256.refs_0_, f32[4,2176]{1,0:T(4,128)S(1)} %collective-permute-done.11.refs_1_, f32[4,2176]{1,0:T(4,128)S(1)} %collective-permute-done.12.refs_2_, f32[4,2176]{1,0:T(4,128)S(1)} %collective-permute-done.13.refs_3_, ...), custom_call_target="tpu_custom_call" | custom-call | flops 34603008 | tf_op jit(solution)/shard_map/pallas_call | solution.py:198
  68.7 1.2 %collective-permute-done.14.b = f32[4,1024]{1,0:T(4,128)S(1)} collective-permute-done((f32[4,1024]{1,0:T(4,128)S(1)}, f32[4,1024]{1,0:T(4,128)S(1)}, u32[]{:S(2)}, u32[]{:S(2)}) %collective-permute-start.14) | collective-permute-done | bytes 16416 | tf_op jit(solution)/shard_map/down_tp/ppermute | solution.py:399
  70.0 0.9 %collective-permute-start.16 = (f32[4,256]{1,0:T(4,128)S(1)}, f32[4,256]{1,0:T(4,128)S(1)}, u32[]{:S(2)}, u32[]{:S(2)}) collective-permute-start(f32[4,256]{1,0:T(4,128)S(1)} %get-tuple-element.36), channel_id=1, source_target_pairs={{0,4},{2,6},{4,0},{6,2},{1,5},{3,7},{5,1},{7,3},{8,12},{10,14},{12... | collective-permute-start | bytes 12296 | tf_op jit(solution)/shard_map/down_2/ppermute | solution.py:393
  70.9 3.4 %collective-permute-start.17 = (f32[4,256]{1,0:T(4,128)S(1)}, f32[4,256]{1,0:T(4,128)S(1)}, u32[]{:S(2)}, u32[]{:S(2)}) collective-permute-start(f32[4,256]{1,0:T(4,128)S(1)} %get-tuple-element.37), channel_id=1, source_target_pairs={{0,6},{2,4},{4,2},{6,0},{1,7},{3,5},{5,3},{7,1},{8,14},{10,12},{12... | collective-permute-start | bytes 12296 | tf_op jit(solution)/shard_map/down_3/ppermute | solution.py:393
  74.6 1.8 %collective-permute-done.17.refs_3_ = f32[4,256]{1,0:T(4,128)S(1)} collective-permute-done((f32[4,256]{1,0:T(4,128)S(1)}, f32[4,256]{1,0:T(4,128)S(1)}, u32[]{:S(2)}, u32[]{:S(2)}) %collective-permute-start.17) | collective-permute-done | bytes 4128 | tf_op jit(solution)/shard_map/down_3/ppermute | solution.py:393
  (73 shorter events, 13.4 us)
Async XLA Ops:
  0.0 1.5 %collective-permute-start = (bf16[4,256]{1,0:T(4,128)(2,1)}, bf16[4,256]{1,0:T(4,128)(2,1)S(1)}, u32[]{:S(2)}, u32[]{:S(2)}) collective-permute-start(bf16[4,256]{1,0:T(4,128)(2,1)} %bitcast.47), channel_id=1, source_target_pairs={{0,1},{1,0},{2,3},{3,2},{4,5},{5,4},{6,7},{7,6},{8,9},{9,8},{10,11... | collective-permute-start | bytes 6152 | tf_op jit(solution)/shard_map/in_tp/ppermute | solution.py:399
  2.2 5.5 %collective-permute-start.1 = (bf16[4,512]{1,0:T(4,128)(2,1)S(1)}, bf16[4,512]{1,0:T(4,128)(2,1)S(1)}, u32[]{:S(2)}, u32[]{:S(2)}) collective-permute-start(bf16[4,512]{1,0:T(4,128)(2,1)S(1)} %pad_maximum_fusion.refs_0_), channel_id=1, source_target_pairs={{0,2},{2,0},{4,6},{6,4},{1,3},{3,1},{5,7},{7,5},{8,10},{10,8},{12,... | collective-permute-start | bytes 12296 | tf_op jit(solution)/shard_map/in_1/ppermute | solution.py:393
  5.1 4.5 %collective-permute-start.2 = (bf16[4,512]{1,0:T(4,128)(2,1)S(1)}, bf16[4,512]{1,0:T(4,128)(2,1)S(1)}, u32[]{:S(2)}, u32[]{:S(2)}) collective-permute-start(bf16[4,512]{1,0:T(4,128)(2,1)S(1)} %pad_maximum_fusion.refs_0_), channel_id=1, source_target_pairs={{0,4},{2,6},{4,0},{6,2},{1,5},{3,7},{5,1},{7,3},{8,12},{10,14},{12... | collective-permute-start | bytes 12296 | tf_op jit(solution)/shard_map/in_2/ppermute | solution.py:393
  7.7 5.4 %collective-permute-start.3 = (bf16[4,512]{1,0:T(4,128)(2,1)S(1)}, bf16[4,512]{1,0:T(4,128)(2,1)S(1)}, u32[]{:S(2)}, u32[]{:S(2)}) collective-permute-start(bf16[4,512]{1,0:T(4,128)(2,1)S(1)} %pad_maximum_fusion.refs_0_), channel_id=1, source_target_pairs={{0,6},{2,4},{4,2},{6,0},{1,7},{3,5},{5,3},{7,1},{8,14},{10,12},{12... | collective-permute-start | bytes 12296 | tf_op jit(solution)/shard_map/in_3/ppermute | solution.py:393
  13.1 1.6 %copy-start.3 = (bf16[2048,16,32]{0,2,1:T(8,128)(2,1)S(1)}, bf16[2048,16,32]{0,2,1:T(8,128)(2,1)}, u32[]{:S(2)}) copy-start(bf16[2048,16,32]{0,2,1:T(8,128)(2,1)} %param.29) | copy-start | bytes 6291460
  14.7 1.6 %copy-start.4 = (bf16[2048,16,32]{0,2,1:T(8,128)(2,1)S(1)}, bf16[2048,16,32]{0,2,1:T(8,128)(2,1)}, u32[]{:S(2)}) copy-start(bf16[2048,16,32]{0,2,1:T(8,128)(2,1)} %param.30) | copy-start | bytes 6291460
  16.3 1.2 %copy-start.6 = (bf16[2048,256]{1,0:T(8,128)(2,1)S(1)}, bf16[2048,256]{1,0:T(8,128)(2,1)}, u32[]{:S(2)}) copy-start(bf16[2048,256]{1,0:T(8,128)(2,1)} %refs_7_.1) | copy-start | bytes 3145732
  20.4 10.3 %copy-start.26 = (bf16[1,3,64,32]{2,3,1,0:T(8,128)(2,1)S(1)}, bf16[1,3,64,32]{2,3,1,0:T(8,128)(2,1)}, u32[]{:S(2)}) copy-start(bf16[1,3,64,32]{2,3,1,0:T(8,128)(2,1)} %param.40) | copy-start | bytes 36868
  20.4 14.9 %copy-start.9 = (bf16[1,128,64,32]{1,3,2,0:T(8,128)(2,1)S(1)}, bf16[1,128,64,32]{1,3,2,0:T(8,128)(2,1)}, u32[]{:S(2)}) copy-start(bf16[1,128,64,32]{1,3,2,0:T(8,128)(2,1)} %param.44) | copy-start | bytes 1572868
  20.4 14.9 %copy-start.12 = (f32[1,128,64]{1,2,0:T(8,128)S(1)}, f32[1,128,64]{1,2,0:T(8,128)}, u32[]{:S(2)}) copy-start(f32[1,128,64]{1,2,0:T(8,128)} %param.46) | copy-start | bytes 98308
  20.4 14.9 %copy-start.13 = (f32[4,1024]{1,0:T(4,128)S(1)}, f32[4,1024]{1,0:T(4,128)}, u32[]{:S(2)}) copy-start(f32[4,1024]{1,0:T(4,128)} %refs_9_.1) | copy-start | bytes 49156
  20.4 14.9 %copy-start.14 = (f32[4,1024]{1,0:T(4,128)S(1)}, f32[4,1024]{1,0:T(4,128)}, u32[]{:S(2)}) copy-start(f32[4,1024]{1,0:T(4,128)} %refs_10_.1) | copy-start | bytes 49156
  20.4 14.9 %copy-start.16 = (bf16[1,3,1024]{2,1,0:T(4,128)(2,1)S(1)}, bf16[1,3,1024]{2,1,0:T(4,128)(2,1)}, u32[]{:S(2)}) copy-start(bf16[1,3,1024]{2,1,0:T(4,128)(2,1)} %param.41) | copy-start | bytes 18436
  23.7 38.6 %copy-start = (bf16[2048,704]{0,1:T(8,128)(2,1)S(1)}, bf16[2048,704]{0,1:T(8,128)(2,1)}, u32[]{:S(2)}) copy-start(bf16[2048,704]{0,1:T(8,128)(2,1)} %param.51) | copy-start | bytes 8650756
  23.7 11.5 %collective-permute-start.4 = (f32[1,1536]{1,0:T(1,128)}, f32[1,1536]{1,0:T(1,128)}, u32[]{:S(2)}, u32[]{:S(2)}) collective-permute-start(f32[1,1536]{1,0:T(1,128)} %get-tuple-element.23), channel_id=1, source_target_pairs={{0,2},{2,0},{4,6},{6,4},{1,3},{3,1},{5,7},{7,5},{8,10},{10,8},{12,... | collective-permute-start | bytes 18440 | tf_op jit(solution)/shard_map/pre_1/ppermute | solution.py:393
  23.7 11.5 %collective-permute-start.5 = (f32[1,1536]{1,0:T(1,128)}, f32[1,1536]{1,0:T(1,128)}, u32[]{:S(2)}, u32[]{:S(2)}) collective-permute-start(f32[1,1536]{1,0:T(1,128)} %get-tuple-element.24), channel_id=1, source_target_pairs={{0,4},{2,6},{4,0},{6,2},{1,5},{3,7},{5,1},{7,3},{8,12},{10,14},{12... | collective-permute-start | bytes 18440 | tf_op jit(solution)/shard_map/pre_2/ppermute | solution.py:393
  24.3 11.0 %collective-permute-start.6 = (f32[1,1536]{1,0:T(1,128)}, f32[1,1536]{1,0:T(1,128)}, u32[]{:S(2)}, u32[]{:S(2)}) collective-permute-start(f32[1,1536]{1,0:T(1,128)} %get-tuple-element.25), channel_id=1, source_target_pairs={{0,6},{2,4},{4,2},{6,0},{1,7},{3,5},{5,3},{7,1},{8,14},{10,12},{12... | collective-permute-start | bytes 18440 | tf_op jit(solution)/shard_map/pre_3/ppermute | solution.py:393
  35.3 1.2 %copy-start.8 = (f32[1,64,32,128]{3,2,1,0:T(8,128)S(1)}, f32[1,64,32,128]{3,2,1,0:T(8,128)}, u32[]{:S(2)}) copy-start(f32[1,64,32,128]{3,2,1,0:T(8,128)} %param.43) | copy-start | bytes 3145732
  43.1 4.4 %collective-permute-start.7 = (f32[1,640]{1,0:T(1,128)S(1)}, f32[1,640]{1,0:T(1,128)S(1)}, u32[]{:S(2)}, u32[]{:S(2)}) collective-permute-start(f32[1,640]{1,0:T(1,128)S(1)} %get-tuple-element.28), channel_id=1, source_target_pairs={{0,2},{2,0},{4,6},{6,4},{1,3},{3,1},{5,7},{7,5},{8,10},{10,8},{12,... | collective-permute-start | bytes 7688 | tf_op jit(solution)/shard_map/gated_1/ppermute | solution.py:393
  43.1 4.6 %collective-permute-start.8 = (f32[1,640]{1,0:T(1,128)S(1)}, f32[1,640]{1,0:T(1,128)S(1)}, u32[]{:S(2)}, u32[]{:S(2)}) collective-permute-start(f32[1,640]{1,0:T(1,128)S(1)} %get-tuple-element.29), channel_id=1, source_target_pairs={{0,4},{2,6},{4,0},{6,2},{1,5},{3,7},{5,1},{7,3},{8,12},{10,14},{12... | collective-permute-start | bytes 7688 | tf_op jit(solution)/shard_map/gated_2/ppermute | solution.py:393
  43.7 5.4 %collective-permute-start.9 = (f32[1,640]{1,0:T(1,128)S(1)}, f32[1,640]{1,0:T(1,128)S(1)}, u32[]{:S(2)}, u32[]{:S(2)}) collective-permute-start(f32[1,640]{1,0:T(1,128)S(1)} %get-tuple-element.30), channel_id=1, source_target_pairs={{0,6},{2,4},{4,2},{6,0},{1,7},{3,5},{5,3},{7,1},{8,14},{10,12},{12... | collective-permute-start | bytes 7688 | tf_op jit(solution)/shard_map/gated_3/ppermute | solution.py:393
  49.1 1.6 %copy-start.5 = (bf16[16,32,2048]{2,1,0:T(8,128)(2,1)S(1)}, bf16[16,32,2048]{2,1,0:T(8,128)(2,1)}, u32[]{:S(2)}) copy-start(bf16[16,32,2048]{2,1,0:T(8,128)(2,1)} %param.49) | copy-start | bytes 6291460
  51.0 1.2 %collective-permute-start.10 = (f32[4,2176]{1,0:T(4,128)S(1)}, f32[4,2176]{1,0:T(4,128)S(1)}, u32[]{:S(2)}, u32[]{:S(2)}) collective-permute-start(f32[4,2176]{1,0:T(4,128)S(1)} %shard_map.255.a), channel_id=1, source_target_pairs={{0,1},{1,0},{2,3},{3,2},{4,5},{5,4},{6,7},{7,6},{8,9},{9,8},{10,11... | collective-permute-start | bytes 104456 | tf_op jit(solution)/shard_map/mixed_tp/ppermute | solution.py:399
  52.3 4.4 %collective-permute-start.11 = (f32[4,2176]{1,0:T(4,128)S(1)}, f32[4,2176]{1,0:T(4,128)S(1)}, u32[]{:S(2)}, u32[]{:S(2)}) collective-permute-start(f32[4,2176]{1,0:T(4,128)S(1)} %shard_map.256.refs_0_), channel_id=1, source_target_pairs={{0,2},{2,0},{4,6},{6,4},{1,3},{3,1},{5,7},{7,5},{8,10},{10,8},{12,... | collective-permute-start | bytes 104456 | tf_op jit(solution)/shard_map/mixed_1/ppermute | solution.py:393
  52.8 6.4 %collective-permute-start.12 = (f32[4,2176]{1,0:T(4,128)S(1)}, f32[4,2176]{1,0:T(4,128)S(1)}, u32[]{:S(2)}, u32[]{:S(2)}) collective-permute-start(f32[4,2176]{1,0:T(4,128)S(1)} %shard_map.256.refs_0_), channel_id=1, source_target_pairs={{0,4},{2,6},{4,0},{6,2},{1,5},{3,7},{5,1},{7,3},{8,12},{10,14},{12... | collective-permute-start | bytes 104456 | tf_op jit(solution)/shard_map/mixed_2/ppermute | solution.py:393
  56.6 5.7 %collective-permute-start.13 = (f32[4,2176]{1,0:T(4,128)S(1)}, f32[4,2176]{1,0:T(4,128)S(1)}, u32[]{:S(2)}, u32[]{:S(2)}) collective-permute-start(f32[4,2176]{1,0:T(4,128)S(1)} %shard_map.256.refs_0_), channel_id=1, source_target_pairs={{0,6},{2,4},{4,2},{6,0},{1,7},{3,5},{5,3},{7,1},{8,14},{10,12},{12... | collective-permute-start | bytes 104456 | tf_op jit(solution)/shard_map/mixed_3/ppermute | solution.py:393
  62.3 1.8 %copy-start.1 = (bf16[2048,704]{0,1:T(8,128)(2,1)S(1)}, bf16[2048,704]{0,1:T(8,128)(2,1)}, u32[]{:S(2)}) copy-start(bf16[2048,704]{0,1:T(8,128)(2,1)} %param.52) | copy-start | bytes 8650756
  64.2 1.8 %copy-start.2 = (bf16[704,2048]{1,0:T(8,128)(2,1)S(1)}, bf16[704,2048]{1,0:T(8,128)(2,1)}, u32[]{:S(2)}) copy-start(bf16[704,2048]{1,0:T(8,128)(2,1)} %refs_8_.3) | copy-start | bytes 8650756
  68.7 1.2 %collective-permute-start.14 = (f32[4,1024]{1,0:T(4,128)S(1)}, f32[4,1024]{1,0:T(4,128)S(1)}, u32[]{:S(2)}, u32[]{:S(2)}) collective-permute-start(f32[4,1024]{1,0:T(4,128)S(1)} %get-tuple-element.33), channel_id=1, source_target_pairs={{0,1},{1,0},{2,3},{3,2},{4,5},{5,4},{6,7},{7,6},{8,9},{9,8},{10,11... | collective-permute-start | bytes 49160 | tf_op jit(solution)/shard_map/down_tp/ppermute | solution.py:399
  69.9 4.4 %collective-permute-start.15 = (f32[4,256]{1,0:T(4,128)S(1)}, f32[4,256]{1,0:T(4,128)S(1)}, u32[]{:S(2)}, u32[]{:S(2)}) collective-permute-start(f32[4,256]{1,0:T(4,128)S(1)} %get-tuple-element.35), channel_id=1, source_target_pairs={{0,2},{2,0},{4,6},{6,4},{1,3},{3,1},{5,7},{7,5},{8,10},{10,8},{12,... | collective-permute-start | bytes 12296 | tf_op jit(solution)/shard_map/down_1/ppermute | solution.py:393
  70.0 4.6 %collective-permute-start.16 = (f32[4,256]{1,0:T(4,128)S(1)}, f32[4,256]{1,0:T(4,128)S(1)}, u32[]{:S(2)}, u32[]{:S(2)}) collective-permute-start(f32[4,256]{1,0:T(4,128)S(1)} %get-tuple-element.36), channel_id=1, source_target_pairs={{0,4},{2,6},{4,0},{6,2},{1,5},{3,7},{5,1},{7,3},{8,12},{10,14},{12... | collective-permute-start | bytes 12296 | tf_op jit(solution)/shard_map/down_2/ppermute | solution.py:393
  70.9 5.4 %collective-permute-start.17 = (f32[4,256]{1,0:T(4,128)S(1)}, f32[4,256]{1,0:T(4,128)S(1)}, u32[]{:S(2)}, u32[]{:S(2)}) collective-permute-start(f32[4,256]{1,0:T(4,128)S(1)} %get-tuple-element.37), channel_id=1, source_target_pairs={{0,6},{2,4},{4,2},{6,0},{1,7},{3,5},{5,3},{7,1},{8,14},{10,12},{12... | collective-permute-start | bytes 12296 | tf_op jit(solution)/shard_map/down_3/ppermute | solution.py:393
  (13 other events, 9.6 us)

commit v2 on v1

--- a/solution.py
+++ b/solution.py
@@ -6,6 +6,7 @@
 from jax.experimental import pallas as pl
 from jax.experimental.pallas import tpu as pltpu
 from jax.sharding import PartitionSpec as P
+
 
 MIXER_HEADS = 64
 HEAD_DIM = 64
@@ -190,7 +191,7 @@
     return values[0]
 
 
-def call(body, outs, args, scratch=(), scalars=(), flops=0):
+def call(body, outs, args, scratch=(), scalars=()):
     args = [
         a if i in scalars else pltpu.with_memory_space_constraint(a, pltpu.VMEM)
         for i, a in enumerate(args)
@@ -205,12 +206,22 @@
         out_specs=[pl.BlockSpec(memory_space=pltpu.VMEM) for _ in outs],
         scratch_shapes=[pltpu.VMEM(s, d) for s, d in scratch],
         compiler_params=pltpu.CompilerParams(vmem_limit_bytes=8 << 20),
-        cost_estimate=pl.CostEstimate(flops=flops, bytes_accessed=0, transcendentals=0),
+        cost_estimate=pl.CostEstimate(flops=20_000_000_000, bytes_accessed=0, transcendentals=0),
     )(*args)
 
 
 def lane(start, size):
     return pl.ds(pl.multiple_of(start, LANES), size)
+
+
+def hold(a, out):
+    out[...] = a[...]
+
+
+def stack(a, b, out):
+    part = a.shape[1]
+    out[:, :part] = a[...]
+    out[:, part:] = b[...]
 
 
 def project(n, *refs):
@@ -345,18 +356,20 @@
     out[:, width:] = rows[:, cols:]
 
 
-def add_pair(a, b, out):
-    out[...] = a[...] + b[...]
+def add_pair(a, b, out, squares):
+    width = out.shape[1]
+    out[...] = (a[:, :width] + b[:, :width]).astype(jnp.bfloat16)
+    squares[...] = a[:, width:] + b[:, width:]
 
 
 def channel_mix(n, channels, *refs):
-    pieces, (x, gain, gate_w, value_w, reduce_w) = refs[:n], refs[n : n + 5]
-    mid_out, keep, send, moved = refs[n + 5 :]
+    pieces, (squares, x, gain, gate_w, value_w, reduce_w) = refs[:n], refs[n : n + 6]
+    mid_out, keep, send, moved = refs[n + 6 :]
     kv, tp = lax.axis_index("kv"), lax.axis_index("tp")
     width = x.shape[1]
     part = mid_out.shape[1]
-    whole = tree(ref[:, :width] for ref in pieces)
-    rms_gate = lax.rsqrt(pieces[0][:, width : width + 1] / channels + epsilon)
+    whole = tree(ref[...].astype(jnp.float32) for ref in pieces)
+    rms_gate = lax.rsqrt(squares[:, :1] / channels + epsilon)
     mid = (x[...].astype(jnp.float32) + rms_gate * whole).astype(jnp.bfloat16)
     mid = mid.astype(jnp.float32)
     rms = lax.rsqrt(jnp.sum(mid * mid, axis=1, keepdims=True) / width + epsilon)
@@ -371,7 +384,7 @@
         send[:, at] = moved[:, lane((2 * i + 1 - tp) * part, part)]
 
 
-def split_pair(n, a, b, *outs):
+def split_pair(a, b, *outs):
     *outs, moved = outs
     kv = lax.axis_index("kv")
     part = outs[0].shape[1]
@@ -385,18 +398,16 @@
     out[...] = (mid[...] + tree(ref[...] for ref in pieces)).astype(jnp.bfloat16)
 
 
-def across(label, values):
+def across(values):
     n = len(values)
     got = [values[0]] + [None] * (n - 1)
-    for k in reversed(range(1, n)):
-        with jax.named_scope(f"{label}_{k}"):
-            got[k] = lax.ppermute(values[k], "kv", [(i, i ^ k) for i in range(n)])
+    for k in range(1, n):
+        got[k] = lax.ppermute(values[k], "kv", [(i, i ^ k) for i in range(n)])
     return got
 
 
-def beside(label, value):
-    with jax.named_scope(label):
-        return lax.ppermute(value, "tp", [(0, 1), (1, 0)])
+def beside(value):
+    return lax.ppermute(value, "tp", [(0, 1), (1, 0)])
 
 
 def layer(*args):
@@ -422,9 +433,9 @@
     ):
         return general(*args)
     f32, bf16 = jnp.float32, jnp.bfloat16
-    x = hidden.T
-    pair = jnp.concatenate([x, beside("in_tp", x)], axis=1)
-    pieces = across("in", [pair] * n)
+    (x,) = call(hold, [((seqs, part), bf16)], [hidden.T])
+    (pair,) = call(stack, [((seqs, 2 * part), bf16)], [x, beside(x)])
+    pieces = across([pair] * n)
     whole, step_pre, *sends = call(
         functools.partial(project, n),
         [((seqs, width), bf16), ((1, heads), f32)] + [((1, 2 * cols + 2 * maps), f32)] * n,
@@ -437,9 +448,8 @@
             output_proj,
             step_proj.T,
         ],
-        flops=2 * seqs * width * (2 * cols + 2 * maps),
-    )
-    pieces = across("pre", sends)
+    )
+    pieces = across(sends)
     sends = call(
         functools.partial(mixer, n),
         [((1, cols + LANES), f32)] * n,
@@ -464,35 +474,34 @@
         ],
         scratch=[((1, channels), f32)] * 2 + [((1, n * maps), f32)] * 2 + [((1, channels), f32)],
         scalars=(0,),
-        flops=1 << 24,
-    )
-    pieces = across("gated", sends)
+    )
+    pieces = across(sends)
     (mixed,) = call(
         functools.partial(out_project, n),
         [((seqs, width + LANES), f32)],
         pieces + [mixer_out.reshape(cols, width)],
         scratch=[((seqs, cols + LANES), f32)],
-        flops=2 * seqs * width * cols,
-    )
-    (mixed,) = call(
-        add_pair, [((seqs, width + LANES), f32)], [mixed, beside("mixed_tp", mixed)]
-    )
-    pieces = across("mixed", [mixed] * n)
+    )
+    mixed, squares = call(
+        add_pair,
+        [((seqs, width), bf16), ((seqs, LANES), f32)],
+        [mixed, beside(mixed)],
+    )
+    pieces = across([mixed] * n)
     mid, keep, send = call(
         functools.partial(channel_mix, n, 2 * channels),
         [((seqs, part), f32)] + [((seqs, width // 2), f32)] * 2,
         pieces
-        + [whole, channel_gain.reshape(1, width), expand_gate.T, expand_value.T, reduce_proj],
+        + [squares, whole, channel_gain.reshape(1, width), expand_gate.T, expand_value.T, reduce_proj],
         scratch=[((seqs, width), f32)],
-        flops=6 * seqs * width * reduce_proj.shape[0],
     )
     sends = call(
-        functools.partial(split_pair, n),
+        split_pair,
         [((seqs, part), f32)] * n,
-        [keep, beside("down_tp", send)],
+        [keep, beside(send)],
         scratch=[((seqs, width // 2), f32)],
     )
-    pieces = across("down", sends)
+    pieces = across(sends)
     (out,) = call(functools.partial(finish, n), [((seqs, part), bf16)], pieces + [mid])
     return out.T
 

time: 77.9 us -> 53.3 us (0.68); the launches traced: 76.9 us -> 53.1 us
  local copies, waits for them, and re-layouts: 27.6 us -> 2 us
  waiting for transfers between devices: 18.1 us -> 21.4 us
  Pallas kernels: 6.16 us -> 4.86 us
    unnamed x58 -> x56, local copies, waits for them, and re-layouts: 24.8 us -> 1.69 us
    ppermute x15, waiting for transfers between devices: 14.7 us -> 18.2 us  [across(): got[k] = lax.ppermute(values[k], 'kv', [(i, i ^ k) for i in range(n)])]
    pallas_call x7 -> x9, Pallas kernels: 6.16 us -> 4.86 us  [call(): pl.pallas_call(body, out_shape=[pltpu.VMEM(s, d) for s, d in outs], in_sp...]
    reshape x1, local copies, waits for them, and re-layouts: 1.02 us -> 0.12 us  [layer(): taps_inner.reshape(-1, channels)]
    reshape x1, local copies, waits for them, and re-layouts: 0.91 us -> 0.11 us  [layer(): recent_inner.reshape(-1, channels)]
  transfers between devices with their start and end apart: 18 -> 18, of which waited for: 11 -> 12; matrix products, arithmetic and copies ran while one was open for 8% -> 1% of each run, Pallas kernels for 0% -> 0%
where the time goes in v2:
time: 53.3 us; the launch traced here: 53.1 us
  starting transfers between devices  23.8 us (45%)
  waiting for transfers between devices  21.4 us (40%)
  Pallas kernels  4.86 us (9%)
  local copies, waits for them, and re-layouts  2 us (4%)
  between operations  1.02 us (2%)
    ppermute x15, starting transfers between devices, across(): got[k] = lax.ppermute(values[k], 'kv', [(i, i ^ k) for i in range(n)])  23.2 us
    ppermute x15, waiting for transfers between devices, across(): got[k] = lax.ppermute(values[k], 'kv', [(i, i ^ k) for i in range(n)])  18.2 us
    pallas_call x9, Pallas kernels, call(): pl.pallas_call(body, out_shape=[pltpu.VMEM(s, d) for s, d in outs], in_sp...  4.86 us
    ppermute x3, waiting for transfers between devices, beside(): return lax.ppermute(value, 'tp', [(0, 1), (1, 0)])  3.21 us
    unnamed x56, local copies, waits for them, and re-layouts  1.69 us
  transfers between devices with their start and end apart: 18, of which 12 were waited for; matrix products, arithmetic and copies ran while one was open for 1% of the time, Pallas kernels for 0%

profile of v2, /device:TPU:0, one launch (start us, length us, event | category | flops | bytes accessed | tf_op | source)
XLA Modules:
  0.0 53.1 jit_solution(5768854540331362672)
XLA Ops:
  0.0 0.7 %copy-done.19 = bf16[256,4]{0,1:T(4,128)(2,1)S(1)} copy-done((bf16[256,4]{0,1:T(4,128)(2,1)S(1)}, bf16[256,4]{0,1:T(4,128)(2,1)}, u32[]{:S(2)}) %copy-start.19) | copy-done | bytes 2072
  0.7 0.6 %collective-permute-start = (bf16[4,256]{1,0:T(4,128)(2,1)S(1)}, bf16[4,256]{1,0:T(4,128)(2,1)S(1)}, u32[]{:S(2)}, u32[]{:S(2)}) collective-permute-start(bf16[4,256]{1,0:T(4,128)(2,1)S(1)} %shard_map.253.a), channel_id=1, source_target_pairs={{0,1},{1,0},{2,3},{3,2},{4,5},{5,4},{6,7},{7,6},{8,9},{9,8},{10,11... | collective-permute-start | bytes 6152 | tf_op jit(solution)/shard_map/ppermute | solution.py:410
  1.3 0.8 %collective-permute-done.b = bf16[4,256]{1,0:T(4,128)(2,1)S(1)} collective-permute-done((bf16[4,256]{1,0:T(4,128)(2,1)S(1)}, bf16[4,256]{1,0:T(4,128)(2,1)S(1)}, u32[]{:S(2)}, u32[]{:S(2)}) %collective-permute-start) | collective-permute-done | bytes 2080 | tf_op jit(solution)/shard_map/ppermute | solution.py:410
  2.1 2.9 %collective-permute-start.1 = (bf16[4,512]{1,0:T(4,128)(2,1)S(1)}, bf16[4,512]{1,0:T(4,128)(2,1)S(1)}, u32[]{:S(2)}, u32[]{:S(2)}) collective-permute-start(bf16[4,512]{1,0:T(4,128)(2,1)S(1)} %shard_map.254.refs_0_), channel_id=1, source_target_pairs={{0,2},{2,0},{4,6},{6,4},{1,3},{3,1},{5,7},{7,5},{8,10},{10,8},{12,... | collective-permute-start | bytes 12296 | tf_op jit(solution)/shard_map/ppermute | solution.py:405
  5.0 2.6 %collective-permute-start.2 = (bf16[4,512]{1,0:T(4,128)(2,1)S(1)}, bf16[4,512]{1,0:T(4,128)(2,1)S(1)}, u32[]{:S(2)}, u32[]{:S(2)}) collective-permute-start(bf16[4,512]{1,0:T(4,128)(2,1)S(1)} %shard_map.254.refs_0_), channel_id=1, source_target_pairs={{0,4},{2,6},{4,0},{6,2},{1,5},{3,7},{5,1},{7,3},{8,12},{10,14},{12... | collective-permute-start | bytes 12296 | tf_op jit(solution)/shard_map/ppermute | solution.py:405
  7.6 1.9 %collective-permute-done.2.refs_2_ = bf16[4,512]{1,0:T(4,128)(2,1)S(1)} collective-permute-done((bf16[4,512]{1,0:T(4,128)(2,1)S(1)}, bf16[4,512]{1,0:T(4,128)(2,1)S(1)}, u32[]{:S(2)}, u32[]{:S(2)}) %collective-permute-start.2) | collective-permute-done | bytes 4128 | tf_op jit(solution)/shard_map/ppermute | solution.py:405
  9.5 3.5 %collective-permute-done.3.refs_3_ = bf16[4,512]{1,0:T(4,128)(2,1)S(1)} collective-permute-done((bf16[4,512]{1,0:T(4,128)(2,1)S(1)}, bf16[4,512]{1,0:T(4,128)(2,1)S(1)}, u32[]{:S(2)}, u32[]{:S(2)}) %collective-permute-start.3) | collective-permute-done | bytes 4128 | tf_op jit(solution)/shard_map/ppermute | solution.py:405
  13.2 1.6 %shard_map.255 = (bf16[4,2048]{1,0:T(4,128)(2,1)S(1)}, f32[1,64]{1,0:T(1,128)S(1)}, f32[1,1536]{1,0:T(1,128)S(1)}, f32[1,1536]{1,0:T(1,128)S(1)}, f32[1,1536]{1,0:T(1,128)S(1)}, /*index=5*/f32[1,1536]{1,0:T(1,128)S(1)}) custom-call(bf16[4,512]{1,0:T(4,128)(2,1)S(1)} %shard_map.254.refs_0_, bf16[4,512]{1,0:T(4,128)(2,1)S(1)} %collective-permute-done.1.refs_1_, ...), custom_call_target="tpu_custom_call" | custom-call | flops 20000000000 | tf_op jit(solution)/shard_map/pallas_call | solution.py:199
  14.9 0.6 %collective-permute-start.5 = (f32[1,1536]{1,0:T(1,128)S(1)}, f32[1,1536]{1,0:T(1,128)S(1)}, u32[]{:S(2)}, u32[]{:S(2)}) collective-permute-start(f32[1,1536]{1,0:T(1,128)S(1)} %get-tuple-element.26), channel_id=1, source_target_pairs={{0,4},{2,6},{4,0},{6,2},{1,5},{3,7},{5,1},{7,3},{8,12},{10,14},{12... | collective-permute-start | bytes 18440 | tf_op jit(solution)/shard_map/ppermute | solution.py:405
  15.5 3.8 %collective-permute-start.6 = (f32[1,1536]{1,0:T(1,128)S(1)}, f32[1,1536]{1,0:T(1,128)S(1)}, u32[]{:S(2)}, u32[]{:S(2)}) collective-permute-start(f32[1,1536]{1,0:T(1,128)S(1)} %get-tuple-element.27), channel_id=1, source_target_pairs={{0,6},{2,4},{4,2},{6,0},{1,7},{3,5},{5,3},{7,1},{8,14},{10,12},{12... | collective-permute-start | bytes 18440 | tf_op jit(solution)/shard_map/ppermute | solution.py:405
  19.3 0.1 reshape.45.refs_8_
  19.6 0.1 reshape.46.refs_11_
  20.5 0.4 collective-permute-done.6.refs_3_
  21.0 0.8 %shard_map.256 = (f32[1,640]{1,0:T(1,128)S(1)}, f32[1,640]{1,0:T(1,128)S(1)}, f32[1,640]{1,0:T(1,128)S(1)}, f32[1,640]{1,0:T(1,128)S(1)}) custom-call(s32[1]{0:T(128)S(6)} %copy.35.length, f32[1,1536]{1,0:T(1,128)S(1)} %get-tuple-element.24.refs_0_, f32[1,1536]{1,0:T(1,128)S(1)} %collective-permute-done.4.refs_1_, ...), custom_call_target="tpu_custom_call" | custom-call | flops 20000000000 | tf_op jit(solution)/shard_map/pallas_call | solution.py:199
  21.9 0.5 collective-permute-start.7
  22.4 3.8 %collective-permute-start.8 = (f32[1,640]{1,0:T(1,128)S(1)}, f32[1,640]{1,0:T(1,128)S(1)}, u32[]{:S(2)}, u32[]{:S(2)}) collective-permute-start(f32[1,640]{1,0:T(1,128)S(1)} %get-tuple-element.31), channel_id=1, source_target_pairs={{0,4},{2,6},{4,0},{6,2},{1,5},{3,7},{5,1},{7,3},{8,12},{10,14},{12... | collective-permute-start | bytes 7688 | tf_op jit(solution)/shard_map/ppermute | solution.py:405
  26.2 1.5 %collective-permute-done.8.refs_2_ = f32[1,640]{1,0:T(1,128)S(1)} collective-permute-done((f32[1,640]{1,0:T(1,128)S(1)}, f32[1,640]{1,0:T(1,128)S(1)}, u32[]{:S(2)}, u32[]{:S(2)}) %collective-permute-start.8) | collective-permute-done | bytes 2592 | tf_op jit(solution)/shard_map/ppermute | solution.py:405
  27.7 3.8 %collective-permute-done.9.refs_3_ = f32[1,640]{1,0:T(1,128)S(1)} collective-permute-done((f32[1,640]{1,0:T(1,128)S(1)}, f32[1,640]{1,0:T(1,128)S(1)}, u32[]{:S(2)}, u32[]{:S(2)}) %collective-permute-start.9) | collective-permute-done | bytes 2592 | tf_op jit(solution)/shard_map/ppermute | solution.py:405
  31.6 0.4 shard_map.257.a
  32.1 1.2 %collective-permute-done.10.b = f32[4,2176]{1,0:T(4,128)S(1)} collective-permute-done((f32[4,2176]{1,0:T(4,128)S(1)}, f32[4,2176]{1,0:T(4,128)S(1)}, u32[]{:S(2)}, u32[]{:S(2)}) %collective-permute-start.10) | collective-permute-done | bytes 34848 | tf_op jit(solution)/shard_map/ppermute | solution.py:410
  33.3 0.6 %collective-permute-start.12 = (bf16[4,2048]{1,0:T(4,128)(2,1)S(1)}, bf16[4,2048]{1,0:T(4,128)(2,1)S(1)}, u32[]{:S(2)}, u32[]{:S(2)}) collective-permute-start(bf16[4,2048]{1,0:T(4,128)(2,1)S(1)} %get-tuple-element.33.refs_0_), channel_id=1, source_target_pairs={{0,4},{2,6},{4,0},{6,2},{1,5},{3,7},{5,1},{7,3},{8,12},{10,14},{12... | collective-permute-start | bytes 49160 | tf_op jit(solution)/shard_map/ppermute | solution.py:405
  34.0 3.8 %collective-permute-start.13 = (bf16[4,2048]{1,0:T(4,128)(2,1)S(1)}, bf16[4,2048]{1,0:T(4,128)(2,1)S(1)}, u32[]{:S(2)}, u32[]{:S(2)}) collective-permute-start(bf16[4,2048]{1,0:T(4,128)(2,1)S(1)} %get-tuple-element.33.refs_0_), channel_id=1, source_target_pairs={{0,6},{2,4},{4,2},{6,0},{1,7},{3,5},{5,3},{7,1},{8,14},{10,12},{12... | collective-permute-start | bytes 49160 | tf_op jit(solution)/shard_map/ppermute | solution.py:405
  37.7 0.3 collective-permute-done.12.refs_2_
  38.0 1.6 %collective-permute-done.13.refs_3_ = bf16[4,2048]{1,0:T(4,128)(2,1)S(1)} collective-permute-done((bf16[4,2048]{1,0:T(4,128)(2,1)S(1)}, bf16[4,2048]{1,0:T(4,128)(2,1)S(1)}, u32[]{:S(2)}, u32[]{:S(2)}) %collective-permute-start.13) | collective-permute-done | bytes 16416 | tf_op jit(solution)/shard_map/ppermute | solution.py:405
  39.6 2.0 %shard_map.259 = (f32[4,256]{1,0:T(4,128)S(1)}, f32[4,1024]{1,0:T(4,128)S(1)}, f32[4,1024]{1,0:T(4,128)S(1)}) custom-call(bf16[4,2048]{1,0:T(4,128)(2,1)S(1)} %get-tuple-element.33.refs_0_, bf16[4,2048]{1,0:T(4,128)(2,1)S(1)} %collective-permute-done.11.refs_1_, bf16[4,2048]{1,0:T(4,128)(2,1)S(1)} %collective-permute-done.12.refs_2_, ...), custom_call_target="tpu_custom_call" | custom-call | flops 20000000000 | tf_op jit(solution)/shard_map/pallas_call | solution.py:199
  41.7 1.2 %collective-permute-done.14.b = f32[4,1024]{1,0:T(4,128)S(1)} collective-permute-done((f32[4,1024]{1,0:T(4,128)S(1)}, f32[4,1024]{1,0:T(4,128)S(1)}, u32[]{:S(2)}, u32[]{:S(2)}) %collective-permute-start.14) | collective-permute-done | bytes 16416 | tf_op jit(solution)/shard_map/ppermute | solution.py:410
  42.9 0.5 collective-permute-start.15
  43.3 3.8 %collective-permute-start.16 = (f32[4,256]{1,0:T(4,128)S(1)}, f32[4,256]{1,0:T(4,128)S(1)}, u32[]{:S(2)}, u32[]{:S(2)}) collective-permute-start(f32[4,256]{1,0:T(4,128)S(1)} %get-tuple-element.40), channel_id=1, source_target_pairs={{0,4},{2,6},{4,0},{6,2},{1,5},{3,7},{5,1},{7,3},{8,12},{10,14},{12... | collective-permute-start | bytes 12296 | tf_op jit(solution)/shard_map/ppermute | solution.py:405
  47.2 0.2 collective-permute-start.17
  47.3 1.4 %collective-permute-done.16.refs_2_ = f32[4,256]{1,0:T(4,128)S(1)} collective-permute-done((f32[4,256]{1,0:T(4,128)S(1)}, f32[4,256]{1,0:T(4,128)S(1)}, u32[]{:S(2)}, u32[]{:S(2)}) %collective-permute-start.16) | collective-permute-done | bytes 4128 | tf_op jit(solution)/shard_map/ppermute | solution.py:405
  48.7 3.8 %collective-permute-done.17.refs_3_ = f32[4,256]{1,0:T(4,128)S(1)} collective-permute-done((f32[4,256]{1,0:T(4,128)S(1)}, f32[4,256]{1,0:T(4,128)S(1)}, u32[]{:S(2)}, u32[]{:S(2)}) %collective-permute-start.17) | collective-permute-done | bytes 4128 | tf_op jit(solution)/shard_map/ppermute | solution.py:405
  52.6 0.6 %copy.34 = bf16[256,4]{0,1:T(4,128)(2,1)} copy(bf16[256,4]{0,1:T(4,128)(2,1)S(1)} %bitcast.29) | data formatting | bytes 4096
  (72 shorter events, 0.8 us)
Async XLA Ops:
  0.7 12.3 %copy-start.3 = (bf16[2048,16,32]{0,2,1:T(8,128)(2,1)S(1)}, bf16[2048,16,32]{0,2,1:T(8,128)(2,1)}, u32[]{:S(2)}) copy-start(bf16[2048,16,32]{0,2,1:T(8,128)(2,1)} %param.29) | copy-start | bytes 6291460
  0.7 12.3 %copy-start.4 = (bf16[2048,16,32]{0,2,1:T(8,128)(2,1)S(1)}, bf16[2048,16,32]{0,2,1:T(8,128)(2,1)}, u32[]{:S(2)}) copy-start(bf16[2048,16,32]{0,2,1:T(8,128)(2,1)} %param.30) | copy-start | bytes 6291460
  0.7 12.3 %copy-start.6 = (bf16[2048,256]{1,0:T(8,128)(2,1)S(1)}, bf16[2048,256]{1,0:T(8,128)(2,1)}, u32[]{:S(2)}) copy-start(bf16[2048,256]{1,0:T(8,128)(2,1)} %refs_7_.1) | copy-start | bytes 3145732
  0.7 12.3 %copy-start.7 = (bf16[2048,256]{1,0:T(8,128)(2,1)S(1)}, bf16[2048,256]{1,0:T(8,128)(2,1)}, u32[]{:S(2)}) copy-start(bf16[2048,256]{1,0:T(8,128)(2,1)} %refs_8_.1) | copy-start | bytes 3145732
  0.7 12.3 %copy-start.10 = (bf16[2048,64]{0,1:T(8,128)(2,1)S(1)}, bf16[2048,64]{0,1:T(8,128)(2,1)}, u32[]{:S(2)}) copy-start(bf16[2048,64]{0,1:T(8,128)(2,1)} %param.33) | copy-start | bytes 786436
  0.7 12.3 %copy-start.15 = (f32[2048]{0:T(1024)S(1)}, f32[2048]{0:T(1024)}, u32[]{:S(2)}) copy-start(f32[2048]{0:T(1024)} %param.28) | copy-start | bytes 24580
  0.7 1.4 %collective-permute-start = (bf16[4,256]{1,0:T(4,128)(2,1)S(1)}, bf16[4,256]{1,0:T(4,128)(2,1)S(1)}, u32[]{:S(2)}, u32[]{:S(2)}) collective-permute-start(bf16[4,256]{1,0:T(4,128)(2,1)S(1)} %shard_map.253.a), channel_id=1, source_target_pairs={{0,1},{1,0},{2,3},{3,2},{4,5},{5,4},{6,7},{7,6},{8,9},{9,8},{10,11... | collective-permute-start | bytes 6152 | tf_op jit(solution)/shard_map/ppermute | solution.py:410
  2.1 5.5 %collective-permute-start.1 = (bf16[4,512]{1,0:T(4,128)(2,1)S(1)}, bf16[4,512]{1,0:T(4,128)(2,1)S(1)}, u32[]{:S(2)}, u32[]{:S(2)}) collective-permute-start(bf16[4,512]{1,0:T(4,128)(2,1)S(1)} %shard_map.254.refs_0_), channel_id=1, source_target_pairs={{0,2},{2,0},{4,6},{6,4},{1,3},{3,1},{5,7},{7,5},{8,10},{10,8},{12,... | collective-permute-start | bytes 12296 | tf_op jit(solution)/shard_map/ppermute | solution.py:405
  5.0 4.5 %collective-permute-start.2 = (bf16[4,512]{1,0:T(4,128)(2,1)S(1)}, bf16[4,512]{1,0:T(4,128)(2,1)S(1)}, u32[]{:S(2)}, u32[]{:S(2)}) collective-permute-start(bf16[4,512]{1,0:T(4,128)(2,1)S(1)} %shard_map.254.refs_0_), channel_id=1, source_target_pairs={{0,4},{2,6},{4,0},{6,2},{1,5},{3,7},{5,1},{7,3},{8,12},{10,14},{12... | collective-permute-start | bytes 12296 | tf_op jit(solution)/shard_map/ppermute | solution.py:405
  7.6 5.4 %collective-permute-start.3 = (bf16[4,512]{1,0:T(4,128)(2,1)S(1)}, bf16[4,512]{1,0:T(4,128)(2,1)S(1)}, u32[]{:S(2)}, u32[]{:S(2)}) collective-permute-start(bf16[4,512]{1,0:T(4,128)(2,1)S(1)} %shard_map.254.refs_0_), channel_id=1, source_target_pairs={{0,6},{2,4},{4,2},{6,0},{1,7},{3,5},{5,3},{7,1},{8,14},{10,12},{12... | collective-permute-start | bytes 12296 | tf_op jit(solution)/shard_map/ppermute | solution.py:405
  13.1 7.8 %copy-start.8 = (f32[1,64,32,128]{3,2,1,0:T(8,128)S(1)}, f32[1,64,32,128]{3,2,1,0:T(8,128)}, u32[]{:S(2)}) copy-start(f32[1,64,32,128]{3,2,1,0:T(8,128)} %param.43) | copy-start | bytes 3145732
  13.1 7.8 %copy-start.9 = (bf16[1,128,64,32]{1,3,2,0:T(8,128)(2,1)S(1)}, bf16[1,128,64,32]{1,3,2,0:T(8,128)(2,1)}, u32[]{:S(2)}) copy-start(bf16[1,128,64,32]{1,3,2,0:T(8,128)(2,1)} %param.44) | copy-start | bytes 1572868
  13.1 7.8 %copy-start.11 = (bf16[1,128,1024]{2,1,0:T(8,128)(2,1)S(1)}, bf16[1,128,1024]{2,1,0:T(8,128)(2,1)}, u32[]{:S(2)}) copy-start(bf16[1,128,1024]{2,1,0:T(8,128)(2,1)} %param.45) | copy-start | bytes 786436
  13.1 7.8 %copy-start.12 = (f32[1,128,64]{1,2,0:T(8,128)S(1)}, f32[1,128,64]{1,2,0:T(8,128)}, u32[]{:S(2)}) copy-start(f32[1,128,64]{1,2,0:T(8,128)} %param.46) | copy-start | bytes 98308
  13.1 7.8 %copy-start.13 = (f32[4,1024]{1,0:T(4,128)S(1)}, f32[4,1024]{1,0:T(4,128)}, u32[]{:S(2)}) copy-start(f32[4,1024]{1,0:T(4,128)} %refs_9_.2) | copy-start | bytes 49156
  13.1 7.8 %copy-start.14 = (f32[4,1024]{1,0:T(4,128)S(1)}, f32[4,1024]{1,0:T(4,128)}, u32[]{:S(2)}) copy-start(f32[4,1024]{1,0:T(4,128)} %refs_10_.1) | copy-start | bytes 49156
  13.2 7.8 %copy-start.16 = (bf16[1,3,1024]{2,1,0:T(4,128)(2,1)S(1)}, bf16[1,3,1024]{2,1,0:T(4,128)(2,1)}, u32[]{:S(2)}) copy-start(bf16[1,3,1024]{2,1,0:T(4,128)(2,1)} %param.41) | copy-start | bytes 18436
  14.8 5.7 %collective-permute-start.4 = (f32[1,1536]{1,0:T(1,128)S(1)}, f32[1,1536]{1,0:T(1,128)S(1)}, u32[]{:S(2)}, u32[]{:S(2)}) collective-permute-start(f32[1,1536]{1,0:T(1,128)S(1)} %get-tuple-element.25), channel_id=1, source_target_pairs={{0,2},{2,0},{4,6},{6,4},{1,3},{3,1},{5,7},{7,5},{8,10},{10,8},{12,... | collective-permute-start | bytes 18440 | tf_op jit(solution)/shard_map/ppermute | solution.py:405
  14.9 5.7 %collective-permute-start.5 = (f32[1,1536]{1,0:T(1,128)S(1)}, f32[1,1536]{1,0:T(1,128)S(1)}, u32[]{:S(2)}, u32[]{:S(2)}) collective-permute-start(f32[1,1536]{1,0:T(1,128)S(1)} %get-tuple-element.26), channel_id=1, source_target_pairs={{0,4},{2,6},{4,0},{6,2},{1,5},{3,7},{5,1},{7,3},{8,12},{10,14},{12... | collective-permute-start | bytes 18440 | tf_op jit(solution)/shard_map/ppermute | solution.py:405
  15.5 5.4 %collective-permute-start.6 = (f32[1,1536]{1,0:T(1,128)S(1)}, f32[1,1536]{1,0:T(1,128)S(1)}, u32[]{:S(2)}, u32[]{:S(2)}) collective-permute-start(f32[1,1536]{1,0:T(1,128)S(1)} %get-tuple-element.27), channel_id=1, source_target_pairs={{0,6},{2,4},{4,2},{6,0},{1,7},{3,5},{5,3},{7,1},{8,14},{10,12},{12... | collective-permute-start | bytes 18440 | tf_op jit(solution)/shard_map/ppermute | solution.py:405
  21.0 10.6 %copy-start.5 = (bf16[16,32,2048]{2,1,0:T(8,128)(2,1)S(1)}, bf16[16,32,2048]{2,1,0:T(8,128)(2,1)}, u32[]{:S(2)}) copy-start(bf16[16,32,2048]{2,1,0:T(8,128)(2,1)} %param.49) | copy-start | bytes 6291460
  21.9 4.4 %collective-permute-start.7 = (f32[1,640]{1,0:T(1,128)S(1)}, f32[1,640]{1,0:T(1,128)S(1)}, u32[]{:S(2)}, u32[]{:S(2)}) collective-permute-start(f32[1,640]{1,0:T(1,128)S(1)} %get-tuple-element.30), channel_id=1, source_target_pairs={{0,2},{2,0},{4,6},{6,4},{1,3},{3,1},{5,7},{7,5},{8,10},{10,8},{12,... | collective-permute-start | bytes 7688 | tf_op jit(solution)/shard_map/ppermute | solution.py:405
  22.4 5.4 %collective-permute-start.8 = (f32[1,640]{1,0:T(1,128)S(1)}, f32[1,640]{1,0:T(1,128)S(1)}, u32[]{:S(2)}, u32[]{:S(2)}) collective-permute-start(f32[1,640]{1,0:T(1,128)S(1)} %get-tuple-element.31), channel_id=1, source_target_pairs={{0,4},{2,6},{4,0},{6,2},{1,5},{3,7},{5,1},{7,3},{8,12},{10,14},{12... | collective-permute-start | bytes 7688 | tf_op jit(solution)/shard_map/ppermute | solution.py:405
  26.2 5.4 %collective-permute-start.9 = (f32[1,640]{1,0:T(1,128)S(1)}, f32[1,640]{1,0:T(1,128)S(1)}, u32[]{:S(2)}, u32[]{:S(2)}) collective-permute-start(f32[1,640]{1,0:T(1,128)S(1)} %get-tuple-element.32), channel_id=1, source_target_pairs={{0,6},{2,4},{4,2},{6,0},{1,7},{3,5},{5,3},{7,1},{8,14},{10,12},{12... | collective-permute-start | bytes 7688 | tf_op jit(solution)/shard_map/ppermute | solution.py:405
  32.0 1.3 %collective-permute-start.10 = (f32[4,2176]{1,0:T(4,128)S(1)}, f32[4,2176]{1,0:T(4,128)S(1)}, u32[]{:S(2)}, u32[]{:S(2)}) collective-permute-start(f32[4,2176]{1,0:T(4,128)S(1)} %shard_map.257.a), channel_id=1, source_target_pairs={{0,1},{1,0},{2,3},{3,2},{4,5},{5,4},{6,7},{7,6},{8,9},{9,8},{10,11... | collective-permute-start | bytes 104456 | tf_op jit(solution)/shard_map/ppermute | solution.py:410
  33.3 4.5 %collective-permute-start.11 = (bf16[4,2048]{1,0:T(4,128)(2,1)S(1)}, bf16[4,2048]{1,0:T(4,128)(2,1)S(1)}, u32[]{:S(2)}, u32[]{:S(2)}) collective-permute-start(bf16[4,2048]{1,0:T(4,128)(2,1)S(1)} %get-tuple-element.33.refs_0_), channel_id=1, source_target_pairs={{0,2},{2,0},{4,6},{6,4},{1,3},{3,1},{5,7},{7,5},{8,10},{10,8},{12,... | collective-permute-start | bytes 49160 | tf_op jit(solution)/shard_map/ppermute | solution.py:405
  33.3 4.7 %collective-permute-start.12 = (bf16[4,2048]{1,0:T(4,128)(2,1)S(1)}, bf16[4,2048]{1,0:T(4,128)(2,1)S(1)}, u32[]{:S(2)}, u32[]{:S(2)}) collective-permute-start(bf16[4,2048]{1,0:T(4,128)(2,1)S(1)} %get-tuple-element.33.refs_0_), channel_id=1, source_target_pairs={{0,4},{2,6},{4,0},{6,2},{1,5},{3,7},{5,1},{7,3},{8,12},{10,14},{12... | collective-permute-start | bytes 49160 | tf_op jit(solution)/shard_map/ppermute | solution.py:405
  34.0 5.6 %collective-permute-start.13 = (bf16[4,2048]{1,0:T(4,128)(2,1)S(1)}, bf16[4,2048]{1,0:T(4,128)(2,1)S(1)}, u32[]{:S(2)}, u32[]{:S(2)}) collective-permute-start(bf16[4,2048]{1,0:T(4,128)(2,1)S(1)} %get-tuple-element.33.refs_0_), channel_id=1, source_target_pairs={{0,6},{2,4},{4,2},{6,0},{1,7},{3,5},{5,3},{7,1},{8,14},{10,12},{12... | collective-permute-start | bytes 49160 | tf_op jit(solution)/shard_map/ppermute | solution.py:405
  41.7 1.2 %collective-permute-start.14 = (f32[4,1024]{1,0:T(4,128)S(1)}, f32[4,1024]{1,0:T(4,128)S(1)}, u32[]{:S(2)}, u32[]{:S(2)}) collective-permute-start(f32[4,1024]{1,0:T(4,128)S(1)} %get-tuple-element.37), channel_id=1, source_target_pairs={{0,1},{1,0},{2,3},{3,2},{4,5},{5,4},{6,7},{7,6},{8,9},{9,8},{10,11... | collective-permute-start | bytes 49160 | tf_op jit(solution)/shard_map/ppermute | solution.py:410
  42.9 4.4 %collective-permute-start.15 = (f32[4,256]{1,0:T(4,128)S(1)}, f32[4,256]{1,0:T(4,128)S(1)}, u32[]{:S(2)}, u32[]{:S(2)}) collective-permute-start(f32[4,256]{1,0:T(4,128)S(1)} %get-tuple-element.39), channel_id=1, source_target_pairs={{0,2},{2,0},{4,6},{6,4},{1,3},{3,1},{5,7},{7,5},{8,10},{10,8},{12,... | collective-permute-start | bytes 12296 | tf_op jit(solution)/shard_map/ppermute | solution.py:405
  43.3 5.4 %collective-permute-start.16 = (f32[4,256]{1,0:T(4,128)S(1)}, f32[4,256]{1,0:T(4,128)S(1)}, u32[]{:S(2)}, u32[]{:S(2)}) collective-permute-start(f32[4,256]{1,0:T(4,128)S(1)} %get-tuple-element.40), channel_id=1, source_target_pairs={{0,4},{2,6},{4,0},{6,2},{1,5},{3,7},{5,1},{7,3},{8,12},{10,14},{12... | collective-permute-start | bytes 12296 | tf_op jit(solution)/shard_map/ppermute | solution.py:405
  47.2 5.4 %collective-permute-start.17 = (f32[4,256]{1,0:T(4,128)S(1)}, f32[4,256]{1,0:T(4,128)S(1)}, u32[]{:S(2)}, u32[]{:S(2)}) collective-permute-start(f32[4,256]{1,0:T(4,128)S(1)} %get-tuple-element.41), channel_id=1, source_target_pairs={{0,6},{2,4},{4,2},{6,0},{1,7},{3,5},{5,3},{7,1},{8,14},{10,12},{12... | collective-permute-start | bytes 12296 | tf_op jit(solution)/shard_map/ppermute | solution.py:405
  (12 other events, 81.7 us)

commit v3 on v2

--- a/solution.py
+++ b/solution.py
@@ -191,14 +191,14 @@
     return values[0]
 
 
-def call(body, outs, args, scratch=(), scalars=()):
+def call(body, outs, args, scratch=(), scalars=(), space=pltpu.VMEM):
     args = [
         a if i in scalars else pltpu.with_memory_space_constraint(a, pltpu.VMEM)
         for i, a in enumerate(args)
     ]
     return pl.pallas_call(
         body,
-        out_shape=[pltpu.VMEM(s, d) for s, d in outs],
+        out_shape=[space(s, d) for s, d in outs],
         in_specs=[
             pl.BlockSpec(memory_space=pltpu.SMEM if i in scalars else pltpu.VMEM)
             for i in range(len(args))
@@ -234,8 +234,9 @@
     part = pieces[0].shape[1] // 2
     for k, ref in enumerate(pieces):
         base = (kv ^ k) * (2 * part)
-        x_out[:, lane(base + tp * part, part)] = ref[:, :part]
-        x_out[:, lane(base + (1 - tp) * part, part)] = ref[:, part:]
+        first = tp if k == 0 else 1 - tp
+        x_out[:, lane(base + first * part, part)] = ref[:, :part]
+        x_out[:, lane(base + (1 - first) * part, part)] = ref[:, part:]
     x = x_out[...].astype(jnp.float32)
     rms = lax.rsqrt(jnp.sum(x * x, axis=1, keepdims=True) / width + epsilon)
     normed = (x * mixer_gain[...]).astype(jnp.bfloat16)
@@ -378,19 +379,18 @@
     mid_out[...] = moved[:, lane((kv * 2 + tp) * part, part)]
     act = silu(rms * dot(normed, gate_w[...], NT)) * (rms * dot(normed, value_w[...], NT))
     moved[...] = dot(act.astype(jnp.bfloat16), reduce_w[...], NN)
-    for i in range(n):
-        at = slice(i * part, (i + 1) * part)
-        keep[:, at] = moved[:, lane((2 * i + tp) * part, part)]
-        send[:, at] = moved[:, lane((2 * i + 1 - tp) * part, part)]
+    for k in range(n):
+        at = slice(k * part, (k + 1) * part)
+        side = tp if k == 0 else 1 - tp
+        keep[:, at] = moved[:, lane((2 * (kv ^ k) + side) * part, part)]
+        send[:, at] = moved[:, lane((2 * (kv ^ k) + 1 - side) * part, part)]
 
 
 def split_pair(a, b, *outs):
-    *outs, moved = outs
-    kv = lax.axis_index("kv")
     part = outs[0].shape[1]
-    moved[...] = a[...] + b[...]
     for k, ref in enumerate(outs):
-        ref[...] = moved[:, lane((kv ^ k) * part, part)]
+        at = slice(k * part, (k + 1) * part)
+        ref[...] = a[:, at] + b[:, at]
 
 
 def finish(n, *refs):
@@ -398,11 +398,15 @@
     out[...] = (mid[...] + tree(ref[...] for ref in pieces)).astype(jnp.bfloat16)
 
 
-def across(values):
+def across(values, cross=False):
     n = len(values)
     got = [values[0]] + [None] * (n - 1)
     for k in range(1, n):
-        got[k] = lax.ppermute(values[k], "kv", [(i, i ^ k) for i in range(n)])
+        if cross:
+            pairs = [(i, i ^ (2 * k + 1)) for i in range(2 * n)]
+            got[k] = lax.ppermute(values[k], ("kv", "tp"), pairs)
+        else:
+            got[k] = lax.ppermute(values[k], "kv", [(i, i ^ k) for i in range(n)])
     return got
 
 
@@ -433,9 +437,11 @@
     ):
         return general(*args)
     f32, bf16 = jnp.float32, jnp.bfloat16
-    (x,) = call(hold, [((seqs, part), bf16)], [hidden.T])
-    (pair,) = call(stack, [((seqs, 2 * part), bf16)], [x, beside(x)])
-    pieces = across([pair] * n)
+    x = hidden.T
+    other = beside(x)
+    (x,) = call(hold, [((seqs, part), bf16)], [x])
+    (pair,) = call(stack, [((seqs, 2 * part), bf16)], [x, other])
+    pieces = across([pair] * n, cross=True)
     whole, step_pre, *sends = call(
         functools.partial(project, n),
         [((seqs, width), bf16), ((1, heads), f32)] + [((1, 2 * cols + 2 * maps), f32)] * n,
@@ -487,7 +493,7 @@
         [((seqs, width), bf16), ((seqs, LANES), f32)],
         [mixed, beside(mixed)],
     )
-    pieces = across([mixed] * n)
+    pieces = across([mixed] * n, cross=True)
     mid, keep, send = call(
         functools.partial(channel_mix, n, 2 * channels),
         [((seqs, part), f32)] + [((seqs, width // 2), f32)] * 2,
@@ -495,14 +501,14 @@
         + [squares, whole, channel_gain.reshape(1, width), expand_gate.T, expand_value.T, reduce_proj],
         scratch=[((seqs, width), f32)],
     )
-    sends = call(
-        split_pair,
-        [((seqs, part), f32)] * n,
-        [keep, beside(send)],
-        scratch=[((seqs, width // 2), f32)],
-    )
-    pieces = across(sends)
-    (out,) = call(functools.partial(finish, n), [((seqs, part), bf16)], pieces + [mid])
+    sends = call(split_pair, [((seqs, part), f32)] * n, [keep, beside(send)])
+    pieces = across(sends, cross=True)
+    (out,) = call(
+        functools.partial(finish, n),
+        [((seqs, part), bf16)],
+        pieces + [mid],
+        space=jax.ShapeDtypeStruct,
+    )
     return out.T
 
 

time: 53.3 us -> 50.1 us (0.940)
  waiting for transfers between devices: 21.4 us -> 19.1 us
  starting transfers between devices: 23.8 us -> 23 us
  local copies, waits for them, and re-layouts: 2 us -> 1.42 us
  Pallas kernels: 4.86 us -> 5.43 us
    ppermute x15 -> x6, starting transfers between devices: 23.2 us -> 8.84 us  [across(): got[k] = lax.ppermute(values[k], 'kv', [(i, i ^ k) for i in range(n)])]
    ppermute x0 -> x9, starting transfers between devices: none -> 13.2 us  [across(): got[k] = lax.ppermute(values[k], ('kv', 'tp'), pairs)]
    ppermute x15 -> x6, waiting for transfers between devices: 18.2 us -> 5.69 us  [across(): got[k] = lax.ppermute(values[k], 'kv', [(i, i ^ k) for i in range(n)])]
    ppermute x0 -> x9, waiting for transfers between devices: none -> 11.1 us  [across(): got[k] = lax.ppermute(values[k], ('kv', 'tp'), pairs)]
    ppermute x3, waiting for transfers between devices: 3.21 us -> 2.34 us  [beside(): return lax.ppermute(value, 'tp', [(0, 1), (1, 0)])]
    unnamed x56 -> x55, local copies, waits for them, and re-layouts: 1.69 us -> 1.11 us
    pallas_call x9, Pallas kernels: 4.86 us -> 5.43 us  [call(): pl.pallas_call(body, out_shape=[space(s, d) for s, d in outs], in_specs=[...]
where the time goes in v3:
time: 50.1 us; the launch traced here: 49.9 us
  starting transfers between devices  23 us (46%)
  waiting for transfers between devices  19.1 us (38%)
  Pallas kernels  5.43 us (11%)
  local copies, waits for them, and re-layouts  1.42 us (3%)
  between operations  1.02 us (2%)
    ppermute x9, starting transfers between devices, across(): got[k] = lax.ppermute(values[k], ('kv', 'tp'), pairs)  13.2 us
    ppermute x9, waiting for transfers between devices, across(): got[k] = lax.ppermute(values[k], ('kv', 'tp'), pairs)  11.1 us
    ppermute x6, starting transfers between devices, across(): got[k] = lax.ppermute(values[k], 'kv', [(i, i ^ k) for i in range(n)])  8.84 us
    ppermute x6, waiting for transfers between devices, across(): got[k] = lax.ppermute(values[k], 'kv', [(i, i ^ k) for i in range(n)])  5.69 us
    pallas_call x9, Pallas kernels, call(): pl.pallas_call(body, out_shape=[space(s, d) for s, d in outs], in_specs=[...  5.43 us
    ppermute x3, waiting for transfers between devices, beside(): return lax.ppermute(value, 'tp', [(0, 1), (1, 0)])  2.34 us
    unnamed x55, local copies, waits for them, and re-layouts  1.11 us
  transfers between devices with their start and end apart: 18, of which 12 were waited for; matrix products, arithmetic and copies ran while one was open for 1% of the time, Pallas kernels for 0%

profile of v3, /device:TPU:0, one launch (start us, length us, event | category | flops | bytes accessed | tf_op | source)
XLA Modules:
  0.0 49.9 jit_solution(2647185790096754686)
XLA Ops:
  0.0 0.5 collective-permute-start
  0.5 0.7 %copy-done.19 = bf16[256,4]{0,1:T(4,128)(2,1)S(1)} copy-done((bf16[256,4]{0,1:T(4,128)(2,1)S(1)}, bf16[256,4]{0,1:T(4,128)(2,1)}, u32[]{:S(2)}) %copy-start.19) | copy-done | bytes 2072
  1.2 0.3 collective-permute-done.b
  1.5 2.7 %collective-permute-start.1 = (bf16[4,512]{1,0:T(4,128)(2,1)S(1)}, bf16[4,512]{1,0:T(4,128)(2,1)S(1)}, u32[]{:S(2)}, u32[]{:S(2)}) collective-permute-start(bf16[4,512]{1,0:T(4,128)(2,1)S(1)} %shard_map.254.refs_0_), channel_id=1, source_target_pairs={{0,3},{1,2},{2,1},{3,0},{4,7},{5,6},{6,5},{7,4},{8,11},{9,10},{10,... | collective-permute-start | bytes 12296 | tf_op jit(solution)/shard_map/ppermute | solution.py:407
  4.2 2.5 %collective-permute-start.2 = (bf16[4,512]{1,0:T(4,128)(2,1)S(1)}, bf16[4,512]{1,0:T(4,128)(2,1)S(1)}, u32[]{:S(2)}, u32[]{:S(2)}) collective-permute-start(bf16[4,512]{1,0:T(4,128)(2,1)S(1)} %shard_map.254.refs_0_), channel_id=1, source_target_pairs={{0,5},{1,4},{2,7},{3,6},{4,1},{5,0},{6,3},{7,2},{8,13},{9,12},{10,... | collective-permute-start | bytes 12296 | tf_op jit(solution)/shard_map/ppermute | solution.py:407
  6.7 1.4 %collective-permute-done.2.refs_2_ = bf16[4,512]{1,0:T(4,128)(2,1)S(1)} collective-permute-done((bf16[4,512]{1,0:T(4,128)(2,1)S(1)}, bf16[4,512]{1,0:T(4,128)(2,1)S(1)}, u32[]{:S(2)}, u32[]{:S(2)}) %collective-permute-start.2) | collective-permute-done | bytes 4128 | tf_op jit(solution)/shard_map/ppermute | solution.py:407
  8.1 3.4 %collective-permute-done.3.refs_3_ = bf16[4,512]{1,0:T(4,128)(2,1)S(1)} collective-permute-done((bf16[4,512]{1,0:T(4,128)(2,1)S(1)}, bf16[4,512]{1,0:T(4,128)(2,1)S(1)}, u32[]{:S(2)}, u32[]{:S(2)}) %collective-permute-start.3) | collective-permute-done | bytes 4128 | tf_op jit(solution)/shard_map/ppermute | solution.py:407
  11.8 1.6 %shard_map.255 = (bf16[4,2048]{1,0:T(4,128)(2,1)S(1)}, f32[1,64]{1,0:T(1,128)S(1)}, f32[1,1536]{1,0:T(1,128)S(1)}, f32[1,1536]{1,0:T(1,128)S(1)}, f32[1,1536]{1,0:T(1,128)S(1)}, /*index=5*/f32[1,1536]{1,0:T(1,128)S(1)}) custom-call(bf16[4,512]{1,0:T(4,128)(2,1)S(1)} %shard_map.254.refs_0_, bf16[4,512]{1,0:T(4,128)(2,1)S(1)} %collective-permute-done.1.refs_1_, ...), custom_call_target="tpu_custom_call" | custom-call | flops 20000000000 | tf_op jit(solution)/shard_map/pallas_call | solution.py:199
  13.4 0.6 %collective-permute-start.5 = (f32[1,1536]{1,0:T(1,128)S(1)}, f32[1,1536]{1,0:T(1,128)S(1)}, u32[]{:S(2)}, u32[]{:S(2)}) collective-permute-start(f32[1,1536]{1,0:T(1,128)S(1)} %get-tuple-element.26), channel_id=1, source_target_pairs={{0,4},{2,6},{4,0},{6,2},{1,5},{3,7},{5,1},{7,3},{8,12},{10,14},{12... | collective-permute-start | bytes 18440 | tf_op jit(solution)/shard_map/ppermute | solution.py:409
  14.1 3.7 %collective-permute-start.6 = (f32[1,1536]{1,0:T(1,128)S(1)}, f32[1,1536]{1,0:T(1,128)S(1)}, u32[]{:S(2)}, u32[]{:S(2)}) collective-permute-start(f32[1,1536]{1,0:T(1,128)S(1)} %get-tuple-element.27), channel_id=1, source_target_pairs={{0,6},{2,4},{4,2},{6,0},{1,7},{3,5},{5,3},{7,1},{8,14},{10,12},{12... | collective-permute-start | bytes 18440 | tf_op jit(solution)/shard_map/ppermute | solution.py:409
  17.9 0.1 reshape.45.refs_8_
  19.1 0.4 collective-permute-done.6.refs_3_
  19.6 0.8 %shard_map.256 = (f32[1,640]{1,0:T(1,128)S(1)}, f32[1,640]{1,0:T(1,128)S(1)}, f32[1,640]{1,0:T(1,128)S(1)}, f32[1,640]{1,0:T(1,128)S(1)}) custom-call(s32[1]{0:T(128)S(6)} %copy.34.length, f32[1,1536]{1,0:T(1,128)S(1)} %get-tuple-element.24.refs_0_, f32[1,1536]{1,0:T(1,128)S(1)} %collective-permute-done.4.refs_1_, ...), custom_call_target="tpu_custom_call" | custom-call | flops 20000000000 | tf_op jit(solution)/shard_map/pallas_call | solution.py:199
  20.4 0.5 collective-permute-start.7
  20.9 3.8 %collective-permute-start.8 = (f32[1,640]{1,0:T(1,128)S(1)}, f32[1,640]{1,0:T(1,128)S(1)}, u32[]{:S(2)}, u32[]{:S(2)}) collective-permute-start(f32[1,640]{1,0:T(1,128)S(1)} %get-tuple-element.31), channel_id=1, source_target_pairs={{0,4},{2,6},{4,0},{6,2},{1,5},{3,7},{5,1},{7,3},{8,12},{10,14},{12... | collective-permute-start | bytes 7688 | tf_op jit(solution)/shard_map/ppermute | solution.py:409
  24.8 1.5 %collective-permute-done.8.refs_2_ = f32[1,640]{1,0:T(1,128)S(1)} collective-permute-done((f32[1,640]{1,0:T(1,128)S(1)}, f32[1,640]{1,0:T(1,128)S(1)}, u32[]{:S(2)}, u32[]{:S(2)}) %collective-permute-start.8) | collective-permute-done | bytes 2592 | tf_op jit(solution)/shard_map/ppermute | solution.py:409
  26.3 3.8 %collective-permute-done.9.refs_3_ = f32[1,640]{1,0:T(1,128)S(1)} collective-permute-done((f32[1,640]{1,0:T(1,128)S(1)}, f32[1,640]{1,0:T(1,128)S(1)}, u32[]{:S(2)}, u32[]{:S(2)}) %collective-permute-start.9) | collective-permute-done | bytes 2592 | tf_op jit(solution)/shard_map/ppermute | solution.py:409
  30.1 0.4 shard_map.257.a
  30.6 1.2 %collective-permute-done.10.b = f32[4,2176]{1,0:T(4,128)S(1)} collective-permute-done((f32[4,2176]{1,0:T(4,128)S(1)}, f32[4,2176]{1,0:T(4,128)S(1)}, u32[]{:S(2)}, u32[]{:S(2)}) %collective-permute-start.10) | collective-permute-done | bytes 34848 | tf_op jit(solution)/shard_map/ppermute | solution.py:414
  31.9 0.4 collective-permute-start.12
  32.3 3.5 %collective-permute-start.13 = (bf16[4,2048]{1,0:T(4,128)(2,1)S(1)}, bf16[4,2048]{1,0:T(4,128)(2,1)S(1)}, u32[]{:S(2)}, u32[]{:S(2)}) collective-permute-start(bf16[4,2048]{1,0:T(4,128)(2,1)S(1)} %get-tuple-element.33.refs_0_), channel_id=1, source_target_pairs={{0,7},{1,6},{2,5},{3,4},{4,3},{5,2},{6,1},{7,0},{8,15},{9,14},{10,... | collective-permute-start | bytes 49160 | tf_op jit(solution)/shard_map/ppermute | solution.py:407
  35.8 0.3 collective-permute-done.12.refs_2_
  36.0 1.3 %collective-permute-done.13.refs_3_ = bf16[4,2048]{1,0:T(4,128)(2,1)S(1)} collective-permute-done((bf16[4,2048]{1,0:T(4,128)(2,1)S(1)}, bf16[4,2048]{1,0:T(4,128)(2,1)S(1)}, u32[]{:S(2)}, u32[]{:S(2)}) %collective-permute-start.13) | collective-permute-done | bytes 16416 | tf_op jit(solution)/shard_map/ppermute | solution.py:407
  37.4 2.0 %shard_map.259 = (f32[4,256]{1,0:T(4,128)S(1)}, f32[4,1024]{1,0:T(4,128)S(1)}, f32[4,1024]{1,0:T(4,128)S(1)}) custom-call(bf16[4,2048]{1,0:T(4,128)(2,1)S(1)} %get-tuple-element.33.refs_0_, bf16[4,2048]{1,0:T(4,128)(2,1)S(1)} %collective-permute-done.11.refs_1_, bf16[4,2048]{1,0:T(4,128)(2,1)S(1)} %collective-permute-done.12.refs_2_, ...), custom_call_target="tpu_custom_call" | custom-call | flops 20000000000 | tf_op jit(solution)/shard_map/pallas_call | solution.py:199
  39.4 0.4 collective-permute-start.14
  39.8 0.8 %collective-permute-done.14.b = f32[4,1024]{1,0:T(4,128)S(1)} collective-permute-done((f32[4,1024]{1,0:T(4,128)S(1)}, f32[4,1024]{1,0:T(4,128)S(1)}, u32[]{:S(2)}, u32[]{:S(2)}) %collective-permute-start.14) | collective-permute-done | bytes 16416 | tf_op jit(solution)/shard_map/ppermute | solution.py:414
  40.6 0.3 collective-permute-start.15
  41.0 3.5 %collective-permute-start.16 = (f32[4,256]{1,0:T(4,128)S(1)}, f32[4,256]{1,0:T(4,128)S(1)}, u32[]{:S(2)}, u32[]{:S(2)}) collective-permute-start(f32[4,256]{1,0:T(4,128)S(1)} %get-tuple-element.40), channel_id=1, source_target_pairs={{0,5},{1,4},{2,7},{3,6},{4,1},{5,0},{6,3},{7,2},{8,13},{9,12},{10,... | collective-permute-start | bytes 12296 | tf_op jit(solution)/shard_map/ppermute | solution.py:407
  44.5 0.2 collective-permute-start.17
  44.7 1.2 %collective-permute-done.16.refs_2_ = f32[4,256]{1,0:T(4,128)S(1)} collective-permute-done((f32[4,256]{1,0:T(4,128)S(1)}, f32[4,256]{1,0:T(4,128)S(1)}, u32[]{:S(2)}, u32[]{:S(2)}) %collective-permute-start.16) | collective-permute-done | bytes 4128 | tf_op jit(solution)/shard_map/ppermute | solution.py:407
  45.8 3.5 %collective-permute-done.17.refs_3_ = f32[4,256]{1,0:T(4,128)S(1)} collective-permute-done((f32[4,256]{1,0:T(4,128)S(1)}, f32[4,256]{1,0:T(4,128)S(1)}, u32[]{:S(2)}, u32[]{:S(2)}) %collective-permute-start.17) | collective-permute-done | bytes 4128 | tf_op jit(solution)/shard_map/ppermute | solution.py:407
  49.3 0.6 %shard_map.261 = bf16[4,256]{1,0:T(4,128)(2,1)} custom-call(f32[4,256]{1,0:T(4,128)S(1)} %get-tuple-element.38.refs_0_, f32[4,256]{1,0:T(4,128)S(1)} %collective-permute-done.15.refs_1_, f32[4,256]{1,0:T(4,128)S(1)} %collective-permute-done.16.refs_2_, f32[4,256]{1,0:T(4,128)S(1)} %collective-permute-done.17.refs_3_, f32[4,256]{1,0:T(4,128)S(1)} %get-tuple-element.42.refs_4_), custom_call_target="tpu_custom_call" | custom-call | flops 20000000000 | tf_op jit(solution)/shard_map/pallas_call | solution.py:199
  (71 shorter events, 1.0 us)
Async XLA Ops:
  0.0 1.5 %collective-permute-start = (bf16[4,256]{1,0:T(4,128)(2,1)}, bf16[4,256]{1,0:T(4,128)(2,1)S(1)}, u32[]{:S(2)}, u32[]{:S(2)}) collective-permute-start(bf16[4,256]{1,0:T(4,128)(2,1)} %bitcast.43), channel_id=1, source_target_pairs={{0,1},{1,0},{2,3},{3,2},{4,5},{5,4},{6,7},{7,6},{8,9},{9,8},{10,11... | collective-permute-start | bytes 6152 | tf_op jit(solution)/shard_map/ppermute | solution.py:414
  1.2 10.4 %copy-start.3 = (bf16[2048,16,32]{0,2,1:T(8,128)(2,1)S(1)}, bf16[2048,16,32]{0,2,1:T(8,128)(2,1)}, u32[]{:S(2)}) copy-start(bf16[2048,16,32]{0,2,1:T(8,128)(2,1)} %param.29) | copy-start | bytes 6291460
  1.2 10.4 %copy-start.4 = (bf16[2048,16,32]{0,2,1:T(8,128)(2,1)S(1)}, bf16[2048,16,32]{0,2,1:T(8,128)(2,1)}, u32[]{:S(2)}) copy-start(bf16[2048,16,32]{0,2,1:T(8,128)(2,1)} %param.30) | copy-start | bytes 6291460
  1.2 10.4 %copy-start.6 = (bf16[2048,256]{1,0:T(8,128)(2,1)S(1)}, bf16[2048,256]{1,0:T(8,128)(2,1)}, u32[]{:S(2)}) copy-start(bf16[2048,256]{1,0:T(8,128)(2,1)} %refs_7_.1) | copy-start | bytes 3145732
  1.2 10.4 %copy-start.7 = (bf16[2048,256]{1,0:T(8,128)(2,1)S(1)}, bf16[2048,256]{1,0:T(8,128)(2,1)}, u32[]{:S(2)}) copy-start(bf16[2048,256]{1,0:T(8,128)(2,1)} %refs_8_.1) | copy-start | bytes 3145732
  1.2 10.4 %copy-start.10 = (bf16[2048,64]{0,1:T(8,128)(2,1)S(1)}, bf16[2048,64]{0,1:T(8,128)(2,1)}, u32[]{:S(2)}) copy-start(bf16[2048,64]{0,1:T(8,128)(2,1)} %param.33) | copy-start | bytes 786436
  1.2 10.4 %copy-start.15 = (f32[2048]{0:T(1024)S(1)}, f32[2048]{0:T(1024)}, u32[]{:S(2)}) copy-start(f32[2048]{0:T(1024)} %param.28) | copy-start | bytes 24580
  1.5 5.2 %collective-permute-start.1 = (bf16[4,512]{1,0:T(4,128)(2,1)S(1)}, bf16[4,512]{1,0:T(4,128)(2,1)S(1)}, u32[]{:S(2)}, u32[]{:S(2)}) collective-permute-start(bf16[4,512]{1,0:T(4,128)(2,1)S(1)} %shard_map.254.refs_0_), channel_id=1, source_target_pairs={{0,3},{1,2},{2,1},{3,0},{4,7},{5,6},{6,5},{7,4},{8,11},{9,10},{10,... | collective-permute-start | bytes 12296 | tf_op jit(solution)/shard_map/ppermute | solution.py:407
  4.2 3.9 %collective-permute-start.2 = (bf16[4,512]{1,0:T(4,128)(2,1)S(1)}, bf16[4,512]{1,0:T(4,128)(2,1)S(1)}, u32[]{:S(2)}, u32[]{:S(2)}) collective-permute-start(bf16[4,512]{1,0:T(4,128)(2,1)S(1)} %shard_map.254.refs_0_), channel_id=1, source_target_pairs={{0,5},{1,4},{2,7},{3,6},{4,1},{5,0},{6,3},{7,2},{8,13},{9,12},{10,... | collective-permute-start | bytes 12296 | tf_op jit(solution)/shard_map/ppermute | solution.py:407
  6.7 4.8 %collective-permute-start.3 = (bf16[4,512]{1,0:T(4,128)(2,1)S(1)}, bf16[4,512]{1,0:T(4,128)(2,1)S(1)}, u32[]{:S(2)}, u32[]{:S(2)}) collective-permute-start(bf16[4,512]{1,0:T(4,128)(2,1)S(1)} %shard_map.254.refs_0_), channel_id=1, source_target_pairs={{0,7},{1,6},{2,5},{3,4},{4,3},{5,2},{6,1},{7,0},{8,15},{9,14},{10,... | collective-permute-start | bytes 12296 | tf_op jit(solution)/shard_map/ppermute | solution.py:407
  11.6 7.9 %copy-start.8 = (f32[1,64,32,128]{3,2,1,0:T(8,128)S(1)}, f32[1,64,32,128]{3,2,1,0:T(8,128)}, u32[]{:S(2)}) copy-start(f32[1,64,32,128]{3,2,1,0:T(8,128)} %param.43) | copy-start | bytes 3145732
  11.7 7.8 %copy-start.9 = (bf16[1,128,64,32]{1,3,2,0:T(8,128)(2,1)S(1)}, bf16[1,128,64,32]{1,3,2,0:T(8,128)(2,1)}, u32[]{:S(2)}) copy-start(bf16[1,128,64,32]{1,3,2,0:T(8,128)(2,1)} %param.44) | copy-start | bytes 1572868
  11.7 7.8 %copy-start.11 = (bf16[1,128,1024]{2,1,0:T(8,128)(2,1)S(1)}, bf16[1,128,1024]{2,1,0:T(8,128)(2,1)}, u32[]{:S(2)}) copy-start(bf16[1,128,1024]{2,1,0:T(8,128)(2,1)} %param.45) | copy-start | bytes 786436
  11.7 7.8 %copy-start.12 = (f32[1,128,64]{1,2,0:T(8,128)S(1)}, f32[1,128,64]{1,2,0:T(8,128)}, u32[]{:S(2)}) copy-start(f32[1,128,64]{1,2,0:T(8,128)} %param.46) | copy-start | bytes 98308
  11.7 7.8 %copy-start.13 = (f32[4,1024]{1,0:T(4,128)S(1)}, f32[4,1024]{1,0:T(4,128)}, u32[]{:S(2)}) copy-start(f32[4,1024]{1,0:T(4,128)} %refs_9_.2) | copy-start | bytes 49156
  11.7 7.8 %copy-start.14 = (f32[4,1024]{1,0:T(4,128)S(1)}, f32[4,1024]{1,0:T(4,128)}, u32[]{:S(2)}) copy-start(f32[4,1024]{1,0:T(4,128)} %refs_10_.1) | copy-start | bytes 49156
  11.7 7.8 %copy-start.16 = (bf16[1,3,1024]{2,1,0:T(4,128)(2,1)S(1)}, bf16[1,3,1024]{2,1,0:T(4,128)(2,1)}, u32[]{:S(2)}) copy-start(bf16[1,3,1024]{2,1,0:T(4,128)(2,1)} %param.41) | copy-start | bytes 18436
  13.4 5.7 %collective-permute-start.4 = (f32[1,1536]{1,0:T(1,128)S(1)}, f32[1,1536]{1,0:T(1,128)S(1)}, u32[]{:S(2)}, u32[]{:S(2)}) collective-permute-start(f32[1,1536]{1,0:T(1,128)S(1)} %get-tuple-element.25), channel_id=1, source_target_pairs={{0,2},{2,0},{4,6},{6,4},{1,3},{3,1},{5,7},{7,5},{8,10},{10,8},{12,... | collective-permute-start | bytes 18440 | tf_op jit(solution)/shard_map/ppermute | solution.py:409
  13.4 5.7 %collective-permute-start.5 = (f32[1,1536]{1,0:T(1,128)S(1)}, f32[1,1536]{1,0:T(1,128)S(1)}, u32[]{:S(2)}, u32[]{:S(2)}) collective-permute-start(f32[1,1536]{1,0:T(1,128)S(1)} %get-tuple-element.26), channel_id=1, source_target_pairs={{0,4},{2,6},{4,0},{6,2},{1,5},{3,7},{5,1},{7,3},{8,12},{10,14},{12... | collective-permute-start | bytes 18440 | tf_op jit(solution)/shard_map/ppermute | solution.py:409
  14.1 5.4 %collective-permute-start.6 = (f32[1,1536]{1,0:T(1,128)S(1)}, f32[1,1536]{1,0:T(1,128)S(1)}, u32[]{:S(2)}, u32[]{:S(2)}) collective-permute-start(f32[1,1536]{1,0:T(1,128)S(1)} %get-tuple-element.27), channel_id=1, source_target_pairs={{0,6},{2,4},{4,2},{6,0},{1,7},{3,5},{5,3},{7,1},{8,14},{10,12},{12... | collective-permute-start | bytes 18440 | tf_op jit(solution)/shard_map/ppermute | solution.py:409
  19.6 10.5 %copy-start.5 = (bf16[16,32,2048]{2,1,0:T(8,128)(2,1)S(1)}, bf16[16,32,2048]{2,1,0:T(8,128)(2,1)}, u32[]{:S(2)}) copy-start(bf16[16,32,2048]{2,1,0:T(8,128)(2,1)} %param.49) | copy-start | bytes 6291460
  20.4 4.4 %collective-permute-start.7 = (f32[1,640]{1,0:T(1,128)S(1)}, f32[1,640]{1,0:T(1,128)S(1)}, u32[]{:S(2)}, u32[]{:S(2)}) collective-permute-start(f32[1,640]{1,0:T(1,128)S(1)} %get-tuple-element.30), channel_id=1, source_target_pairs={{0,2},{2,0},{4,6},{6,4},{1,3},{3,1},{5,7},{7,5},{8,10},{10,8},{12,... | collective-permute-start | bytes 7688 | tf_op jit(solution)/shard_map/ppermute | solution.py:409
  20.9 5.4 %collective-permute-start.8 = (f32[1,640]{1,0:T(1,128)S(1)}, f32[1,640]{1,0:T(1,128)S(1)}, u32[]{:S(2)}, u32[]{:S(2)}) collective-permute-start(f32[1,640]{1,0:T(1,128)S(1)} %get-tuple-element.31), channel_id=1, source_target_pairs={{0,4},{2,6},{4,0},{6,2},{1,5},{3,7},{5,1},{7,3},{8,12},{10,14},{12... | collective-permute-start | bytes 7688 | tf_op jit(solution)/shard_map/ppermute | solution.py:409
  24.7 5.4 %collective-permute-start.9 = (f32[1,640]{1,0:T(1,128)S(1)}, f32[1,640]{1,0:T(1,128)S(1)}, u32[]{:S(2)}, u32[]{:S(2)}) collective-permute-start(f32[1,640]{1,0:T(1,128)S(1)} %get-tuple-element.32), channel_id=1, source_target_pairs={{0,6},{2,4},{4,2},{6,0},{1,7},{3,5},{5,3},{7,1},{8,14},{10,12},{12... | collective-permute-start | bytes 7688 | tf_op jit(solution)/shard_map/ppermute | solution.py:409
  30.5 1.3 %collective-permute-start.10 = (f32[4,2176]{1,0:T(4,128)S(1)}, f32[4,2176]{1,0:T(4,128)S(1)}, u32[]{:S(2)}, u32[]{:S(2)}) collective-permute-start(f32[4,2176]{1,0:T(4,128)S(1)} %shard_map.257.a), channel_id=1, source_target_pairs={{0,1},{1,0},{2,3},{3,2},{4,5},{5,4},{6,7},{7,6},{8,9},{9,8},{10,11... | collective-permute-start | bytes 104456 | tf_op jit(solution)/shard_map/ppermute | solution.py:414
  31.8 3.9 %collective-permute-start.11 = (bf16[4,2048]{1,0:T(4,128)(2,1)S(1)}, bf16[4,2048]{1,0:T(4,128)(2,1)S(1)}, u32[]{:S(2)}, u32[]{:S(2)}) collective-permute-start(bf16[4,2048]{1,0:T(4,128)(2,1)S(1)} %get-tuple-element.33.refs_0_), channel_id=1, source_target_pairs={{0,3},{1,2},{2,1},{3,0},{4,7},{5,6},{6,5},{7,4},{8,11},{9,10},{10,... | collective-permute-start | bytes 49160 | tf_op jit(solution)/shard_map/ppermute | solution.py:407
  31.9 4.1 %collective-permute-start.12 = (bf16[4,2048]{1,0:T(4,128)(2,1)S(1)}, bf16[4,2048]{1,0:T(4,128)(2,1)S(1)}, u32[]{:S(2)}, u32[]{:S(2)}) collective-permute-start(bf16[4,2048]{1,0:T(4,128)(2,1)S(1)} %get-tuple-element.33.refs_0_), channel_id=1, source_target_pairs={{0,5},{1,4},{2,7},{3,6},{4,1},{5,0},{6,3},{7,2},{8,13},{9,12},{10,... | collective-permute-start | bytes 49160 | tf_op jit(solution)/shard_map/ppermute | solution.py:407
  32.3 5.1 %collective-permute-start.13 = (bf16[4,2048]{1,0:T(4,128)(2,1)S(1)}, bf16[4,2048]{1,0:T(4,128)(2,1)S(1)}, u32[]{:S(2)}, u32[]{:S(2)}) collective-permute-start(bf16[4,2048]{1,0:T(4,128)(2,1)S(1)} %get-tuple-element.33.refs_0_), channel_id=1, source_target_pairs={{0,7},{1,6},{2,5},{3,4},{4,3},{5,2},{6,1},{7,0},{8,15},{9,14},{10,... | collective-permute-start | bytes 49160 | tf_op jit(solution)/shard_map/ppermute | solution.py:407
  39.4 1.2 %collective-permute-start.14 = (f32[4,1024]{1,0:T(4,128)S(1)}, f32[4,1024]{1,0:T(4,128)S(1)}, u32[]{:S(2)}, u32[]{:S(2)}) collective-permute-start(f32[4,1024]{1,0:T(4,128)S(1)} %get-tuple-element.37), channel_id=1, source_target_pairs={{0,1},{1,0},{2,3},{3,2},{4,5},{5,4},{6,7},{7,6},{8,9},{9,8},{10,11... | collective-permute-start | bytes 49160 | tf_op jit(solution)/shard_map/ppermute | solution.py:414
  40.6 4.1 %collective-permute-start.15 = (f32[4,256]{1,0:T(4,128)S(1)}, f32[4,256]{1,0:T(4,128)S(1)}, u32[]{:S(2)}, u32[]{:S(2)}) collective-permute-start(f32[4,256]{1,0:T(4,128)S(1)} %get-tuple-element.39), channel_id=1, source_target_pairs={{0,3},{1,2},{2,1},{3,0},{4,7},{5,6},{6,5},{7,4},{8,11},{9,10},{10,... | collective-permute-start | bytes 12296 | tf_op jit(solution)/shard_map/ppermute | solution.py:407
  41.0 4.9 %collective-permute-start.16 = (f32[4,256]{1,0:T(4,128)S(1)}, f32[4,256]{1,0:T(4,128)S(1)}, u32[]{:S(2)}, u32[]{:S(2)}) collective-permute-start(f32[4,256]{1,0:T(4,128)S(1)} %get-tuple-element.40), channel_id=1, source_target_pairs={{0,5},{1,4},{2,7},{3,6},{4,1},{5,0},{6,3},{7,2},{8,13},{9,12},{10,... | collective-permute-start | bytes 12296 | tf_op jit(solution)/shard_map/ppermute | solution.py:407
  44.5 4.8 %collective-permute-start.17 = (f32[4,256]{1,0:T(4,128)S(1)}, f32[4,256]{1,0:T(4,128)S(1)}, u32[]{:S(2)}, u32[]{:S(2)}) collective-permute-start(f32[4,256]{1,0:T(4,128)S(1)} %get-tuple-element.41), channel_id=1, source_target_pairs={{0,7},{1,6},{2,5},{3,4},{4,3},{5,2},{6,1},{7,0},{8,15},{9,14},{10,... | collective-permute-start | bytes 12296 | tf_op jit(solution)/shard_map/ppermute | solution.py:407
  (12 other events, 78.6 us)

commit v4 on v3

--- a/solution.py
+++ b/solution.py
@@ -398,15 +398,12 @@
     out[...] = (mid[...] + tree(ref[...] for ref in pieces)).astype(jnp.bfloat16)
 
 
-def across(values, cross=False):
+def across(values, first=1):
     n = len(values)
-    got = [values[0]] + [None] * (n - 1)
-    for k in range(1, n):
-        if cross:
-            pairs = [(i, i ^ (2 * k + 1)) for i in range(2 * n)]
-            got[k] = lax.ppermute(values[k], ("kv", "tp"), pairs)
-        else:
-            got[k] = lax.ppermute(values[k], "kv", [(i, i ^ k) for i in range(n)])
+    got = list(values[:first])
+    for k in range(first, n):
+        pairs = [(i, i ^ (2 * k + 1)) for i in range(2 * n)]
+        got.append(lax.ppermute(values[k], ("kv", "tp"), pairs))
     return got
 
 
@@ -441,7 +438,11 @@
     other = beside(x)
     (x,) = call(hold, [((seqs, part), bf16)], [x])
     (pair,) = call(stack, [((seqs, 2 * part), bf16)], [x, other])
-    pieces = across([pair] * n, cross=True)
+    pieces = across([pair] * n)
+    states, block_inner, taps_inner, recent_inner, norm_gain = (
+        beside(v)
+        for v in (states, block_inner, taps_inner, recent_inner, norm_gain)
+    )
     whole, step_pre, *sends = call(
         functools.partial(project, n),
         [((seqs, width), bf16), ((1, heads), f32)] + [((1, 2 * cols + 2 * maps), f32)] * n,
@@ -455,7 +456,7 @@
             step_proj.T,
         ],
     )
-    pieces = across(sends)
+    pieces = across(sends, first=0)
     sends = call(
         functools.partial(mixer, n),
         [((1, cols + LANES), f32)] * n,
@@ -481,7 +482,7 @@
         scratch=[((1, channels), f32)] * 2 + [((1, n * maps), f32)] * 2 + [((1, channels), f32)],
         scalars=(0,),
     )
-    pieces = across(sends)
+    pieces = across(sends, first=0)
     (mixed,) = call(
         functools.partial(out_project, n),
         [((seqs, width + LANES), f32)],
@@ -493,7 +494,7 @@
         [((seqs, width), bf16), ((seqs, LANES), f32)],
         [mixed, beside(mixed)],
     )
-    pieces = across([mixed] * n, cross=True)
+    pieces = across([mixed] * n)
     mid, keep, send = call(
         functools.partial(channel_mix, n, 2 * channels),
         [((seqs, part), f32)] + [((seqs, width // 2), f32)] * 2,
@@ -502,7 +503,7 @@
         scratch=[((seqs, width), f32)],
     )
     sends = call(split_pair, [((seqs, part), f32)] * n, [keep, beside(send)])
-    pieces = across(sends, cross=True)
+    pieces = across(sends)
     (out,) = call(
         functools.partial(finish, n),
         [((seqs, part), bf16)],

time: 50.1 us -> 47.7 us (0.952)
  waiting for transfers between devices: 19.1 us -> 15.8 us
  starting transfers between devices: 23 us -> 23.9 us
    ppermute x15 -> x17, waiting for transfers between devices: 16.8 us -> 13.4 us  [across(): got.append(lax.ppermute(values[k], ('kv', 'tp'), pairs))]
    ppermute x3 -> x8, starting transfers between devices: 0.92 us -> 2.17 us  [beside(): return lax.ppermute(value, 'tp', [(0, 1), (1, 0)])]
    ppermute x15 -> x17, starting transfers between devices: 22 us -> 21.7 us  [across(): got.append(lax.ppermute(values[k], ('kv', 'tp'), pairs))]
    unnamed x55 -> x50, local copies, waits for them, and re-layouts: 1.11 us -> 0.83 us
    ppermute x3 -> x8, waiting for transfers between devices: 2.34 us -> 2.38 us  [beside(): return lax.ppermute(value, 'tp', [(0, 1), (1, 0)])]
  transfers between devices with their start and end apart: 18 -> 25, of which waited for: 12 -> 13; matrix products, arithmetic and copies ran while one was open for 1% -> 1% of each run, Pallas kernels for 0% -> 3%
where the time goes in v4:
time: 47.7 us; the launch traced here: 47.6 us
  starting transfers between devices  23.9 us (50%)
  waiting for transfers between devices  15.8 us (33%)
  Pallas kernels  5.43 us (11%)
  local copies, waits for them, and re-layouts  1.42 us (3%)
  between operations  0.99 us (2%)
    ppermute x17, starting transfers between devices, across(): got.append(lax.ppermute(values[k], ('kv', 'tp'), pairs))  21.7 us
    ppermute x17, waiting for transfers between devices, across(): got.append(lax.ppermute(values[k], ('kv', 'tp'), pairs))  13.4 us
    pallas_call x9, Pallas kernels, call(): pl.pallas_call(body, out_shape=[space(s, d) for s, d in outs], in_specs=[...  5.43 us
    ppermute x8, waiting for transfers between devices, beside(): return lax.ppermute(value, 'tp', [(0, 1), (1, 0)])  2.38 us
    ppermute x8, starting transfers between devices, beside(): return lax.ppermute(value, 'tp', [(0, 1), (1, 0)])  2.17 us
  transfers between devices with their start and end apart: 25, of which 13 were waited for; matrix products, arithmetic and copies ran while one was open for 1% of the time, Pallas kernels for 3%

profile of v4, /device:TPU:0, one launch (start us, length us, event | category | flops | bytes accessed | tf_op | source)
XLA Modules:
  0.0 47.6 jit_solution(14539797317011567079)
XLA Ops:
  0.0 0.5 %collective-permute-start = (bf16[4,256]{1,0:T(4,128)(2,1)}, bf16[4,256]{1,0:T(4,128)(2,1)S(1)}, u32[]{:S(2)}, u32[]{:S(2)}) collective-permute-start(bf16[4,256]{1,0:T(4,128)(2,1)} %bitcast.43), channel_id=1, source_target_pairs={{0,1},{1,0},{2,3},{3,2},{4,5},{5,4},{6,7},{7,6},{8,9},{9,8},{10,11... | collective-permute-start | bytes 6152 | tf_op jit(solution)/shard_map/ppermute | solution.py:411
  0.5 0.7 %copy-done.17 = bf16[256,4]{0,1:T(4,128)(2,1)S(1)} copy-done((bf16[256,4]{0,1:T(4,128)(2,1)S(1)}, bf16[256,4]{0,1:T(4,128)(2,1)}, u32[]{:S(2)}) %copy-start.17) | copy-done | bytes 2072
  1.5 4.7 %collective-permute-start.3 = (bf16[4,512]{1,0:T(4,128)(2,1)S(1)}, bf16[4,512]{1,0:T(4,128)(2,1)S(1)}, u32[]{:S(2)}, u32[]{:S(2)}) collective-permute-start(bf16[4,512]{1,0:T(4,128)(2,1)S(1)} %shard_map.254.refs_0_), channel_id=1, source_target_pairs={{0,7},{1,6},{2,5},{3,4},{4,3},{5,2},{6,1},{7,0},{8,15},{9,14},{10,... | collective-permute-start | bytes 12296 | tf_op jit(solution)/shard_map/ppermute | solution.py:406
  6.2 0.5 %collective-permute-start.1 = (bf16[4,512]{1,0:T(4,128)(2,1)S(1)}, bf16[4,512]{1,0:T(4,128)(2,1)S(1)}, u32[]{:S(2)}, u32[]{:S(2)}) collective-permute-start(bf16[4,512]{1,0:T(4,128)(2,1)S(1)} %shard_map.254.refs_0_), channel_id=1, source_target_pairs={{0,3},{1,2},{2,1},{3,0},{4,7},{5,6},{6,5},{7,4},{8,11},{9,10},{10,... | collective-permute-start | bytes 12296 | tf_op jit(solution)/shard_map/ppermute | solution.py:406
  6.9 0.3 collective-permute-start.9
  7.9 2.3 %collective-permute-done.2.refs_2_ = bf16[4,512]{1,0:T(4,128)(2,1)S(1)} collective-permute-done((bf16[4,512]{1,0:T(4,128)(2,1)S(1)}, bf16[4,512]{1,0:T(4,128)(2,1)S(1)}, u32[]{:S(2)}, u32[]{:S(2)}) %collective-permute-start.2) | collective-permute-done | bytes 4128 | tf_op jit(solution)/shard_map/ppermute | solution.py:406
  10.2 0.3 collective-permute-start.11
  10.8 1.6 %shard_map.255 = (bf16[4,2048]{1,0:T(4,128)(2,1)S(1)}, f32[1,64]{1,0:T(1,128)S(1)}, f32[1,1536]{1,0:T(1,128)S(1)}, f32[1,1536]{1,0:T(1,128)S(1)}, f32[1,1536]{1,0:T(1,128)S(1)}, /*index=5*/f32[1,1536]{1,0:T(1,128)S(1)}) custom-call(bf16[4,512]{1,0:T(4,128)(2,1)S(1)} %shard_map.254.refs_0_, bf16[4,512]{1,0:T(4,128)(2,1)S(1)} %collective-permute-done.1.refs_1_, ...), custom_call_target="tpu_custom_call" | custom-call | flops 20000000000 | tf_op jit(solution)/shard_map/pallas_call | solution.py:199
  12.4 0.4 collective-permute-start.4
  12.8 1.0 %collective-permute-done.4.refs_0_ = f32[1,1536]{1,0:T(1,128)S(1)} collective-permute-done((f32[1,1536]{1,0:T(1,128)S(1)}, f32[1,1536]{1,0:T(1,128)S(1)}, u32[]{:S(2)}, u32[]{:S(2)}) %collective-permute-start.4) | collective-permute-done | bytes 6176 | tf_op jit(solution)/shard_map/ppermute | solution.py:406
  13.8 1.6 %collective-permute-start.6 = (f32[1,1536]{1,0:T(1,128)S(1)}, f32[1,1536]{1,0:T(1,128)S(1)}, u32[]{:S(2)}, u32[]{:S(2)}) collective-permute-start(f32[1,1536]{1,0:T(1,128)S(1)} %get-tuple-element.26), channel_id=1, source_target_pairs={{0,5},{1,4},{2,7},{3,6},{4,1},{5,0},{6,3},{7,2},{8,13},{9,12},{10,... | collective-permute-start | bytes 18440 | tf_op jit(solution)/shard_map/ppermute | solution.py:406
  15.4 2.4 %collective-permute-start.7 = (f32[1,1536]{1,0:T(1,128)S(1)}, f32[1,1536]{1,0:T(1,128)S(1)}, u32[]{:S(2)}, u32[]{:S(2)}) collective-permute-start(f32[1,1536]{1,0:T(1,128)S(1)} %get-tuple-element.27), channel_id=1, source_target_pairs={{0,7},{1,6},{2,5},{3,4},{4,3},{5,2},{6,1},{7,0},{8,15},{9,14},{10,... | collective-permute-start | bytes 18440 | tf_op jit(solution)/shard_map/ppermute | solution.py:406
  19.1 1.1 %collective-permute-done.7.refs_3_ = f32[1,1536]{1,0:T(1,128)S(1)} collective-permute-done((f32[1,1536]{1,0:T(1,128)S(1)}, f32[1,1536]{1,0:T(1,128)S(1)}, u32[]{:S(2)}, u32[]{:S(2)}) %collective-permute-start.7) | collective-permute-done | bytes 6176 | tf_op jit(solution)/shard_map/ppermute | solution.py:406
  20.4 0.8 %shard_map.256 = (f32[1,640]{1,0:T(1,128)S(1)}, f32[1,640]{1,0:T(1,128)S(1)}, f32[1,640]{1,0:T(1,128)S(1)}, f32[1,640]{1,0:T(1,128)S(1)}) custom-call(s32[1]{0:T(128)S(6)} %copy.34.length, f32[1,1536]{1,0:T(1,128)S(1)} %collective-permute-done.4.refs_0_, f32[1,1536]{1,0:T(1,128)S(1)} %collective-permute-done.5.refs_1_, ...), custom_call_target="tpu_custom_call" | custom-call | flops 20000000000 | tf_op jit(solution)/shard_map/pallas_call | solution.py:199
  21.2 0.3 collective-permute-start.13
  21.5 2.8 %collective-permute-start.15 = (f32[1,640]{1,0:T(1,128)S(1)}, f32[1,640]{1,0:T(1,128)S(1)}, u32[]{:S(2)}, u32[]{:S(2)}) collective-permute-start(f32[1,640]{1,0:T(1,128)S(1)} %get-tuple-element.31), channel_id=1, source_target_pairs={{0,5},{1,4},{2,7},{3,6},{4,1},{5,0},{6,3},{7,2},{8,13},{9,12},{10,... | collective-permute-start | bytes 7688 | tf_op jit(solution)/shard_map/ppermute | solution.py:406
  24.3 1.1 %collective-permute-start.16 = (f32[1,640]{1,0:T(1,128)S(1)}, f32[1,640]{1,0:T(1,128)S(1)}, u32[]{:S(2)}, u32[]{:S(2)}) collective-permute-start(f32[1,640]{1,0:T(1,128)S(1)} %get-tuple-element.32), channel_id=1, source_target_pairs={{0,7},{1,6},{2,5},{3,4},{4,3},{5,2},{6,1},{7,0},{8,15},{9,14},{10,... | collective-permute-start | bytes 7688 | tf_op jit(solution)/shard_map/ppermute | solution.py:406
  25.6 3.5 %collective-permute-done.16.refs_3_ = f32[1,640]{1,0:T(1,128)S(1)} collective-permute-done((f32[1,640]{1,0:T(1,128)S(1)}, f32[1,640]{1,0:T(1,128)S(1)}, u32[]{:S(2)}, u32[]{:S(2)}) %collective-permute-start.16) | collective-permute-done | bytes 2592 | tf_op jit(solution)/shard_map/ppermute | solution.py:406
  29.2 0.4 shard_map.257.a
  29.8 1.0 %collective-permute-done.17.b = f32[4,2176]{1,0:T(4,128)S(1)} collective-permute-done((f32[4,2176]{1,0:T(4,128)S(1)}, f32[4,2176]{1,0:T(4,128)S(1)}, u32[]{:S(2)}, u32[]{:S(2)}) %collective-permute-start.17) | collective-permute-done | bytes 34848 | tf_op jit(solution)/shard_map/ppermute | solution.py:411
  30.8 1.2 %collective-permute-start.20 = (bf16[4,2048]{1,0:T(4,128)(2,1)S(1)}, bf16[4,2048]{1,0:T(4,128)(2,1)S(1)}, u32[]{:S(2)}, u32[]{:S(2)}) collective-permute-start(bf16[4,2048]{1,0:T(4,128)(2,1)S(1)} %get-tuple-element.33.refs_0_), channel_id=1, source_target_pairs={{0,7},{1,6},{2,5},{3,4},{4,3},{5,2},{6,1},{7,0},{8,15},{9,14},{10,... | collective-permute-start | bytes 49160 | tf_op jit(solution)/shard_map/ppermute | solution.py:406
  32.0 2.8 %collective-permute-start.18 = (bf16[4,2048]{1,0:T(4,128)(2,1)S(1)}, bf16[4,2048]{1,0:T(4,128)(2,1)S(1)}, u32[]{:S(2)}, u32[]{:S(2)}) collective-permute-start(bf16[4,2048]{1,0:T(4,128)(2,1)S(1)} %get-tuple-element.33.refs_0_), channel_id=1, source_target_pairs={{0,3},{1,2},{2,1},{3,0},{4,7},{5,6},{6,5},{7,4},{8,11},{9,10},{10,... | collective-permute-start | bytes 49160 | tf_op jit(solution)/shard_map/ppermute | solution.py:406
  34.8 1.1 %collective-permute-done.20.refs_3_ = bf16[4,2048]{1,0:T(4,128)(2,1)S(1)} collective-permute-done((bf16[4,2048]{1,0:T(4,128)(2,1)S(1)}, bf16[4,2048]{1,0:T(4,128)(2,1)S(1)}, u32[]{:S(2)}, u32[]{:S(2)}) %collective-permute-start.20) | collective-permute-done | bytes 16416 | tf_op jit(solution)/shard_map/ppermute | solution.py:406
  35.9 0.8 %collective-permute-done.19.refs_2_ = bf16[4,2048]{1,0:T(4,128)(2,1)S(1)} collective-permute-done((bf16[4,2048]{1,0:T(4,128)(2,1)S(1)}, bf16[4,2048]{1,0:T(4,128)(2,1)S(1)}, u32[]{:S(2)}, u32[]{:S(2)}) %collective-permute-start.19) | collective-permute-done | bytes 16416 | tf_op jit(solution)/shard_map/ppermute | solution.py:406
  36.7 2.0 %shard_map.259 = (f32[4,256]{1,0:T(4,128)S(1)}, f32[4,1024]{1,0:T(4,128)S(1)}, f32[4,1024]{1,0:T(4,128)S(1)}) custom-call(bf16[4,2048]{1,0:T(4,128)(2,1)S(1)} %get-tuple-element.33.refs_0_, bf16[4,2048]{1,0:T(4,128)(2,1)S(1)} %collective-permute-done.18.refs_1_, bf16[4,2048]{1,0:T(4,128)(2,1)S(1)} %collective-permute-done.19.refs_2_, ...), custom_call_target="tpu_custom_call" | custom-call | flops 20000000000 | tf_op jit(solution)/shard_map/pallas_call | solution.py:199
  38.9 1.1 %collective-permute-done.21.b = f32[4,1024]{1,0:T(4,128)S(1)} collective-permute-done((f32[4,1024]{1,0:T(4,128)S(1)}, f32[4,1024]{1,0:T(4,128)S(1)}, u32[]{:S(2)}, u32[]{:S(2)}) %collective-permute-start.21) | collective-permute-done | bytes 16416 | tf_op jit(solution)/shard_map/ppermute | solution.py:411
  40.0 1.2 %collective-permute-start.22 = (f32[4,256]{1,0:T(4,128)S(1)}, f32[4,256]{1,0:T(4,128)S(1)}, u32[]{:S(2)}, u32[]{:S(2)}) collective-permute-start(f32[4,256]{1,0:T(4,128)S(1)} %get-tuple-element.39), channel_id=1, source_target_pairs={{0,3},{1,2},{2,1},{3,0},{4,7},{5,6},{6,5},{7,4},{8,11},{9,10},{10,... | collective-permute-start | bytes 12296 | tf_op jit(solution)/shard_map/ppermute | solution.py:406
  41.2 0.9 %collective-permute-start.23 = (f32[4,256]{1,0:T(4,128)S(1)}, f32[4,256]{1,0:T(4,128)S(1)}, u32[]{:S(2)}, u32[]{:S(2)}) collective-permute-start(f32[4,256]{1,0:T(4,128)S(1)} %get-tuple-element.40), channel_id=1, source_target_pairs={{0,5},{1,4},{2,7},{3,6},{4,1},{5,0},{6,3},{7,2},{8,13},{9,12},{10,... | collective-permute-start | bytes 12296 | tf_op jit(solution)/shard_map/ppermute | solution.py:406
  42.1 1.7 %collective-permute-start.24 = (f32[4,256]{1,0:T(4,128)S(1)}, f32[4,256]{1,0:T(4,128)S(1)}, u32[]{:S(2)}, u32[]{:S(2)}) collective-permute-start(f32[4,256]{1,0:T(4,128)S(1)} %get-tuple-element.41), channel_id=1, source_target_pairs={{0,7},{1,6},{2,5},{3,4},{4,3},{5,2},{6,1},{7,0},{8,15},{9,14},{10,... | collective-permute-start | bytes 12296 | tf_op jit(solution)/shard_map/ppermute | solution.py:406
  43.9 1.3 %collective-permute-done.23.refs_2_ = f32[4,256]{1,0:T(4,128)S(1)} collective-permute-done((f32[4,256]{1,0:T(4,128)S(1)}, f32[4,256]{1,0:T(4,128)S(1)}, u32[]{:S(2)}, u32[]{:S(2)}) %collective-permute-start.23) | collective-permute-done | bytes 4128 | tf_op jit(solution)/shard_map/ppermute | solution.py:406
  45.2 1.8 %collective-permute-done.24.refs_3_ = f32[4,256]{1,0:T(4,128)S(1)} collective-permute-done((f32[4,256]{1,0:T(4,128)S(1)}, f32[4,256]{1,0:T(4,128)S(1)}, u32[]{:S(2)}, u32[]{:S(2)}) %collective-permute-start.24) | collective-permute-done | bytes 4128 | tf_op jit(solution)/shard_map/ppermute | solution.py:406
  47.0 0.6 %shard_map.261 = bf16[4,256]{1,0:T(4,128)(2,1)} custom-call(f32[4,256]{1,0:T(4,128)S(1)} %get-tuple-element.38.refs_0_, f32[4,256]{1,0:T(4,128)S(1)} %collective-permute-done.22.refs_1_, f32[4,256]{1,0:T(4,128)S(1)} %collective-permute-done.23.refs_2_, f32[4,256]{1,0:T(4,128)S(1)} %collective-permute-done.24.refs_3_, f32[4,256]{1,0:T(4,128)S(1)} %get-tuple-element.42.refs_4_), custom_call_target="tpu_custom_call" | custom-call | flops 20000000000 | tf_op jit(solution)/shard_map/pallas_call | solution.py:199
  (83 shorter events, 2.5 us)
Async XLA Ops:
  0.0 1.5 %collective-permute-start = (bf16[4,256]{1,0:T(4,128)(2,1)}, bf16[4,256]{1,0:T(4,128)(2,1)S(1)}, u32[]{:S(2)}, u32[]{:S(2)}) collective-permute-start(bf16[4,256]{1,0:T(4,128)(2,1)} %bitcast.43), channel_id=1, source_target_pairs={{0,1},{1,0},{2,3},{3,2},{4,5},{5,4},{6,7},{7,6},{8,9},{9,8},{10,11... | collective-permute-start | bytes 6152 | tf_op jit(solution)/shard_map/ppermute | solution.py:411
  1.5 6.0 %collective-permute-start.3 = (bf16[4,512]{1,0:T(4,128)(2,1)S(1)}, bf16[4,512]{1,0:T(4,128)(2,1)S(1)}, u32[]{:S(2)}, u32[]{:S(2)}) collective-permute-start(bf16[4,512]{1,0:T(4,128)(2,1)S(1)} %shard_map.254.refs_0_), channel_id=1, source_target_pairs={{0,7},{1,6},{2,5},{3,4},{4,3},{5,2},{6,1},{7,0},{8,15},{9,14},{10,... | collective-permute-start | bytes 12296 | tf_op jit(solution)/shard_map/ppermute | solution.py:406
  6.2 3.9 %collective-permute-start.2 = (bf16[4,512]{1,0:T(4,128)(2,1)S(1)}, bf16[4,512]{1,0:T(4,128)(2,1)S(1)}, u32[]{:S(2)}, u32[]{:S(2)}) collective-permute-start(bf16[4,512]{1,0:T(4,128)(2,1)S(1)} %shard_map.254.refs_0_), channel_id=1, source_target_pairs={{0,5},{1,4},{2,7},{3,6},{4,1},{5,0},{6,3},{7,2},{8,13},{9,12},{10,... | collective-permute-start | bytes 12296 | tf_op jit(solution)/shard_map/ppermute | solution.py:406
  6.2 4.3 %collective-permute-start.1 = (bf16[4,512]{1,0:T(4,128)(2,1)S(1)}, bf16[4,512]{1,0:T(4,128)(2,1)S(1)}, u32[]{:S(2)}, u32[]{:S(2)}) collective-permute-start(bf16[4,512]{1,0:T(4,128)(2,1)S(1)} %shard_map.254.refs_0_), channel_id=1, source_target_pairs={{0,3},{1,2},{2,1},{3,0},{4,7},{5,6},{6,5},{7,4},{8,11},{9,10},{10,... | collective-permute-start | bytes 12296 | tf_op jit(solution)/shard_map/ppermute | solution.py:406
  6.7 5.6 %collective-permute-start.12 = (f32[64,32]{0,1:T(8,128)S(1)}, f32[64,32]{0,1:T(8,128)S(1)}, u32[]{:S(2)}, u32[]{:S(2)}) collective-permute-start(f32[64,32]{0,1:T(8,128)S(1)} %copy-done.24), channel_id=1, source_target_pairs={{0,1},{1,0},{2,3},{3,2},{4,5},{5,4},{6,7},{7,6},{8,9},{9,8},{10,11... | collective-permute-start | bytes 24584 | tf_op jit(solution)/shard_map/ppermute | solution.py:411
  6.9 6.9 %collective-permute-start.9 = (bf16[1,3,64,32]{2,3,1,0:T(8,128)(2,1)S(1)}, bf16[1,3,64,32]{2,3,1,0:T(8,128)(2,1)S(1)}, u32[]{:S(2)}, u32[]{:S(2)}) collective-permute-start(bf16[1,3,64,32]{2,3,1,0:T(8,128)(2,1)S(1)} %copy-done.23), channel_id=1, source_target_pairs={{0,1},{1,0},{2,3},{3,2},{4,5},{5,4},{6,7},{7,6},{8,9},{9,8},{10,11... | collective-permute-start | bytes 36872 | tf_op jit(solution)/shard_map/ppermute | solution.py:411
  7.6 7.9 %collective-permute-start.8 = (f32[4,64,32]{1,2,0:T(8,128)S(1)}, f32[4,64,32]{1,2,0:T(8,128)S(1)}, u32[]{:S(2)}, u32[]{:S(2)}) collective-permute-start(f32[4,64,32]{1,2,0:T(8,128)S(1)} %copy-done.22), channel_id=1, source_target_pairs={{0,1},{1,0},{2,3},{3,2},{4,5},{5,4},{6,7},{7,6},{8,9},{9,8},{10,11... | collective-permute-start | bytes 98312 | tf_op jit(solution)/shard_map/ppermute | solution.py:411
  10.2 10.1 %collective-permute-start.11 = (bf16[1,128,64,32]{1,3,2,0:T(8,128)(2,1)}, bf16[1,128,64,32]{1,3,2,0:T(8,128)(2,1)S(1)}, u32[]{:S(2)}, u32[]{:S(2)}) collective-permute-start(bf16[1,128,64,32]{1,3,2,0:T(8,128)(2,1)} %param.44), channel_id=1, source_target_pairs={{0,1},{1,0},{2,3},{3,2},{4,5},{5,4},{6,7},{7,6},{8,9},{9,8},{10,11... | collective-permute-start | bytes 1572872 | tf_op jit(solution)/shard_map/ppermute | solution.py:411
  10.5 9.8 %collective-permute-start.10 = (f32[1,64,32,128]{3,2,1,0:T(8,128)S(1)}, f32[1,64,32,128]{3,2,1,0:T(8,128)S(1)}, u32[]{:S(2)}, u32[]{:S(2)}) collective-permute-start(f32[1,64,32,128]{3,2,1,0:T(8,128)S(1)} %copy-done.21), channel_id=1, source_target_pairs={{0,1},{1,0},{2,3},{3,2},{4,5},{5,4},{6,7},{7,6},{8,9},{9,8},{10,11... | collective-permute-start | bytes 3145736 | tf_op jit(solution)/shard_map/ppermute | solution.py:411
  10.7 9.6 %copy-start.9 = (bf16[1,128,1024]{2,1,0:T(8,128)(2,1)S(1)}, bf16[1,128,1024]{2,1,0:T(8,128)(2,1)}, u32[]{:S(2)}) copy-start(bf16[1,128,1024]{2,1,0:T(8,128)(2,1)} %param.45) | copy-start | bytes 786436
  10.7 9.6 %copy-start.10 = (f32[1,128,64]{1,2,0:T(8,128)S(1)}, f32[1,128,64]{1,2,0:T(8,128)}, u32[]{:S(2)}) copy-start(f32[1,128,64]{1,2,0:T(8,128)} %param.46) | copy-start | bytes 98308
  10.7 9.6 %copy-start.11 = (f32[4,1024]{1,0:T(4,128)S(1)}, f32[4,1024]{1,0:T(4,128)}, u32[]{:S(2)}) copy-start(f32[4,1024]{1,0:T(4,128)} %refs_9_.2) | copy-start | bytes 49156
  10.7 9.6 %copy-start.12 = (f32[4,1024]{1,0:T(4,128)S(1)}, f32[4,1024]{1,0:T(4,128)}, u32[]{:S(2)}) copy-start(f32[4,1024]{1,0:T(4,128)} %refs_10_.1) | copy-start | bytes 49156
  10.8 9.6 %copy-start.14 = (bf16[1,3,1024]{2,1,0:T(4,128)(2,1)S(1)}, bf16[1,3,1024]{2,1,0:T(4,128)(2,1)}, u32[]{:S(2)}) copy-start(bf16[1,3,1024]{2,1,0:T(4,128)(2,1)} %param.41) | copy-start | bytes 18436
  10.8 9.6 %copy-start.15 = (bf16[1,3,1024]{2,1,0:T(4,128)(2,1)S(1)}, bf16[1,3,1024]{2,1,0:T(4,128)(2,1)}, u32[]{:S(2)}) copy-start(bf16[1,3,1024]{2,1,0:T(4,128)(2,1)} %param.42) | copy-start | bytes 18436
  10.8 9.6 %copy-start.18 = (f32[64]{0:T(128)S(1)}, f32[64]{0:T(128)}, u32[]{:S(2)}) copy-start(f32[64]{0:T(128)} %param.34) | copy-start | bytes 772
  12.4 1.4 %collective-permute-start.4 = (f32[1,1536]{1,0:T(1,128)S(1)}, f32[1,1536]{1,0:T(1,128)S(1)}, u32[]{:S(2)}, u32[]{:S(2)}) collective-permute-start(f32[1,1536]{1,0:T(1,128)S(1)} %get-tuple-element.24), channel_id=1, source_target_pairs={{0,1},{1,0},{2,3},{3,2},{4,5},{5,4},{6,7},{7,6},{8,9},{9,8},{10,11... | collective-permute-start | bytes 18440 | tf_op jit(solution)/shard_map/ppermute | solution.py:406
  13.8 5.3 %collective-permute-start.5 = (f32[1,1536]{1,0:T(1,128)S(1)}, f32[1,1536]{1,0:T(1,128)S(1)}, u32[]{:S(2)}, u32[]{:S(2)}) collective-permute-start(f32[1,1536]{1,0:T(1,128)S(1)} %get-tuple-element.25), channel_id=1, source_target_pairs={{0,3},{1,2},{2,1},{3,0},{4,7},{5,6},{6,5},{7,4},{8,11},{9,10},{10,... | collective-permute-start | bytes 18440 | tf_op jit(solution)/shard_map/ppermute | solution.py:406
  13.8 5.3 %collective-permute-start.6 = (f32[1,1536]{1,0:T(1,128)S(1)}, f32[1,1536]{1,0:T(1,128)S(1)}, u32[]{:S(2)}, u32[]{:S(2)}) collective-permute-start(f32[1,1536]{1,0:T(1,128)S(1)} %get-tuple-element.26), channel_id=1, source_target_pairs={{0,5},{1,4},{2,7},{3,6},{4,1},{5,0},{6,3},{7,2},{8,13},{9,12},{10,... | collective-permute-start | bytes 18440 | tf_op jit(solution)/shard_map/ppermute | solution.py:406
  15.4 4.9 %collective-permute-start.7 = (f32[1,1536]{1,0:T(1,128)S(1)}, f32[1,1536]{1,0:T(1,128)S(1)}, u32[]{:S(2)}, u32[]{:S(2)}) collective-permute-start(f32[1,1536]{1,0:T(1,128)S(1)} %get-tuple-element.27), channel_id=1, source_target_pairs={{0,7},{1,6},{2,5},{3,4},{4,3},{5,2},{6,1},{7,0},{8,15},{9,14},{10,... | collective-permute-start | bytes 18440 | tf_op jit(solution)/shard_map/ppermute | solution.py:406
  21.2 4.2 %collective-permute-start.13 = (f32[1,640]{1,0:T(1,128)S(1)}, f32[1,640]{1,0:T(1,128)S(1)}, u32[]{:S(2)}, u32[]{:S(2)}) collective-permute-start(f32[1,640]{1,0:T(1,128)S(1)} %get-tuple-element.29), channel_id=1, source_target_pairs={{0,1},{1,0},{2,3},{3,2},{4,5},{5,4},{6,7},{7,6},{8,9},{9,8},{10,11... | collective-permute-start | bytes 7688 | tf_op jit(solution)/shard_map/ppermute | solution.py:406
  21.5 3.9 %collective-permute-start.14 = (f32[1,640]{1,0:T(1,128)S(1)}, f32[1,640]{1,0:T(1,128)S(1)}, u32[]{:S(2)}, u32[]{:S(2)}) collective-permute-start(f32[1,640]{1,0:T(1,128)S(1)} %get-tuple-element.30), channel_id=1, source_target_pairs={{0,3},{1,2},{2,1},{3,0},{4,7},{5,6},{6,5},{7,4},{8,11},{9,10},{10,... | collective-permute-start | bytes 7688 | tf_op jit(solution)/shard_map/ppermute | solution.py:406
  21.5 4.1 %collective-permute-start.15 = (f32[1,640]{1,0:T(1,128)S(1)}, f32[1,640]{1,0:T(1,128)S(1)}, u32[]{:S(2)}, u32[]{:S(2)}) collective-permute-start(f32[1,640]{1,0:T(1,128)S(1)} %get-tuple-element.31), channel_id=1, source_target_pairs={{0,5},{1,4},{2,7},{3,6},{4,1},{5,0},{6,3},{7,2},{8,13},{9,12},{10,... | collective-permute-start | bytes 7688 | tf_op jit(solution)/shard_map/ppermute | solution.py:406
  24.3 4.8 %collective-permute-start.16 = (f32[1,640]{1,0:T(1,128)S(1)}, f32[1,640]{1,0:T(1,128)S(1)}, u32[]{:S(2)}, u32[]{:S(2)}) collective-permute-start(f32[1,640]{1,0:T(1,128)S(1)} %get-tuple-element.32), channel_id=1, source_target_pairs={{0,7},{1,6},{2,5},{3,4},{4,3},{5,2},{6,1},{7,0},{8,15},{9,14},{10,... | collective-permute-start | bytes 7688 | tf_op jit(solution)/shard_map/ppermute | solution.py:406
  29.6 1.3 %collective-permute-start.17 = (f32[4,2176]{1,0:T(4,128)S(1)}, f32[4,2176]{1,0:T(4,128)S(1)}, u32[]{:S(2)}, u32[]{:S(2)}) collective-permute-start(f32[4,2176]{1,0:T(4,128)S(1)} %shard_map.257.a), channel_id=1, source_target_pairs={{0,1},{1,0},{2,3},{3,2},{4,5},{5,4},{6,7},{7,6},{8,9},{9,8},{10,11... | collective-permute-start | bytes 104456 | tf_op jit(solution)/shard_map/ppermute | solution.py:411
  30.8 5.0 %collective-permute-start.20 = (bf16[4,2048]{1,0:T(4,128)(2,1)S(1)}, bf16[4,2048]{1,0:T(4,128)(2,1)S(1)}, u32[]{:S(2)}, u32[]{:S(2)}) collective-permute-start(bf16[4,2048]{1,0:T(4,128)(2,1)S(1)} %get-tuple-element.33.refs_0_), channel_id=1, source_target_pairs={{0,7},{1,6},{2,5},{3,4},{4,3},{5,2},{6,1},{7,0},{8,15},{9,14},{10,... | collective-permute-start | bytes 49160 | tf_op jit(solution)/shard_map/ppermute | solution.py:406
  32.0 4.7 %collective-permute-start.19 = (bf16[4,2048]{1,0:T(4,128)(2,1)S(1)}, bf16[4,2048]{1,0:T(4,128)(2,1)S(1)}, u32[]{:S(2)}, u32[]{:S(2)}) collective-permute-start(bf16[4,2048]{1,0:T(4,128)(2,1)S(1)} %get-tuple-element.33.refs_0_), channel_id=1, source_target_pairs={{0,5},{1,4},{2,7},{3,6},{4,1},{5,0},{6,3},{7,2},{8,13},{9,12},{10,... | collective-permute-start | bytes 49160 | tf_op jit(solution)/shard_map/ppermute | solution.py:406
  32.0 4.7 %collective-permute-start.18 = (bf16[4,2048]{1,0:T(4,128)(2,1)S(1)}, bf16[4,2048]{1,0:T(4,128)(2,1)S(1)}, u32[]{:S(2)}, u32[]{:S(2)}) collective-permute-start(bf16[4,2048]{1,0:T(4,128)(2,1)S(1)} %get-tuple-element.33.refs_0_), channel_id=1, source_target_pairs={{0,3},{1,2},{2,1},{3,0},{4,7},{5,6},{6,5},{7,4},{8,11},{9,10},{10,... | collective-permute-start | bytes 49160 | tf_op jit(solution)/shard_map/ppermute | solution.py:406
  38.8 1.2 %collective-permute-start.21 = (f32[4,1024]{1,0:T(4,128)S(1)}, f32[4,1024]{1,0:T(4,128)S(1)}, u32[]{:S(2)}, u32[]{:S(2)}) collective-permute-start(f32[4,1024]{1,0:T(4,128)S(1)} %get-tuple-element.37), channel_id=1, source_target_pairs={{0,1},{1,0},{2,3},{3,2},{4,5},{5,4},{6,7},{7,6},{8,9},{9,8},{10,11... | collective-permute-start | bytes 49160 | tf_op jit(solution)/shard_map/ppermute | solution.py:411
  40.0 3.9 %collective-permute-start.22 = (f32[4,256]{1,0:T(4,128)S(1)}, f32[4,256]{1,0:T(4,128)S(1)}, u32[]{:S(2)}, u32[]{:S(2)}) collective-permute-start(f32[4,256]{1,0:T(4,128)S(1)} %get-tuple-element.39), channel_id=1, source_target_pairs={{0,3},{1,2},{2,1},{3,0},{4,7},{5,6},{6,5},{7,4},{8,11},{9,10},{10,... | collective-permute-start | bytes 12296 | tf_op jit(solution)/shard_map/ppermute | solution.py:406
  41.2 4.0 %collective-permute-start.23 = (f32[4,256]{1,0:T(4,128)S(1)}, f32[4,256]{1,0:T(4,128)S(1)}, u32[]{:S(2)}, u32[]{:S(2)}) collective-permute-start(f32[4,256]{1,0:T(4,128)S(1)} %get-tuple-element.40), channel_id=1, source_target_pairs={{0,5},{1,4},{2,7},{3,6},{4,1},{5,0},{6,3},{7,2},{8,13},{9,12},{10,... | collective-permute-start | bytes 12296 | tf_op jit(solution)/shard_map/ppermute | solution.py:406
  42.1 4.8 %collective-permute-start.24 = (f32[4,256]{1,0:T(4,128)S(1)}, f32[4,256]{1,0:T(4,128)S(1)}, u32[]{:S(2)}, u32[]{:S(2)}) collective-permute-start(f32[4,256]{1,0:T(4,128)S(1)} %get-tuple-element.41), channel_id=1, source_target_pairs={{0,7},{1,6},{2,5},{3,4},{4,3},{5,2},{6,1},{7,0},{8,15},{9,14},{10,... | collective-permute-start | bytes 12296 | tf_op jit(solution)/shard_map/ppermute | solution.py:406
  (18 other events, 141.1 us)

commit v5 on v4

--- a/solution.py
+++ b/solution.py
@@ -192,22 +192,17 @@
 
 
 def call(body, outs, args, scratch=(), scalars=(), space=pltpu.VMEM):
-    args = [
-        a if i in scalars else pltpu.with_memory_space_constraint(a, pltpu.VMEM)
-        for i, a in enumerate(args)
-    ]
+    args = [pltpu.with_memory_space_constraint(a, pltpu.VMEM) for a in args]
     return pl.pallas_call(
         body,
         out_shape=[space(s, d) for s, d in outs],
-        in_specs=[
-            pl.BlockSpec(memory_space=pltpu.SMEM if i in scalars else pltpu.VMEM)
-            for i in range(len(args))
-        ],
+        in_specs=[pl.BlockSpec(memory_space=pltpu.VMEM) for _ in args]
+        + [pl.BlockSpec(memory_space=pltpu.SMEM) for _ in scalars],
         out_specs=[pl.BlockSpec(memory_space=pltpu.VMEM) for _ in outs],
         scratch_shapes=[pltpu.VMEM(s, d) for s, d in scratch],
         compiler_params=pltpu.CompilerParams(vmem_limit_bytes=8 << 20),
         cost_estimate=pl.CostEstimate(flops=20_000_000_000, bytes_accessed=0, transcendentals=0),
-    )(*args)
+    )(*args, *scalars)
 
 
 def lane(start, size):
@@ -219,48 +214,70 @@
 
 
 def stack(a, b, out):
+    tp = lax.axis_index("tp")
     part = a.shape[1]
-    out[:, :part] = a[...]
-    out[:, part:] = b[...]
+    out[:, lane(tp * part, part)] = a[...]
+    out[:, lane((1 - tp) * part, part)] = b[...]
+
+
+def pack(taps, recent, gain, out):
+    n, last = taps.shape[0], out.shape[0] - 1
+    out[:n] = taps[...]
+    out[n:last] = recent[...].astype(jnp.float32)
+    out[last] = gain[...]
+
+
+def products(piece, base, gain, gate_w, inner_w, input_w, output_w, step_w):
+    at = lane(base, piece.shape[1])
+    normed = (piece[...].astype(jnp.float32) * gain[:, at]).astype(jnp.bfloat16)
+    return (
+        dot(normed, gate_w[:, at], NT),
+        dot(normed, inner_w[:, at], NT),
+        dot(normed, input_w[at, :], NN),
+        dot(normed, output_w[at, :], NN),
+        dot(normed, step_w[:, at], NT),
+    )
+
+
+def project_own(piece, *refs):
+    base = lax.axis_index("kv") * piece.shape[1]
+    for out, value in zip(refs[6:], products(piece, base, *refs[:6])):
+        out[...] = value
 
 
 def project(n, *refs):
-    pieces, refs = refs[:n], refs[n:]
-    mixer_gain, gate_w, inner_w, input_w, output_w, step_w = refs[:6]
-    x_out, step_out = refs[6:8]
-    sends = refs[8:]
-    kv, tp = lax.axis_index("kv"), lax.axis_index("tp")
+    pieces, weights, sums = refs[:n], refs[n : n + 6], refs[n + 6 : n + 11]
+    x_out, step_out, *sends = refs[n + 11 :]
+    kv = lax.axis_index("kv")
     width = x_out.shape[1]
-    part = pieces[0].shape[1] // 2
+    part = pieces[0].shape[1]
+    totals = [ref[...] for ref in sums]
     for k, ref in enumerate(pieces):
-        base = (kv ^ k) * (2 * part)
-        first = tp if k == 0 else 1 - tp
-        x_out[:, lane(base + first * part, part)] = ref[:, :part]
-        x_out[:, lane(base + (1 - first) * part, part)] = ref[:, part:]
+        base = (kv ^ k) * part
+        x_out[:, lane(base, part)] = ref[...]
+        if k:
+            totals = [a + b for a, b in zip(totals, products(ref, base, *weights))]
     x = x_out[...].astype(jnp.float32)
     rms = lax.rsqrt(jnp.sum(x * x, axis=1, keepdims=True) / width + epsilon)
-    normed = (x * mixer_gain[...]).astype(jnp.bfloat16)
     at = 0
-    for weight, dims in ((gate_w, NT), (inner_w, NT), (input_w, NN), (output_w, NN)):
-        value = rms * dot(normed, weight[...], dims)
-        value = value.astype(jnp.bfloat16).astype(jnp.float32)
+    for value in totals[:-1]:
+        value = (rms * value).astype(jnp.bfloat16).astype(jnp.float32)
         row = lax.broadcasted_iota(jnp.int32, value.shape, 0)
         for k, ref in enumerate(sends):
             picked = jnp.sum(jnp.where(row == (kv ^ k), value, 0.0), axis=0, keepdims=True)
             ref[:, at : at + value.shape[1]] = picked
         at += value.shape[1]
-    steps = (rms * dot(normed, step_w[...], NT)).astype(jnp.bfloat16).astype(jnp.float32)
+    steps = (rms * totals[-1]).astype(jnp.bfloat16).astype(jnp.float32)
     row = lax.broadcasted_iota(jnp.int32, steps.shape, 0)
     step_out[...] = jnp.sum(jnp.where(row == kv, steps, 0.0), axis=0, keepdims=True)
 
 
-def mixer(n, length, *refs):
+def mixer(n, *refs):
     pieces, refs = refs[:n], refs[n:]
     step_pre, step_bias, decay_log, skip_gain = refs[:4]
-    taps_inner, taps_input, taps_output = refs[4:7]
-    recent_inner, recent_input, recent_output = refs[7:10]
-    states, block_inner, block_input, block_decay, norm_gain = refs[10:15]
-    sends, (gate_row, inner_row, input_row, output_row, gated_row) = refs[15:-5], refs[-5:]
+    packed, taps_input, taps_output, recent_input, recent_output = refs[4:9]
+    states, block_inner, block_input, block_decay, length = refs[9:14]
+    sends, (gate_row, inner_row, input_row, output_row, gated_row) = refs[14:-5], refs[-5:]
     kv = lax.axis_index("kv")
     heads, span = block_decay.shape
     channels = gate_row.shape[1]
@@ -278,13 +295,15 @@
         output_row[:, lane(src * maps, maps)] = ref[:, 2 * cols + maps :]
 
     def conv(recent, newest, taps):
-        weights = taps[...]
-        past = jnp.sum(recent[...].astype(jnp.float32) * weights[:-1], axis=0, keepdims=True)
-        return silu(past + weights[-1:] * newest)
-
-    conv_output = conv(recent_output, output_row[...], taps_output).astype(jnp.bfloat16)
-    conv_input = conv(recent_input, input_row[...], taps_input)
-    conv_inner = conv(recent_inner, inner_row[...], taps_inner)
+        past = jnp.sum(recent.astype(jnp.float32) * taps[:-1], axis=0, keepdims=True)
+        return silu(past + taps[-1:] * newest)
+
+    count = taps_input.shape[0]
+    conv_output = conv(recent_output[...], output_row[...], taps_output[...]).astype(jnp.bfloat16)
+    conv_input = conv(recent_input[...], input_row[...], taps_input[...])
+    last = packed.shape[0] - 1
+    conv_inner = conv(packed[count:last], inner_row[...], packed[:count])
+    norm_gain = packed[last:]
     readout = conv_output.astype(jnp.float32)
 
     eye = lax.broadcasted_iota(jnp.int32, (heads, heads), 0) == lax.broadcasted_iota(
@@ -326,15 +345,18 @@
     for g in range(groups):
         head = slice(g * per_group, (g + 1) * per_group)
         rows = slice(g * chunk, (g + 1) * chunk)
-        weight = (decayed[head] * score[g : g + 1]).astype(jnp.bfloat16)
-        from_block = dot(weight, block_inner[rows, :], NT)
-        state = states[rows, :]
-        high = state.astype(jnp.bfloat16)
-        low = (state - high.astype(jnp.float32)).astype(jnp.bfloat16)
-        out_map = jnp.broadcast_to(
-            readout[:, g * size : (g + 1) * size], (per_group, size)
-        ).astype(jnp.bfloat16)
-        from_state = dot(out_map, high, NT) + dot(out_map, low, NT)
+        weight = decayed[head] * score[g : g + 1]
+        out_map = jnp.broadcast_to(readout[:, g * size : (g + 1) * size], (per_group, size))
+        left = jnp.concatenate(
+            [
+                jnp.concatenate([weight, jnp.zeros((per_group, size), jnp.float32)], axis=1),
+                jnp.concatenate([jnp.zeros((per_group, span), jnp.float32), out_map], axis=1),
+            ],
+            axis=0,
+        )
+        right = jnp.concatenate([block_inner[rows, :], states[rows, :].astype(jnp.bfloat16)], axis=1)
+        product = dot(left.astype(jnp.bfloat16), right, NT)
+        from_block, from_state = product[:per_group], product[per_group:]
         direct = own_score[g : g + 1] * step[head] + skip[head]
         both = from_block + grown[head] * from_state + direct * conv_inner[:, rows]
         mix = jnp.sum(jnp.where(mine, both, 0.0), axis=0, keepdims=True)
@@ -439,48 +461,56 @@
     (x,) = call(hold, [((seqs, part), bf16)], [x])
     (pair,) = call(stack, [((seqs, 2 * part), bf16)], [x, other])
     pieces = across([pair] * n)
-    states, block_inner, taps_inner, recent_inner, norm_gain = (
-        beside(v)
-        for v in (states, block_inner, taps_inner, recent_inner, norm_gain)
+    taps = taps_inner.shape[0]
+    rows = 2 * taps
+    (packed,) = call(
+        pack,
+        [((rows, half, heads), f32)],
+        [taps_inner.transpose(0, 2, 1), recent_inner[0].transpose(0, 2, 1), norm_gain.T],
+    )
+    packed, states, block_inner = (
+        beside(v) for v in (packed, states, block_inner)
+    )
+    weights = [
+        mixer_gain.reshape(1, width),
+        gate_proj.transpose(1, 2, 0).reshape(cols, width),
+        inner_proj.transpose(1, 2, 0).reshape(cols, width),
+        input_proj,
+        output_proj,
+        step_proj.T,
+    ]
+    sums = call(
+        project_own,
+        [((seqs, c), f32) for c in (cols, cols, maps, maps, heads)],
+        [pair] + weights,
     )
     whole, step_pre, *sends = call(
         functools.partial(project, n),
         [((seqs, width), bf16), ((1, heads), f32)] + [((1, 2 * cols + 2 * maps), f32)] * n,
-        pieces
-        + [
-            mixer_gain.reshape(1, width),
-            gate_proj.transpose(1, 2, 0).reshape(cols, width),
-            inner_proj.transpose(1, 2, 0).reshape(cols, width),
-            input_proj,
-            output_proj,
-            step_proj.T,
-        ],
+        pieces + weights + list(sums),
     )
     pieces = across(sends, first=0)
     sends = call(
         functools.partial(mixer, n),
         [((1, cols + LANES), f32)] * n,
-        [lengths]
-        + pieces
+        pieces
         + [
             step_pre,
             step_bias.reshape(1, heads),
             decay_log.reshape(1, heads),
             skip_gain.reshape(1, heads),
-            taps_inner.reshape(-1, channels),
+            packed.transpose(0, 2, 1).reshape(rows, channels),
             taps_input,
             taps_output,
-            recent_inner.reshape(-1, channels),
             recent_input[0],
             recent_output[0],
             states.reshape(channels, size),
             block_inner.transpose(0, 2, 3, 1).reshape(channels, -1),
             block_input[0],
             block_decay[0].T,
-            norm_gain.reshape(1, channels),
         ],
+        scalars=[lengths],
         scratch=[((1, channels), f32)] * 2 + [((1, n * maps), f32)] * 2 + [((1, channels), f32)],
-        scalars=(0,),
     )
     pieces = across(sends, first=0)
     (mixed,) = call(

time: 47.7 us -> 48.4 us (1.015)
  starting transfers between devices: 23.9 us -> 22.2 us
  local copies, waits for them, and re-layouts: 1.42 us -> 2.96 us
  waiting for transfers between devices: 15.8 us -> 16.4 us
    unnamed x50, local copies, waits for them, and re-layouts: 0.83 us -> 2.69 us
    ppermute x17, starting transfers between devices: 21.7 us -> 20.3 us  [across(): got.append(lax.ppermute(values[k], ('kv', 'tp'), pairs))]
    ppermute x17, waiting for transfers between devices: 13.4 us -> 14.3 us  [across(): got.append(lax.ppermute(values[k], ('kv', 'tp'), pairs))]
    ppermute x8 -> x6, waiting for transfers between devices: 2.38 us -> 2.12 us  [beside(): return lax.ppermute(value, 'tp', [(0, 1), (1, 0)])]
    ppermute x8 -> x6, starting transfers between devices: 2.17 us -> 1.93 us  [beside(): return lax.ppermute(value, 'tp', [(0, 1), (1, 0)])]
    pallas_call x9 -> x11, Pallas kernels: 5.43 us -> 5.47 us  [call(): pl.pallas_call(body, out_shape=[space(s, d) for s, d in outs], in_specs=[...]
  transfers between devices with their start and end apart: 25 -> 23, of which waited for: 13 -> 11; matrix products, arithmetic and copies ran while one was open for 1% -> 1% of each run, Pallas kernels for 3% -> 4%
where the time goes in v5:
time: 48.4 us; the launch traced here: 48 us
  starting transfers between devices  22.2 us (46%)
  waiting for transfers between devices  16.4 us (34%)
  Pallas kernels  5.47 us (11%)
  local copies, waits for them, and re-layouts  2.96 us (6%)
  between operations  0.95 us (2%)
    ppermute x17, starting transfers between devices, across(): got.append(lax.ppermute(values[k], ('kv', 'tp'), pairs))  20.3 us
    ppermute x17, waiting for transfers between devices, across(): got.append(lax.ppermute(values[k], ('kv', 'tp'), pairs))  14.3 us
    pallas_call x11, Pallas kernels, call(): pl.pallas_call(body, out_shape=[space(s, d) for s, d in outs], in_specs=[...  5.47 us
    unnamed x50, local copies, waits for them, and re-layouts  2.69 us
    ppermute x6, waiting for transfers between devices, beside(): return lax.ppermute(value, 'tp', [(0, 1), (1, 0)])  2.12 us
    ppermute x6, starting transfers between devices, beside(): return lax.ppermute(value, 'tp', [(0, 1), (1, 0)])  1.93 us
  transfers between devices with their start and end apart: 23, of which 11 were waited for; matrix products, arithmetic and copies ran while one was open for 1% of the time, Pallas kernels for 4%

profile of v5, /device:TPU:0, one launch (start us, length us, event | category | flops | bytes accessed | tf_op | source)
XLA Modules:
  0.0 48.0 jit_solution(8499106260384793799)
XLA Ops:
  0.0 0.5 %collective-permute-start = (bf16[4,256]{1,0:T(4,128)(2,1)}, bf16[4,256]{1,0:T(4,128)(2,1)S(1)}, u32[]{:S(2)}, u32[]{:S(2)}) collective-permute-start(bf16[4,256]{1,0:T(4,128)(2,1)} %bitcast.54), channel_id=1, source_target_pairs={{0,1},{1,0},{2,3},{3,2},{4,5},{5,4},{6,7},{7,6},{8,9},{9,8},{10,11... | collective-permute-start | bytes 6152 | tf_op jit(solution)/shard_map/ppermute | solution.py:433
  0.5 0.8 %copy-done.10 = f32[4,64,32]{1,2,0:T(8,128)S(1)} copy-done((f32[4,64,32]{1,2,0:T(8,128)S(1)}, f32[4,64,32]{1,2,0:T(8,128)}, u32[]{:S(2)}) %copy-start.10) | copy-done | bytes 32792
  1.3 0.7 %copy-done.12 = bf16[1,3,64,32]{2,3,1,0:T(8,128)(2,1)S(1)} copy-done((bf16[1,3,64,32]{2,3,1,0:T(8,128)(2,1)S(1)}, bf16[1,3,64,32]{2,3,1,0:T(8,128)(2,1)}, u32[]{:S(2)}) %copy-start.12) | copy-done | bytes 12312
  2.1 0.7 %copy-done.13 = f32[64,32]{0,1:T(8,128)S(1)} copy-done((f32[64,32]{0,1:T(8,128)S(1)}, f32[64,32]{0,1:T(8,128)}, u32[]{:S(2)}) %copy-start.13) | copy-done | bytes 8216
  2.9 0.5 %collective-permute-start.10 = (bf16[1,128,64,32]{1,3,2,0:T(8,128)(2,1)}, bf16[1,128,64,32]{1,3,2,0:T(8,128)(2,1)S(1)}, u32[]{:S(2)}, u32[]{:S(2)}) collective-permute-start(bf16[1,128,64,32]{1,3,2,0:T(8,128)(2,1)} %param.44), channel_id=1, source_target_pairs={{0,1},{1,0},{2,3},{3,2},{4,5},{5,4},{6,7},{7,6},{8,9},{9,8},{10,11... | collective-permute-start | bytes 1572872 | tf_op jit(solution)/shard_map/ppermute | solution.py:433
  3.5 4.8 %collective-permute-start.3 = (bf16[4,512]{1,0:T(4,128)(2,1)S(1)}, bf16[4,512]{1,0:T(4,128)(2,1)S(1)}, u32[]{:S(2)}, u32[]{:S(2)}) collective-permute-start(bf16[4,512]{1,0:T(4,128)(2,1)S(1)} %shard_map.254.piece.refs_0_), channel_id=1, source_target_pairs={{0,7},{1,6},{2,5},{3,4},{4,3},{5,2},{6,1},{7,0},{8,15},{9,14},{10,... | collective-permute-start | bytes 12296 | tf_op jit(solution)/shard_map/ppermute | solution.py:428
  8.6 0.5 shard_map.255
  9.1 0.6 %collective-permute-done.3.refs_3_ = bf16[4,512]{1,0:T(4,128)(2,1)S(1)} collective-permute-done((bf16[4,512]{1,0:T(4,128)(2,1)S(1)}, bf16[4,512]{1,0:T(4,128)(2,1)S(1)}, u32[]{:S(2)}, u32[]{:S(2)}) %collective-permute-start.3) | collective-permute-done | bytes 4128 | tf_op jit(solution)/shard_map/ppermute | solution.py:428
  9.8 0.5 %collective-permute-start.9 = (f32[1,64,32,128]{3,2,1,0:T(8,128)S(1)}, f32[1,64,32,128]{3,2,1,0:T(8,128)S(1)}, u32[]{:S(2)}, u32[]{:S(2)}) collective-permute-start(f32[1,64,32,128]{3,2,1,0:T(8,128)S(1)} %copy-done.24), channel_id=1, source_target_pairs={{0,1},{1,0},{2,3},{3,2},{4,5},{5,4},{6,7},{7,6},{8,9},{9,8},{10,11... | collective-permute-start | bytes 3145736 | tf_op jit(solution)/shard_map/ppermute | solution.py:433
  10.3 1.9 %collective-permute-done.2.refs_2_ = bf16[4,512]{1,0:T(4,128)(2,1)S(1)} collective-permute-done((bf16[4,512]{1,0:T(4,128)(2,1)S(1)}, bf16[4,512]{1,0:T(4,128)(2,1)S(1)}, u32[]{:S(2)}, u32[]{:S(2)}) %collective-permute-start.2) | collective-permute-done | bytes 4128 | tf_op jit(solution)/shard_map/ppermute | solution.py:428
  12.3 1.3 %shard_map.256 = (bf16[4,2048]{1,0:T(4,128)(2,1)S(1)}, f32[1,64]{1,0:T(1,128)S(1)}, f32[1,1536]{1,0:T(1,128)S(1)}, f32[1,1536]{1,0:T(1,128)S(1)}, f32[1,1536]{1,0:T(1,128)S(1)}, /*index=5*/f32[1,1536]{1,0:T(1,128)S(1)}) custom-call(bf16[4,512]{1,0:T(4,128)(2,1)S(1)} %shard_map.254.piece.refs_0_, bf16[4,512]{1,0:T(4,128)(2,1)S(1)} %collective-permute-done.1.refs_1_, ...), custom_call_target="tpu_custom_call" | custom-call | flops 20000000000 | tf_op jit(solution)/shard_map/pallas_call | solution.py:196
  13.8 1.1 %collective-permute-done.4.refs_0_ = f32[1,1536]{1,0:T(1,128)S(1)} collective-permute-done((f32[1,1536]{1,0:T(1,128)S(1)}, f32[1,1536]{1,0:T(1,128)S(1)}, u32[]{:S(2)}, u32[]{:S(2)}) %collective-permute-start.4) | collective-permute-done | bytes 6176 | tf_op jit(solution)/shard_map/ppermute | solution.py:428
  14.8 1.7 %collective-permute-start.6 = (f32[1,1536]{1,0:T(1,128)S(1)}, f32[1,1536]{1,0:T(1,128)S(1)}, u32[]{:S(2)}, u32[]{:S(2)}) collective-permute-start(f32[1,1536]{1,0:T(1,128)S(1)} %get-tuple-element.36), channel_id=1, source_target_pairs={{0,5},{1,4},{2,7},{3,6},{4,1},{5,0},{6,3},{7,2},{8,13},{9,12},{10,... | collective-permute-start | bytes 18440 | tf_op jit(solution)/shard_map/ppermute | solution.py:428
  16.6 1.3 %collective-permute-start.7 = (f32[1,1536]{1,0:T(1,128)S(1)}, f32[1,1536]{1,0:T(1,128)S(1)}, u32[]{:S(2)}, u32[]{:S(2)}) collective-permute-start(f32[1,1536]{1,0:T(1,128)S(1)} %get-tuple-element.37), channel_id=1, source_target_pairs={{0,7},{1,6},{2,5},{3,4},{4,3},{5,2},{6,1},{7,0},{8,15},{9,14},{10,... | collective-permute-start | bytes 18440 | tf_op jit(solution)/shard_map/ppermute | solution.py:428
  18.8 2.6 %collective-permute-done.7.refs_3_ = f32[1,1536]{1,0:T(1,128)S(1)} collective-permute-done((f32[1,1536]{1,0:T(1,128)S(1)}, f32[1,1536]{1,0:T(1,128)S(1)}, u32[]{:S(2)}, u32[]{:S(2)}) %collective-permute-start.7) | collective-permute-done | bytes 6176 | tf_op jit(solution)/shard_map/ppermute | solution.py:428
  21.5 0.7 %shard_map.258 = (f32[1,640]{1,0:T(1,128)S(1)}, f32[1,640]{1,0:T(1,128)S(1)}, f32[1,640]{1,0:T(1,128)S(1)}, f32[1,640]{1,0:T(1,128)S(1)}) custom-call(f32[1,1536]{1,0:T(1,128)S(1)} %collective-permute-done.4.refs_0_, f32[1,1536]{1,0:T(1,128)S(1)} %collective-permute-done.5.refs_1_, f32[1,1536]{1,0:T(1,128)S(1)} %collective-permute-done.6.refs_2_, ...), custom_call_target="tpu_custom_call" | custom-call | flops 20000000000 | tf_op jit(solution)/shard_map/pallas_call | solution.py:196
  22.4 1.8 %collective-permute-start.13 = (f32[1,640]{1,0:T(1,128)S(1)}, f32[1,640]{1,0:T(1,128)S(1)}, u32[]{:S(2)}, u32[]{:S(2)}) collective-permute-start(f32[1,640]{1,0:T(1,128)S(1)} %get-tuple-element.41), channel_id=1, source_target_pairs={{0,5},{1,4},{2,7},{3,6},{4,1},{5,0},{6,3},{7,2},{8,13},{9,12},{10,... | collective-permute-start | bytes 7688 | tf_op jit(solution)/shard_map/ppermute | solution.py:428
  24.2 2.2 %collective-permute-start.14 = (f32[1,640]{1,0:T(1,128)S(1)}, f32[1,640]{1,0:T(1,128)S(1)}, u32[]{:S(2)}, u32[]{:S(2)}) collective-permute-start(f32[1,640]{1,0:T(1,128)S(1)} %get-tuple-element.42), channel_id=1, source_target_pairs={{0,7},{1,6},{2,5},{3,4},{4,3},{5,2},{6,1},{7,0},{8,15},{9,14},{10,... | collective-permute-start | bytes 7688 | tf_op jit(solution)/shard_map/ppermute | solution.py:428
  26.5 2.6 %collective-permute-done.14.refs_3_ = f32[1,640]{1,0:T(1,128)S(1)} collective-permute-done((f32[1,640]{1,0:T(1,128)S(1)}, f32[1,640]{1,0:T(1,128)S(1)}, u32[]{:S(2)}, u32[]{:S(2)}) %collective-permute-start.14) | collective-permute-done | bytes 2592 | tf_op jit(solution)/shard_map/ppermute | solution.py:428
  29.6 1.1 %collective-permute-done.15.b = f32[4,2176]{1,0:T(4,128)S(1)} collective-permute-done((f32[4,2176]{1,0:T(4,128)S(1)}, f32[4,2176]{1,0:T(4,128)S(1)}, u32[]{:S(2)}, u32[]{:S(2)}) %collective-permute-start.15) | collective-permute-done | bytes 34848 | tf_op jit(solution)/shard_map/ppermute | solution.py:433
  30.7 2.3 %collective-permute-start.18 = (bf16[4,2048]{1,0:T(4,128)(2,1)S(1)}, bf16[4,2048]{1,0:T(4,128)(2,1)S(1)}, u32[]{:S(2)}, u32[]{:S(2)}) collective-permute-start(bf16[4,2048]{1,0:T(4,128)(2,1)S(1)} %get-tuple-element.43.refs_0_), channel_id=1, source_target_pairs={{0,7},{1,6},{2,5},{3,4},{4,3},{5,2},{6,1},{7,0},{8,15},{9,14},{10,... | collective-permute-start | bytes 49160 | tf_op jit(solution)/shard_map/ppermute | solution.py:428
  33.0 1.7 %collective-permute-start.16 = (bf16[4,2048]{1,0:T(4,128)(2,1)S(1)}, bf16[4,2048]{1,0:T(4,128)(2,1)S(1)}, u32[]{:S(2)}, u32[]{:S(2)}) collective-permute-start(bf16[4,2048]{1,0:T(4,128)(2,1)S(1)} %get-tuple-element.43.refs_0_), channel_id=1, source_target_pairs={{0,3},{1,2},{2,1},{3,0},{4,7},{5,6},{6,5},{7,4},{8,11},{9,10},{10,... | collective-permute-start | bytes 49160 | tf_op jit(solution)/shard_map/ppermute | solution.py:428
  34.7 1.1 %collective-permute-done.18.refs_3_ = bf16[4,2048]{1,0:T(4,128)(2,1)S(1)} collective-permute-done((bf16[4,2048]{1,0:T(4,128)(2,1)S(1)}, bf16[4,2048]{1,0:T(4,128)(2,1)S(1)}, u32[]{:S(2)}, u32[]{:S(2)}) %collective-permute-start.18) | collective-permute-done | bytes 16416 | tf_op jit(solution)/shard_map/ppermute | solution.py:428
  35.8 1.3 %collective-permute-done.17.refs_2_ = bf16[4,2048]{1,0:T(4,128)(2,1)S(1)} collective-permute-done((bf16[4,2048]{1,0:T(4,128)(2,1)S(1)}, bf16[4,2048]{1,0:T(4,128)(2,1)S(1)}, u32[]{:S(2)}, u32[]{:S(2)}) %collective-permute-start.17) | collective-permute-done | bytes 16416 | tf_op jit(solution)/shard_map/ppermute | solution.py:428
  37.1 2.0 %shard_map.261 = (f32[4,256]{1,0:T(4,128)S(1)}, f32[4,1024]{1,0:T(4,128)S(1)}, f32[4,1024]{1,0:T(4,128)S(1)}) custom-call(bf16[4,2048]{1,0:T(4,128)(2,1)S(1)} %get-tuple-element.43.refs_0_, bf16[4,2048]{1,0:T(4,128)(2,1)S(1)} %collective-permute-done.16.refs_1_, bf16[4,2048]{1,0:T(4,128)(2,1)S(1)} %collective-permute-done.17.refs_2_, ...), custom_call_target="tpu_custom_call" | custom-call | flops 20000000000 | tf_op jit(solution)/shard_map/pallas_call | solution.py:196
  39.3 1.0 %collective-permute-done.19.b = f32[4,1024]{1,0:T(4,128)S(1)} collective-permute-done((f32[4,1024]{1,0:T(4,128)S(1)}, f32[4,1024]{1,0:T(4,128)S(1)}, u32[]{:S(2)}, u32[]{:S(2)}) %collective-permute-start.19) | collective-permute-done | bytes 16416 | tf_op jit(solution)/shard_map/ppermute | solution.py:433
  40.4 0.8 %collective-permute-start.20 = (f32[4,256]{1,0:T(4,128)S(1)}, f32[4,256]{1,0:T(4,128)S(1)}, u32[]{:S(2)}, u32[]{:S(2)}) collective-permute-start(f32[4,256]{1,0:T(4,128)S(1)} %get-tuple-element.49), channel_id=1, source_target_pairs={{0,3},{1,2},{2,1},{3,0},{4,7},{5,6},{6,5},{7,4},{8,11},{9,10},{10,... | collective-permute-start | bytes 12296 | tf_op jit(solution)/shard_map/ppermute | solution.py:428
  41.1 1.5 %collective-permute-start.21 = (f32[4,256]{1,0:T(4,128)S(1)}, f32[4,256]{1,0:T(4,128)S(1)}, u32[]{:S(2)}, u32[]{:S(2)}) collective-permute-start(f32[4,256]{1,0:T(4,128)S(1)} %get-tuple-element.50), channel_id=1, source_target_pairs={{0,5},{1,4},{2,7},{3,6},{4,1},{5,0},{6,3},{7,2},{8,13},{9,12},{10,... | collective-permute-start | bytes 12296 | tf_op jit(solution)/shard_map/ppermute | solution.py:428
  42.6 1.6 %collective-permute-start.22 = (f32[4,256]{1,0:T(4,128)S(1)}, f32[4,256]{1,0:T(4,128)S(1)}, u32[]{:S(2)}, u32[]{:S(2)}) collective-permute-start(f32[4,256]{1,0:T(4,128)S(1)} %get-tuple-element.51), channel_id=1, source_target_pairs={{0,7},{1,6},{2,5},{3,4},{4,3},{5,2},{6,1},{7,0},{8,15},{9,14},{10,... | collective-permute-start | bytes 12296 | tf_op jit(solution)/shard_map/ppermute | solution.py:428
  44.2 0.8 %collective-permute-done.21.refs_2_ = f32[4,256]{1,0:T(4,128)S(1)} collective-permute-done((f32[4,256]{1,0:T(4,128)S(1)}, f32[4,256]{1,0:T(4,128)S(1)}, u32[]{:S(2)}, u32[]{:S(2)}) %collective-permute-start.21) | collective-permute-done | bytes 4128 | tf_op jit(solution)/shard_map/ppermute | solution.py:428
  45.0 2.4 %collective-permute-done.22.refs_3_ = f32[4,256]{1,0:T(4,128)S(1)} collective-permute-done((f32[4,256]{1,0:T(4,128)S(1)}, f32[4,256]{1,0:T(4,128)S(1)}, u32[]{:S(2)}, u32[]{:S(2)}) %collective-permute-start.22) | collective-permute-done | bytes 4128 | tf_op jit(solution)/shard_map/ppermute | solution.py:428
  47.5 0.6 %shard_map.263 = bf16[4,256]{1,0:T(4,128)(2,1)} custom-call(f32[4,256]{1,0:T(4,128)S(1)} %get-tuple-element.48.refs_0_, f32[4,256]{1,0:T(4,128)S(1)} %collective-permute-done.20.refs_1_, f32[4,256]{1,0:T(4,128)S(1)} %collective-permute-done.21.refs_2_, f32[4,256]{1,0:T(4,128)S(1)} %collective-permute-done.22.refs_3_, f32[4,256]{1,0:T(4,128)S(1)} %get-tuple-element.52.refs_4_), custom_call_target="tpu_custom_call" | custom-call | flops 20000000000 | tf_op jit(solution)/shard_map/pallas_call | solution.py:196
  (77 shorter events, 2.2 us)
Async XLA Ops:
  0.0 3.5 %collective-permute-start = (bf16[4,256]{1,0:T(4,128)(2,1)}, bf16[4,256]{1,0:T(4,128)(2,1)S(1)}, u32[]{:S(2)}, u32[]{:S(2)}) collective-permute-start(bf16[4,256]{1,0:T(4,128)(2,1)} %bitcast.54), channel_id=1, source_target_pairs={{0,1},{1,0},{2,3},{3,2},{4,5},{5,4},{6,7},{7,6},{8,9},{9,8},{10,11... | collective-permute-start | bytes 6152 | tf_op jit(solution)/shard_map/ppermute | solution.py:433
  2.8 13.8 %collective-permute-start.8 = (f32[8,32,64]{2,1,0:T(8,128)S(1)}, f32[8,32,64]{2,1,0:T(8,128)S(1)}, u32[]{:S(2)}, u32[]{:S(2)}) collective-permute-start(f32[8,32,64]{2,1,0:T(8,128)S(1)} %shard_map.257), channel_id=1, source_target_pairs={{0,1},{1,0},{2,3},{3,2},{4,5},{5,4},{6,7},{7,6},{8,9},{9,8},{10,11... | collective-permute-start | bytes 196616 | tf_op jit(solution)/shard_map/ppermute | solution.py:433
  2.9 18.5 %collective-permute-start.10 = (bf16[1,128,64,32]{1,3,2,0:T(8,128)(2,1)}, bf16[1,128,64,32]{1,3,2,0:T(8,128)(2,1)S(1)}, u32[]{:S(2)}, u32[]{:S(2)}) collective-permute-start(bf16[1,128,64,32]{1,3,2,0:T(8,128)(2,1)} %param.44), channel_id=1, source_target_pairs={{0,1},{1,0},{2,3},{3,2},{4,5},{5,4},{6,7},{7,6},{8,9},{9,8},{10,11... | collective-permute-start | bytes 1572872 | tf_op jit(solution)/shard_map/ppermute | solution.py:433
  3.5 6.1 %collective-permute-start.3 = (bf16[4,512]{1,0:T(4,128)(2,1)S(1)}, bf16[4,512]{1,0:T(4,128)(2,1)S(1)}, u32[]{:S(2)}, u32[]{:S(2)}) collective-permute-start(bf16[4,512]{1,0:T(4,128)(2,1)S(1)} %shard_map.254.piece.refs_0_), channel_id=1, source_target_pairs={{0,7},{1,6},{2,5},{3,4},{4,3},{5,2},{6,1},{7,0},{8,15},{9,14},{10,... | collective-permute-start | bytes 12296 | tf_op jit(solution)/shard_map/ppermute | solution.py:428
  8.3 3.9 %collective-permute-start.2 = (bf16[4,512]{1,0:T(4,128)(2,1)S(1)}, bf16[4,512]{1,0:T(4,128)(2,1)S(1)}, u32[]{:S(2)}, u32[]{:S(2)}) collective-permute-start(bf16[4,512]{1,0:T(4,128)(2,1)S(1)} %shard_map.254.piece.refs_0_), channel_id=1, source_target_pairs={{0,5},{1,4},{2,7},{3,6},{4,1},{5,0},{6,3},{7,2},{8,13},{9,12},{10,... | collective-permute-start | bytes 12296 | tf_op jit(solution)/shard_map/ppermute | solution.py:428
  8.3 3.9 %collective-permute-start.1 = (bf16[4,512]{1,0:T(4,128)(2,1)S(1)}, bf16[4,512]{1,0:T(4,128)(2,1)S(1)}, u32[]{:S(2)}, u32[]{:S(2)}) collective-permute-start(bf16[4,512]{1,0:T(4,128)(2,1)S(1)} %shard_map.254.piece.refs_0_), channel_id=1, source_target_pairs={{0,3},{1,2},{2,1},{3,0},{4,7},{5,6},{6,5},{7,4},{8,11},{9,10},{10,... | collective-permute-start | bytes 12296 | tf_op jit(solution)/shard_map/ppermute | solution.py:428
  9.8 11.6 %collective-permute-start.9 = (f32[1,64,32,128]{3,2,1,0:T(8,128)S(1)}, f32[1,64,32,128]{3,2,1,0:T(8,128)S(1)}, u32[]{:S(2)}, u32[]{:S(2)}) collective-permute-start(f32[1,64,32,128]{3,2,1,0:T(8,128)S(1)} %copy-done.24), channel_id=1, source_target_pairs={{0,1},{1,0},{2,3},{3,2},{4,5},{5,4},{6,7},{7,6},{8,9},{9,8},{10,11... | collective-permute-start | bytes 3145736 | tf_op jit(solution)/shard_map/ppermute | solution.py:433
  12.2 9.2 %copy-start.9 = (bf16[1,128,1024]{2,1,0:T(8,128)(2,1)S(1)}, bf16[1,128,1024]{2,1,0:T(8,128)(2,1)}, u32[]{:S(2)}) copy-start(bf16[1,128,1024]{2,1,0:T(8,128)(2,1)} %param.45) | copy-start | bytes 786436
  12.3 9.2 %copy-start.11 = (f32[1,128,64]{1,2,0:T(8,128)S(1)}, f32[1,128,64]{1,2,0:T(8,128)}, u32[]{:S(2)}) copy-start(f32[1,128,64]{1,2,0:T(8,128)} %param.46) | copy-start | bytes 98308
  12.3 9.2 %copy-start.14 = (f32[4,1024]{1,0:T(4,128)S(1)}, f32[4,1024]{1,0:T(4,128)}, u32[]{:S(2)}) copy-start(f32[4,1024]{1,0:T(4,128)} %refs_9_.2) | copy-start | bytes 49156
  12.3 9.2 %copy-start.15 = (f32[4,1024]{1,0:T(4,128)S(1)}, f32[4,1024]{1,0:T(4,128)}, u32[]{:S(2)}) copy-start(f32[4,1024]{1,0:T(4,128)} %refs_10_.1) | copy-start | bytes 49156
  12.3 9.2 %copy-start.17 = (bf16[1,3,1024]{2,1,0:T(4,128)(2,1)S(1)}, bf16[1,3,1024]{2,1,0:T(4,128)(2,1)}, u32[]{:S(2)}) copy-start(bf16[1,3,1024]{2,1,0:T(4,128)(2,1)} %param.41) | copy-start | bytes 18436
  12.3 9.2 %copy-start.18 = (bf16[1,3,1024]{2,1,0:T(4,128)(2,1)S(1)}, bf16[1,3,1024]{2,1,0:T(4,128)(2,1)}, u32[]{:S(2)}) copy-start(bf16[1,3,1024]{2,1,0:T(4,128)(2,1)} %param.42) | copy-start | bytes 18436
  12.3 9.2 %copy-start.21 = (f32[64]{0:T(128)S(1)}, f32[64]{0:T(128)}, u32[]{:S(2)}) copy-start(f32[64]{0:T(128)} %param.34) | copy-start | bytes 772
  12.3 9.2 %copy-start.22 = (f32[64]{0:T(128)S(1)}, f32[64]{0:T(128)}, u32[]{:S(2)}) copy-start(f32[64]{0:T(128)} %param.35) | copy-start | bytes 772
  12.3 9.2 %copy-start.23 = (f32[64]{0:T(128)S(1)}, f32[64]{0:T(128)}, u32[]{:S(2)}) copy-start(f32[64]{0:T(128)} %param.36) | copy-start | bytes 772
  13.6 1.2 %collective-permute-start.4 = (f32[1,1536]{1,0:T(1,128)S(1)}, f32[1,1536]{1,0:T(1,128)S(1)}, u32[]{:S(2)}, u32[]{:S(2)}) collective-permute-start(f32[1,1536]{1,0:T(1,128)S(1)} %get-tuple-element.34), channel_id=1, source_target_pairs={{0,1},{1,0},{2,3},{3,2},{4,5},{5,4},{6,7},{7,6},{8,9},{9,8},{10,11... | collective-permute-start | bytes 18440 | tf_op jit(solution)/shard_map/ppermute | solution.py:428
  13.8 5.0 %collective-permute-start.5 = (f32[1,1536]{1,0:T(1,128)S(1)}, f32[1,1536]{1,0:T(1,128)S(1)}, u32[]{:S(2)}, u32[]{:S(2)}) collective-permute-start(f32[1,1536]{1,0:T(1,128)S(1)} %get-tuple-element.35), channel_id=1, source_target_pairs={{0,3},{1,2},{2,1},{3,0},{4,7},{5,6},{6,5},{7,4},{8,11},{9,10},{10,... | collective-permute-start | bytes 18440 | tf_op jit(solution)/shard_map/ppermute | solution.py:428
  14.8 4.0 %collective-permute-start.6 = (f32[1,1536]{1,0:T(1,128)S(1)}, f32[1,1536]{1,0:T(1,128)S(1)}, u32[]{:S(2)}, u32[]{:S(2)}) collective-permute-start(f32[1,1536]{1,0:T(1,128)S(1)} %get-tuple-element.36), channel_id=1, source_target_pairs={{0,5},{1,4},{2,7},{3,6},{4,1},{5,0},{6,3},{7,2},{8,13},{9,12},{10,... | collective-permute-start | bytes 18440 | tf_op jit(solution)/shard_map/ppermute | solution.py:428
  16.6 4.9 %collective-permute-start.7 = (f32[1,1536]{1,0:T(1,128)S(1)}, f32[1,1536]{1,0:T(1,128)S(1)}, u32[]{:S(2)}, u32[]{:S(2)}) collective-permute-start(f32[1,1536]{1,0:T(1,128)S(1)} %get-tuple-element.37), channel_id=1, source_target_pairs={{0,7},{1,6},{2,5},{3,4},{4,3},{5,2},{6,1},{7,0},{8,15},{9,14},{10,... | collective-permute-start | bytes 18440 | tf_op jit(solution)/shard_map/ppermute | solution.py:428
  22.2 4.2 %collective-permute-start.11 = (f32[1,640]{1,0:T(1,128)S(1)}, f32[1,640]{1,0:T(1,128)S(1)}, u32[]{:S(2)}, u32[]{:S(2)}) collective-permute-start(f32[1,640]{1,0:T(1,128)S(1)} %get-tuple-element.39), channel_id=1, source_target_pairs={{0,1},{1,0},{2,3},{3,2},{4,5},{5,4},{6,7},{7,6},{8,9},{9,8},{10,11... | collective-permute-start | bytes 7688 | tf_op jit(solution)/shard_map/ppermute | solution.py:428
  22.4 4.1 %collective-permute-start.12 = (f32[1,640]{1,0:T(1,128)S(1)}, f32[1,640]{1,0:T(1,128)S(1)}, u32[]{:S(2)}, u32[]{:S(2)}) collective-permute-start(f32[1,640]{1,0:T(1,128)S(1)} %get-tuple-element.40), channel_id=1, source_target_pairs={{0,3},{1,2},{2,1},{3,0},{4,7},{5,6},{6,5},{7,4},{8,11},{9,10},{10,... | collective-permute-start | bytes 7688 | tf_op jit(solution)/shard_map/ppermute | solution.py:428
  22.4 4.1 %collective-permute-start.13 = (f32[1,640]{1,0:T(1,128)S(1)}, f32[1,640]{1,0:T(1,128)S(1)}, u32[]{:S(2)}, u32[]{:S(2)}) collective-permute-start(f32[1,640]{1,0:T(1,128)S(1)} %get-tuple-element.41), channel_id=1, source_target_pairs={{0,5},{1,4},{2,7},{3,6},{4,1},{5,0},{6,3},{7,2},{8,13},{9,12},{10,... | collective-permute-start | bytes 7688 | tf_op jit(solution)/shard_map/ppermute | solution.py:428
  24.2 4.8 %collective-permute-start.14 = (f32[1,640]{1,0:T(1,128)S(1)}, f32[1,640]{1,0:T(1,128)S(1)}, u32[]{:S(2)}, u32[]{:S(2)}) collective-permute-start(f32[1,640]{1,0:T(1,128)S(1)} %get-tuple-element.42), channel_id=1, source_target_pairs={{0,7},{1,6},{2,5},{3,4},{4,3},{5,2},{6,1},{7,0},{8,15},{9,14},{10,... | collective-permute-start | bytes 7688 | tf_op jit(solution)/shard_map/ppermute | solution.py:428
  29.4 1.3 %collective-permute-start.15 = (f32[4,2176]{1,0:T(4,128)S(1)}, f32[4,2176]{1,0:T(4,128)S(1)}, u32[]{:S(2)}, u32[]{:S(2)}) collective-permute-start(f32[4,2176]{1,0:T(4,128)S(1)} %shard_map.259.a), channel_id=1, source_target_pairs={{0,1},{1,0},{2,3},{3,2},{4,5},{5,4},{6,7},{7,6},{8,9},{9,8},{10,11... | collective-permute-start | bytes 104456 | tf_op jit(solution)/shard_map/ppermute | solution.py:433
  30.7 5.0 %collective-permute-start.18 = (bf16[4,2048]{1,0:T(4,128)(2,1)S(1)}, bf16[4,2048]{1,0:T(4,128)(2,1)S(1)}, u32[]{:S(2)}, u32[]{:S(2)}) collective-permute-start(bf16[4,2048]{1,0:T(4,128)(2,1)S(1)} %get-tuple-element.43.refs_0_), channel_id=1, source_target_pairs={{0,7},{1,6},{2,5},{3,4},{4,3},{5,2},{6,1},{7,0},{8,15},{9,14},{10,... | collective-permute-start | bytes 49160 | tf_op jit(solution)/shard_map/ppermute | solution.py:428
  33.0 4.1 %collective-permute-start.17 = (bf16[4,2048]{1,0:T(4,128)(2,1)S(1)}, bf16[4,2048]{1,0:T(4,128)(2,1)S(1)}, u32[]{:S(2)}, u32[]{:S(2)}) collective-permute-start(bf16[4,2048]{1,0:T(4,128)(2,1)S(1)} %get-tuple-element.43.refs_0_), channel_id=1, source_target_pairs={{0,5},{1,4},{2,7},{3,6},{4,1},{5,0},{6,3},{7,2},{8,13},{9,12},{10,... | collective-permute-start | bytes 49160 | tf_op jit(solution)/shard_map/ppermute | solution.py:428
  33.0 4.1 %collective-permute-start.16 = (bf16[4,2048]{1,0:T(4,128)(2,1)S(1)}, bf16[4,2048]{1,0:T(4,128)(2,1)S(1)}, u32[]{:S(2)}, u32[]{:S(2)}) collective-permute-start(bf16[4,2048]{1,0:T(4,128)(2,1)S(1)} %get-tuple-element.43.refs_0_), channel_id=1, source_target_pairs={{0,3},{1,2},{2,1},{3,0},{4,7},{5,6},{6,5},{7,4},{8,11},{9,10},{10,... | collective-permute-start | bytes 49160 | tf_op jit(solution)/shard_map/ppermute | solution.py:428
  39.2 1.2 %collective-permute-start.19 = (f32[4,1024]{1,0:T(4,128)S(1)}, f32[4,1024]{1,0:T(4,128)S(1)}, u32[]{:S(2)}, u32[]{:S(2)}) collective-permute-start(f32[4,1024]{1,0:T(4,128)S(1)} %get-tuple-element.47), channel_id=1, source_target_pairs={{0,1},{1,0},{2,3},{3,2},{4,5},{5,4},{6,7},{7,6},{8,9},{9,8},{10,11... | collective-permute-start | bytes 49160 | tf_op jit(solution)/shard_map/ppermute | solution.py:433
  40.4 3.9 %collective-permute-start.20 = (f32[4,256]{1,0:T(4,128)S(1)}, f32[4,256]{1,0:T(4,128)S(1)}, u32[]{:S(2)}, u32[]{:S(2)}) collective-permute-start(f32[4,256]{1,0:T(4,128)S(1)} %get-tuple-element.49), channel_id=1, source_target_pairs={{0,3},{1,2},{2,1},{3,0},{4,7},{5,6},{6,5},{7,4},{8,11},{9,10},{10,... | collective-permute-start | bytes 12296 | tf_op jit(solution)/shard_map/ppermute | solution.py:428
  41.1 3.9 %collective-permute-start.21 = (f32[4,256]{1,0:T(4,128)S(1)}, f32[4,256]{1,0:T(4,128)S(1)}, u32[]{:S(2)}, u32[]{:S(2)}) collective-permute-start(f32[4,256]{1,0:T(4,128)S(1)} %get-tuple-element.50), channel_id=1, source_target_pairs={{0,5},{1,4},{2,7},{3,6},{4,1},{5,0},{6,3},{7,2},{8,13},{9,12},{10,... | collective-permute-start | bytes 12296 | tf_op jit(solution)/shard_map/ppermute | solution.py:428
  42.6 4.8 %collective-permute-start.22 = (f32[4,256]{1,0:T(4,128)S(1)}, f32[4,256]{1,0:T(4,128)S(1)}, u32[]{:S(2)}, u32[]{:S(2)}) collective-permute-start(f32[4,256]{1,0:T(4,128)S(1)} %get-tuple-element.51), channel_id=1, source_target_pairs={{0,7},{1,6},{2,5},{3,4},{4,3},{5,2},{6,1},{7,0},{8,15},{9,14},{10,... | collective-permute-start | bytes 12296 | tf_op jit(solution)/shard_map/ppermute | solution.py:428
  (16 other events, 73.0 us)

commit v6 on v5

--- a/solution.py
+++ b/solution.py
@@ -191,7 +191,7 @@
     return values[0]
 
 
-def call(body, outs, args, scratch=(), scalars=(), space=pltpu.VMEM):
+def call(body, outs, args, scratch=(), scalars=(), space=pltpu.VMEM, flops=20_000_000_000):
     args = [pltpu.with_memory_space_constraint(a, pltpu.VMEM) for a in args]
     return pl.pallas_call(
         body,
@@ -201,7 +201,7 @@
         out_specs=[pl.BlockSpec(memory_space=pltpu.VMEM) for _ in outs],
         scratch_shapes=[pltpu.VMEM(s, d) for s, d in scratch],
         compiler_params=pltpu.CompilerParams(vmem_limit_bytes=8 << 20),
-        cost_estimate=pl.CostEstimate(flops=20_000_000_000, bytes_accessed=0, transcendentals=0),
+        cost_estimate=pl.CostEstimate(flops=flops, bytes_accessed=0, transcendentals=0),
     )(*args, *scalars)
 
 
@@ -270,6 +270,10 @@
     steps = (rms * totals[-1]).astype(jnp.bfloat16).astype(jnp.float32)
     row = lax.broadcasted_iota(jnp.int32, steps.shape, 0)
     step_out[...] = jnp.sum(jnp.where(row == kv, steps, 0.0), axis=0, keepdims=True)
+
+
+def flip(a, *refs):
+    refs[-1][...] = a[...].T
 
 
 def mixer(n, *refs):
@@ -385,9 +389,18 @@
     squares[...] = a[:, width:] + b[:, width:]
 
 
+def down(n, act, reduce_w, out, other):
+    kv, tp = lax.axis_index("kv"), lax.axis_index("tp")
+    part = out.shape[1] // n
+    for k in range(n):
+        side = tp if (k == 0) != other else 1 - tp
+        block = reduce_w[:, lane((2 * (kv ^ k) + side) * part, part)]
+        out[:, k * part : (k + 1) * part] = dot(act, block, NN)
+
+
 def channel_mix(n, channels, *refs):
     pieces, (squares, x, gain, gate_w, value_w, reduce_w) = refs[:n], refs[n : n + 6]
-    mid_out, keep, send, moved = refs[n + 6 :]
+    mid_out, act_out, send, moved = refs[n + 6 :]
     kv, tp = lax.axis_index("kv"), lax.axis_index("tp")
     width = x.shape[1]
     part = mid_out.shape[1]
@@ -399,13 +412,14 @@
     normed = (mid * gain[...]).astype(jnp.bfloat16)
     moved[...] = mid
     mid_out[...] = moved[:, lane((kv * 2 + tp) * part, part)]
-    act = silu(rms * dot(normed, gate_w[...], NT)) * (rms * dot(normed, value_w[...], NT))
-    moved[...] = dot(act.astype(jnp.bfloat16), reduce_w[...], NN)
-    for k in range(n):
-        at = slice(k * part, (k + 1) * part)
-        side = tp if k == 0 else 1 - tp
-        keep[:, at] = moved[:, lane((2 * (kv ^ k) + side) * part, part)]
-        send[:, at] = moved[:, lane((2 * (kv ^ k) + 1 - side) * part, part)]
+    act = silu(rms * dot(normed, gate_w[...], NN)) * (rms * dot(normed, value_w[...], NN))
+    act = act.astype(jnp.bfloat16)
+    act_out[...] = act
+    down(n, act, reduce_w, send, True)
+
+
+def keep_own(n, act, reduce_w, out):
+    down(n, act[...], reduce_w, out, False)
 
 
 def split_pair(a, b, *outs):
@@ -513,6 +527,13 @@
         scratch=[((1, channels), f32)] * 2 + [((1, n * maps), f32)] * 2 + [((1, channels), f32)],
     )
     pieces = across(sends, first=0)
+    hidden_units = reduce_proj.shape[0]
+    (gate_w,) = call(
+        flip,
+        [((width, hidden_units), bf16)],
+        [expand_gate.T, mixer_out.reshape(cols, width)],
+        flops=1,
+    )
     (mixed,) = call(
         functools.partial(out_project, n),
         [((seqs, width + LANES), f32)],
@@ -525,14 +546,22 @@
         [mixed, beside(mixed)],
     )
     pieces = across([mixed] * n)
-    mid, keep, send = call(
+    (value_w,) = call(flip, [((width, hidden_units), bf16)], [expand_value.T], flops=1)
+    mid, act, send = call(
         functools.partial(channel_mix, n, 2 * channels),
-        [((seqs, part), f32)] + [((seqs, width // 2), f32)] * 2,
+        [((seqs, part), f32), ((seqs, hidden_units), bf16), ((seqs, width // 2), f32)],
         pieces
-        + [squares, whole, channel_gain.reshape(1, width), expand_gate.T, expand_value.T, reduce_proj],
+        + [squares, whole, channel_gain.reshape(1, width), gate_w, value_w, reduce_proj],
         scratch=[((seqs, width), f32)],
     )
-    sends = call(split_pair, [((seqs, part), f32)] * n, [keep, beside(send)])
+    other = beside(send)
+    (keep,) = call(
+        functools.partial(keep_own, n),
+        [((seqs, width // 2), f32)],
+        [act, reduce_proj],
+        flops=1,
+    )
+    sends = call(split_pair, [((seqs, part), f32)] * n, [keep, other])
     pieces = across(sends)
     (out,) = call(
         functools.partial(finish, n),

time: 48.4 us -> 49.2 us (1.017)
  waiting for transfers between devices: 16.4 us -> 13.8 us
  local copies, waits for them, and re-layouts: 2.96 us -> 4.76 us
  Pallas kernels: 5.47 us -> 6.69 us
    ppermute x17, waiting for transfers between devices: 14.3 us -> 12.2 us  [across(): got.append(lax.ppermute(values[k], ('kv', 'tp'), pairs))]
    unnamed x50, local copies, waits for them, and re-layouts: 2.69 us -> 4.49 us
    pallas_call x11 -> x14, Pallas kernels: 5.47 us -> 6.69 us  [call(): pl.pallas_call(body, out_shape=[space(s, d) for s, d in outs], in_specs=[...]
  transfers between devices with their start and end apart: 23 -> 23, of which waited for: 11 -> 8; matrix products, arithmetic and copies ran while one was open for 1% -> 1% of each run, Pallas kernels for 4% -> 8%
where the time goes in v6:
time: 49.2 us; the launch traced here: 48.8 us
  starting transfers between devices  22.5 us (46%)
  waiting for transfers between devices  13.8 us (28%)
  Pallas kernels  6.69 us (14%)
  local copies, waits for them, and re-layouts  4.76 us (10%)
  between operations  0.96 us (2%)
    ppermute x17, starting transfers between devices, across(): got.append(lax.ppermute(values[k], ('kv', 'tp'), pairs))  20.5 us
    ppermute x17, waiting for transfers between devices, across(): got.append(lax.ppermute(values[k], ('kv', 'tp'), pairs))  12.2 us
    pallas_call x14, Pallas kernels, call(): pl.pallas_call(body, out_shape=[space(s, d) for s, d in outs], in_specs=[...  6.69 us
    unnamed x50, local copies, waits for them, and re-layouts  4.49 us
    ppermute x6, starting transfers between devices, beside(): return lax.ppermute(value, 'tp', [(0, 1), (1, 0)])  2.07 us
    ppermute x6, waiting for transfers between devices, beside(): return lax.ppermute(value, 'tp', [(0, 1), (1, 0)])  1.64 us
  transfers between devices with their start and end apart: 23, of which 8 were waited for; matrix products, arithmetic and copies ran while one was open for 1% of the time, Pallas kernels for 8%

profile of v6, /device:TPU:0, one launch (start us, length us, event | category | flops | bytes accessed | tf_op | source)
XLA Modules:
  0.0 48.8 jit_solution(12137072159811105549)
XLA Ops:
  0.0 0.5 %collective-permute-start = (bf16[4,256]{1,0:T(4,128)(2,1)}, bf16[4,256]{1,0:T(4,128)(2,1)S(1)}, u32[]{:S(2)}, u32[]{:S(2)}) collective-permute-start(bf16[4,256]{1,0:T(4,128)(2,1)} %bitcast.55), channel_id=1, source_target_pairs={{0,1},{1,0},{2,3},{3,2},{4,5},{5,4},{6,7},{7,6},{8,9},{9,8},{10,11... | collective-permute-start | bytes 6152 | tf_op jit(solution)/shard_map/ppermute | solution.py:447
  0.5 0.8 %copy-done.10 = f32[4,64,32]{1,2,0:T(8,128)S(1)} copy-done((f32[4,64,32]{1,2,0:T(8,128)S(1)}, f32[4,64,32]{1,2,0:T(8,128)}, u32[]{:S(2)}) %copy-start.10) | copy-done | bytes 32792
  1.3 0.7 %copy-done.12 = bf16[1,3,64,32]{2,3,1,0:T(8,128)(2,1)S(1)} copy-done((bf16[1,3,64,32]{2,3,1,0:T(8,128)(2,1)S(1)}, bf16[1,3,64,32]{2,3,1,0:T(8,128)(2,1)}, u32[]{:S(2)}) %copy-start.12) | copy-done | bytes 12312
  2.1 0.7 %copy-done.13 = f32[64,32]{0,1:T(8,128)S(1)} copy-done((f32[64,32]{0,1:T(8,128)S(1)}, f32[64,32]{0,1:T(8,128)}, u32[]{:S(2)}) %copy-start.13) | copy-done | bytes 8216
  2.9 0.5 %collective-permute-start.10 = (bf16[1,128,64,32]{1,3,2,0:T(8,128)(2,1)}, bf16[1,128,64,32]{1,3,2,0:T(8,128)(2,1)S(1)}, u32[]{:S(2)}, u32[]{:S(2)}) collective-permute-start(bf16[1,128,64,32]{1,3,2,0:T(8,128)(2,1)} %param.44), channel_id=1, source_target_pairs={{0,1},{1,0},{2,3},{3,2},{4,5},{5,4},{6,7},{7,6},{8,9},{9,8},{10,11... | collective-permute-start | bytes 1572872 | tf_op jit(solution)/shard_map/ppermute | solution.py:447
  3.5 4.8 %collective-permute-start.3 = (bf16[4,512]{1,0:T(4,128)(2,1)S(1)}, bf16[4,512]{1,0:T(4,128)(2,1)S(1)}, u32[]{:S(2)}, u32[]{:S(2)}) collective-permute-start(bf16[4,512]{1,0:T(4,128)(2,1)S(1)} %shard_map.254.piece.refs_0_), channel_id=1, source_target_pairs={{0,7},{1,6},{2,5},{3,4},{4,3},{5,2},{6,1},{7,0},{8,15},{9,14},{10,... | collective-permute-start | bytes 12296 | tf_op jit(solution)/shard_map/ppermute | solution.py:442
  8.6 0.5 shard_map.255
  9.1 0.6 %collective-permute-done.3.refs_3_ = bf16[4,512]{1,0:T(4,128)(2,1)S(1)} collective-permute-done((bf16[4,512]{1,0:T(4,128)(2,1)S(1)}, bf16[4,512]{1,0:T(4,128)(2,1)S(1)}, u32[]{:S(2)}, u32[]{:S(2)}) %collective-permute-start.3) | collective-permute-done | bytes 4128 | tf_op jit(solution)/shard_map/ppermute | solution.py:442
  9.8 0.5 %collective-permute-start.9 = (f32[1,64,32,128]{3,2,1,0:T(8,128)S(1)}, f32[1,64,32,128]{3,2,1,0:T(8,128)S(1)}, u32[]{:S(2)}, u32[]{:S(2)}) collective-permute-start(f32[1,64,32,128]{3,2,1,0:T(8,128)S(1)} %copy-done.24), channel_id=1, source_target_pairs={{0,1},{1,0},{2,3},{3,2},{4,5},{5,4},{6,7},{7,6},{8,9},{9,8},{10,11... | collective-permute-start | bytes 3145736 | tf_op jit(solution)/shard_map/ppermute | solution.py:447
  10.3 1.9 %collective-permute-done.2.refs_2_ = bf16[4,512]{1,0:T(4,128)(2,1)S(1)} collective-permute-done((bf16[4,512]{1,0:T(4,128)(2,1)S(1)}, bf16[4,512]{1,0:T(4,128)(2,1)S(1)}, u32[]{:S(2)}, u32[]{:S(2)}) %collective-permute-start.2) | collective-permute-done | bytes 4128 | tf_op jit(solution)/shard_map/ppermute | solution.py:442
  12.3 1.3 %shard_map.256 = (bf16[4,2048]{1,0:T(4,128)(2,1)S(1)}, f32[1,64]{1,0:T(1,128)S(1)}, f32[1,1536]{1,0:T(1,128)S(1)}, f32[1,1536]{1,0:T(1,128)S(1)}, f32[1,1536]{1,0:T(1,128)S(1)}, /*index=5*/f32[1,1536]{1,0:T(1,128)S(1)}) custom-call(bf16[4,512]{1,0:T(4,128)(2,1)S(1)} %shard_map.254.piece.refs_0_, bf16[4,512]{1,0:T(4,128)(2,1)S(1)} %collective-permute-done.1.refs_1_, ...), custom_call_target="tpu_custom_call" | custom-call | flops 20000000000 | tf_op jit(solution)/shard_map/pallas_call | solution.py:196
  13.8 1.1 %collective-permute-done.4.refs_0_ = f32[1,1536]{1,0:T(1,128)S(1)} collective-permute-done((f32[1,1536]{1,0:T(1,128)S(1)}, f32[1,1536]{1,0:T(1,128)S(1)}, u32[]{:S(2)}, u32[]{:S(2)}) %collective-permute-start.4) | collective-permute-done | bytes 6176 | tf_op jit(solution)/shard_map/ppermute | solution.py:442
  14.8 1.7 %collective-permute-start.6 = (f32[1,1536]{1,0:T(1,128)S(1)}, f32[1,1536]{1,0:T(1,128)S(1)}, u32[]{:S(2)}, u32[]{:S(2)}) collective-permute-start(f32[1,1536]{1,0:T(1,128)S(1)} %get-tuple-element.36), channel_id=1, source_target_pairs={{0,5},{1,4},{2,7},{3,6},{4,1},{5,0},{6,3},{7,2},{8,13},{9,12},{10,... | collective-permute-start | bytes 18440 | tf_op jit(solution)/shard_map/ppermute | solution.py:442
  16.6 1.3 %collective-permute-start.7 = (f32[1,1536]{1,0:T(1,128)S(1)}, f32[1,1536]{1,0:T(1,128)S(1)}, u32[]{:S(2)}, u32[]{:S(2)}) collective-permute-start(f32[1,1536]{1,0:T(1,128)S(1)} %get-tuple-element.37), channel_id=1, source_target_pairs={{0,7},{1,6},{2,5},{3,4},{4,3},{5,2},{6,1},{7,0},{8,15},{9,14},{10,... | collective-permute-start | bytes 18440 | tf_op jit(solution)/shard_map/ppermute | solution.py:442
  18.8 2.6 %collective-permute-done.7.refs_3_ = f32[1,1536]{1,0:T(1,128)S(1)} collective-permute-done((f32[1,1536]{1,0:T(1,128)S(1)}, f32[1,1536]{1,0:T(1,128)S(1)}, u32[]{:S(2)}, u32[]{:S(2)}) %collective-permute-start.7) | collective-permute-done | bytes 6176 | tf_op jit(solution)/shard_map/ppermute | solution.py:442
  21.5 0.7 %shard_map.258 = (f32[1,640]{1,0:T(1,128)S(1)}, f32[1,640]{1,0:T(1,128)S(1)}, f32[1,640]{1,0:T(1,128)S(1)}, f32[1,640]{1,0:T(1,128)S(1)}) custom-call(f32[1,1536]{1,0:T(1,128)S(1)} %collective-permute-done.4.refs_0_, f32[1,1536]{1,0:T(1,128)S(1)} %collective-permute-done.5.refs_1_, f32[1,1536]{1,0:T(1,128)S(1)} %collective-permute-done.6.refs_2_, ...), custom_call_target="tpu_custom_call" | custom-call | flops 20000000000 | tf_op jit(solution)/shard_map/pallas_call | solution.py:196
  22.4 1.8 %collective-permute-start.13 = (f32[1,640]{1,0:T(1,128)S(1)}, f32[1,640]{1,0:T(1,128)S(1)}, u32[]{:S(2)}, u32[]{:S(2)}) collective-permute-start(f32[1,640]{1,0:T(1,128)S(1)} %get-tuple-element.41), channel_id=1, source_target_pairs={{0,5},{1,4},{2,7},{3,6},{4,1},{5,0},{6,3},{7,2},{8,13},{9,12},{10,... | collective-permute-start | bytes 7688 | tf_op jit(solution)/shard_map/ppermute | solution.py:442
  24.2 2.2 %collective-permute-start.14 = (f32[1,640]{1,0:T(1,128)S(1)}, f32[1,640]{1,0:T(1,128)S(1)}, u32[]{:S(2)}, u32[]{:S(2)}) collective-permute-start(f32[1,640]{1,0:T(1,128)S(1)} %get-tuple-element.42), channel_id=1, source_target_pairs={{0,7},{1,6},{2,5},{3,4},{4,3},{5,2},{6,1},{7,0},{8,15},{9,14},{10,... | collective-permute-start | bytes 7688 | tf_op jit(solution)/shard_map/ppermute | solution.py:442
  26.5 2.6 %collective-permute-done.14.refs_3_ = f32[1,640]{1,0:T(1,128)S(1)} collective-permute-done((f32[1,640]{1,0:T(1,128)S(1)}, f32[1,640]{1,0:T(1,128)S(1)}, u32[]{:S(2)}, u32[]{:S(2)}) %collective-permute-start.14) | collective-permute-done | bytes 2592 | tf_op jit(solution)/shard_map/ppermute | solution.py:442
  29.6 1.1 %collective-permute-done.15.b = f32[4,2176]{1,0:T(4,128)S(1)} collective-permute-done((f32[4,2176]{1,0:T(4,128)S(1)}, f32[4,2176]{1,0:T(4,128)S(1)}, u32[]{:S(2)}, u32[]{:S(2)}) %collective-permute-start.15) | collective-permute-done | bytes 34848 | tf_op jit(solution)/shard_map/ppermute | solution.py:447
  30.7 2.3 %collective-permute-start.18 = (bf16[4,2048]{1,0:T(4,128)(2,1)S(1)}, bf16[4,2048]{1,0:T(4,128)(2,1)S(1)}, u32[]{:S(2)}, u32[]{:S(2)}) collective-permute-start(bf16[4,2048]{1,0:T(4,128)(2,1)S(1)} %get-tuple-element.43.refs_0_), channel_id=1, source_target_pairs={{0,7},{1,6},{2,5},{3,4},{4,3},{5,2},{6,1},{7,0},{8,15},{9,14},{10,... | collective-permute-start | bytes 49160 | tf_op jit(solution)/shard_map/ppermute | solution.py:442
  32.9 1.7 %collective-permute-start.16 = (bf16[4,2048]{1,0:T(4,128)(2,1)S(1)}, bf16[4,2048]{1,0:T(4,128)(2,1)S(1)}, u32[]{:S(2)}, u32[]{:S(2)}) collective-permute-start(bf16[4,2048]{1,0:T(4,128)(2,1)S(1)} %get-tuple-element.43.refs_0_), channel_id=1, source_target_pairs={{0,3},{1,2},{2,1},{3,0},{4,7},{5,6},{6,5},{7,4},{8,11},{9,10},{10,... | collective-permute-start | bytes 49160 | tf_op jit(solution)/shard_map/ppermute | solution.py:442
  34.6 0.9 %shard_map.261.refs_7_ = bf16[2048,704]{1,0:T(8,128)(2,1)S(1)} custom-call(bf16[704,2048]{1,0:T(8,128)(2,1)S(1)} %bitcast.34, bf16[512,2048]{1,0:T(8,128)(2,1)S(1)} %bitcast.36), custom_call_target="tpu_custom_call" | custom-call | flops 1 | tf_op jit(solution)/shard_map/pallas_call | solution.py:196
  35.5 0.9 %copy-done = bf16[2048,704]{0,1:T(8,128)(2,1)S(1)} copy-done((bf16[2048,704]{0,1:T(8,128)(2,1)S(1)}, bf16[2048,704]{0,1:T(8,128)(2,1)}, u32[]{:S(2)}) %copy-start) | copy-done | bytes 2883608
  36.4 0.9 %shard_map.262.refs_8_ = bf16[2048,704]{1,0:T(8,128)(2,1)S(1)} custom-call(bf16[704,2048]{1,0:T(8,128)(2,1)S(1)} %bitcast.33), custom_call_target="tpu_custom_call" | custom-call | flops 1 | tf_op jit(solution)/shard_map/pallas_call | solution.py:196
  37.3 0.9 %copy-done.1 = bf16[704,2048]{1,0:T(8,128)(2,1)S(1)} copy-done((bf16[704,2048]{1,0:T(8,128)(2,1)S(1)}, bf16[704,2048]{1,0:T(8,128)(2,1)}, u32[]{:S(2)}) %copy-start.1) | copy-done | bytes 2883608
  38.2 1.2 %shard_map.263 = (f32[4,256]{1,0:T(4,128)S(1)}, bf16[4,704]{1,0:T(4,128)(2,1)S(1)}, f32[4,1024]{1,0:T(4,128)S(1)}) custom-call(bf16[4,2048]{1,0:T(4,128)(2,1)S(1)} %get-tuple-element.43.refs_0_, bf16[4,2048]{1,0:T(4,128)(2,1)S(1)} %collective-permute-done.16.refs_1_, bf16[4,2048]{1,0:T(4,128)(2,1)S(1)} %collective-permute-done.17.refs_2_, ...), custom_call_target="tpu_custom_call" | custom-call | flops 20000000000 | tf_op jit(solution)/shard_map/pallas_call | solution.py:196
  40.1 0.5 %collective-permute-done.19.b = f32[4,1024]{1,0:T(4,128)S(1)} collective-permute-done((f32[4,1024]{1,0:T(4,128)S(1)}, f32[4,1024]{1,0:T(4,128)S(1)}, u32[]{:S(2)}, u32[]{:S(2)}) %collective-permute-start.19) | collective-permute-done | bytes 16416 | tf_op jit(solution)/shard_map/ppermute | solution.py:447
  40.7 2.6 %collective-permute-start.21 = (f32[4,256]{1,0:T(4,128)S(1)}, f32[4,256]{1,0:T(4,128)S(1)}, u32[]{:S(2)}, u32[]{:S(2)}) collective-permute-start(f32[4,256]{1,0:T(4,128)S(1)} %get-tuple-element.50), channel_id=1, source_target_pairs={{0,5},{1,4},{2,7},{3,6},{4,1},{5,0},{6,3},{7,2},{8,13},{9,12},{10,... | collective-permute-start | bytes 12296 | tf_op jit(solution)/shard_map/ppermute | solution.py:442
  43.4 1.3 %collective-permute-start.22 = (f32[4,256]{1,0:T(4,128)S(1)}, f32[4,256]{1,0:T(4,128)S(1)}, u32[]{:S(2)}, u32[]{:S(2)}) collective-permute-start(f32[4,256]{1,0:T(4,128)S(1)} %get-tuple-element.51), channel_id=1, source_target_pairs={{0,7},{1,6},{2,5},{3,4},{4,3},{5,2},{6,1},{7,0},{8,15},{9,14},{10,... | collective-permute-start | bytes 12296 | tf_op jit(solution)/shard_map/ppermute | solution.py:442
  44.7 3.5 %collective-permute-done.22.refs_3_ = f32[4,256]{1,0:T(4,128)S(1)} collective-permute-done((f32[4,256]{1,0:T(4,128)S(1)}, f32[4,256]{1,0:T(4,128)S(1)}, u32[]{:S(2)}, u32[]{:S(2)}) %collective-permute-start.22) | collective-permute-done | bytes 4128 | tf_op jit(solution)/shard_map/ppermute | solution.py:442
  48.2 0.6 %shard_map.266 = bf16[4,256]{1,0:T(4,128)(2,1)} custom-call(f32[4,256]{1,0:T(4,128)S(1)} %get-tuple-element.48.refs_0_, f32[4,256]{1,0:T(4,128)S(1)} %collective-permute-done.20.refs_1_, f32[4,256]{1,0:T(4,128)S(1)} %collective-permute-done.21.refs_2_, f32[4,256]{1,0:T(4,128)S(1)} %collective-permute-done.22.refs_3_, f32[4,256]{1,0:T(4,128)S(1)} %get-tuple-element.52.refs_4_), custom_call_target="tpu_custom_call" | custom-call | flops 20000000000 | tf_op jit(solution)/shard_map/pallas_call | solution.py:196
  (80 shorter events, 2.7 us)
Async XLA Ops:
  0.0 3.5 %collective-permute-start = (bf16[4,256]{1,0:T(4,128)(2,1)}, bf16[4,256]{1,0:T(4,128)(2,1)S(1)}, u32[]{:S(2)}, u32[]{:S(2)}) collective-permute-start(bf16[4,256]{1,0:T(4,128)(2,1)} %bitcast.55), channel_id=1, source_target_pairs={{0,1},{1,0},{2,3},{3,2},{4,5},{5,4},{6,7},{7,6},{8,9},{9,8},{10,11... | collective-permute-start | bytes 6152 | tf_op jit(solution)/shard_map/ppermute | solution.py:447
  2.8 13.8 %collective-permute-start.8 = (f32[8,32,64]{2,1,0:T(8,128)S(1)}, f32[8,32,64]{2,1,0:T(8,128)S(1)}, u32[]{:S(2)}, u32[]{:S(2)}) collective-permute-start(f32[8,32,64]{2,1,0:T(8,128)S(1)} %shard_map.257), channel_id=1, source_target_pairs={{0,1},{1,0},{2,3},{3,2},{4,5},{5,4},{6,7},{7,6},{8,9},{9,8},{10,11... | collective-permute-start | bytes 196616 | tf_op jit(solution)/shard_map/ppermute | solution.py:447
  2.9 18.5 %collective-permute-start.10 = (bf16[1,128,64,32]{1,3,2,0:T(8,128)(2,1)}, bf16[1,128,64,32]{1,3,2,0:T(8,128)(2,1)S(1)}, u32[]{:S(2)}, u32[]{:S(2)}) collective-permute-start(bf16[1,128,64,32]{1,3,2,0:T(8,128)(2,1)} %param.44), channel_id=1, source_target_pairs={{0,1},{1,0},{2,3},{3,2},{4,5},{5,4},{6,7},{7,6},{8,9},{9,8},{10,11... | collective-permute-start | bytes 1572872 | tf_op jit(solution)/shard_map/ppermute | solution.py:447
  3.5 6.1 %collective-permute-start.3 = (bf16[4,512]{1,0:T(4,128)(2,1)S(1)}, bf16[4,512]{1,0:T(4,128)(2,1)S(1)}, u32[]{:S(2)}, u32[]{:S(2)}) collective-permute-start(bf16[4,512]{1,0:T(4,128)(2,1)S(1)} %shard_map.254.piece.refs_0_), channel_id=1, source_target_pairs={{0,7},{1,6},{2,5},{3,4},{4,3},{5,2},{6,1},{7,0},{8,15},{9,14},{10,... | collective-permute-start | bytes 12296 | tf_op jit(solution)/shard_map/ppermute | solution.py:442
  8.3 3.9 %collective-permute-start.2 = (bf16[4,512]{1,0:T(4,128)(2,1)S(1)}, bf16[4,512]{1,0:T(4,128)(2,1)S(1)}, u32[]{:S(2)}, u32[]{:S(2)}) collective-permute-start(bf16[4,512]{1,0:T(4,128)(2,1)S(1)} %shard_map.254.piece.refs_0_), channel_id=1, source_target_pairs={{0,5},{1,4},{2,7},{3,6},{4,1},{5,0},{6,3},{7,2},{8,13},{9,12},{10,... | collective-permute-start | bytes 12296 | tf_op jit(solution)/shard_map/ppermute | solution.py:442
  8.3 3.9 %collective-permute-start.1 = (bf16[4,512]{1,0:T(4,128)(2,1)S(1)}, bf16[4,512]{1,0:T(4,128)(2,1)S(1)}, u32[]{:S(2)}, u32[]{:S(2)}) collective-permute-start(bf16[4,512]{1,0:T(4,128)(2,1)S(1)} %shard_map.254.piece.refs_0_), channel_id=1, source_target_pairs={{0,3},{1,2},{2,1},{3,0},{4,7},{5,6},{6,5},{7,4},{8,11},{9,10},{10,... | collective-permute-start | bytes 12296 | tf_op jit(solution)/shard_map/ppermute | solution.py:442
  9.8 11.6 %collective-permute-start.9 = (f32[1,64,32,128]{3,2,1,0:T(8,128)S(1)}, f32[1,64,32,128]{3,2,1,0:T(8,128)S(1)}, u32[]{:S(2)}, u32[]{:S(2)}) collective-permute-start(f32[1,64,32,128]{3,2,1,0:T(8,128)S(1)} %copy-done.24), channel_id=1, source_target_pairs={{0,1},{1,0},{2,3},{3,2},{4,5},{5,4},{6,7},{7,6},{8,9},{9,8},{10,11... | collective-permute-start | bytes 3145736 | tf_op jit(solution)/shard_map/ppermute | solution.py:447
  12.2 9.2 %copy-start.9 = (bf16[1,128,1024]{2,1,0:T(8,128)(2,1)S(1)}, bf16[1,128,1024]{2,1,0:T(8,128)(2,1)}, u32[]{:S(2)}) copy-start(bf16[1,128,1024]{2,1,0:T(8,128)(2,1)} %param.45) | copy-start | bytes 786436
  12.3 9.2 %copy-start.11 = (f32[1,128,64]{1,2,0:T(8,128)S(1)}, f32[1,128,64]{1,2,0:T(8,128)}, u32[]{:S(2)}) copy-start(f32[1,128,64]{1,2,0:T(8,128)} %param.46) | copy-start | bytes 98308
  12.3 9.2 %copy-start.14 = (f32[4,1024]{1,0:T(4,128)S(1)}, f32[4,1024]{1,0:T(4,128)}, u32[]{:S(2)}) copy-start(f32[4,1024]{1,0:T(4,128)} %refs_9_.2) | copy-start | bytes 49156
  12.3 9.2 %copy-start.15 = (f32[4,1024]{1,0:T(4,128)S(1)}, f32[4,1024]{1,0:T(4,128)}, u32[]{:S(2)}) copy-start(f32[4,1024]{1,0:T(4,128)} %refs_10_.1) | copy-start | bytes 49156
  12.3 9.2 %copy-start.17 = (bf16[1,3,1024]{2,1,0:T(4,128)(2,1)S(1)}, bf16[1,3,1024]{2,1,0:T(4,128)(2,1)}, u32[]{:S(2)}) copy-start(bf16[1,3,1024]{2,1,0:T(4,128)(2,1)} %param.41) | copy-start | bytes 18436
  12.3 9.2 %copy-start.18 = (bf16[1,3,1024]{2,1,0:T(4,128)(2,1)S(1)}, bf16[1,3,1024]{2,1,0:T(4,128)(2,1)}, u32[]{:S(2)}) copy-start(bf16[1,3,1024]{2,1,0:T(4,128)(2,1)} %param.42) | copy-start | bytes 18436
  12.3 9.2 %copy-start.21 = (f32[64]{0:T(128)S(1)}, f32[64]{0:T(128)}, u32[]{:S(2)}) copy-start(f32[64]{0:T(128)} %param.34) | copy-start | bytes 772
  12.3 9.2 %copy-start.22 = (f32[64]{0:T(128)S(1)}, f32[64]{0:T(128)}, u32[]{:S(2)}) copy-start(f32[64]{0:T(128)} %param.35) | copy-start | bytes 772
  12.3 9.2 %copy-start.23 = (f32[64]{0:T(128)S(1)}, f32[64]{0:T(128)}, u32[]{:S(2)}) copy-start(f32[64]{0:T(128)} %param.36) | copy-start | bytes 772
  13.6 1.2 %collective-permute-start.4 = (f32[1,1536]{1,0:T(1,128)S(1)}, f32[1,1536]{1,0:T(1,128)S(1)}, u32[]{:S(2)}, u32[]{:S(2)}) collective-permute-start(f32[1,1536]{1,0:T(1,128)S(1)} %get-tuple-element.34), channel_id=1, source_target_pairs={{0,1},{1,0},{2,3},{3,2},{4,5},{5,4},{6,7},{7,6},{8,9},{9,8},{10,11... | collective-permute-start | bytes 18440 | tf_op jit(solution)/shard_map/ppermute | solution.py:442
  13.8 5.0 %collective-permute-start.5 = (f32[1,1536]{1,0:T(1,128)S(1)}, f32[1,1536]{1,0:T(1,128)S(1)}, u32[]{:S(2)}, u32[]{:S(2)}) collective-permute-start(f32[1,1536]{1,0:T(1,128)S(1)} %get-tuple-element.35), channel_id=1, source_target_pairs={{0,3},{1,2},{2,1},{3,0},{4,7},{5,6},{6,5},{7,4},{8,11},{9,10},{10,... | collective-permute-start | bytes 18440 | tf_op jit(solution)/shard_map/ppermute | solution.py:442
  14.8 4.0 %collective-permute-start.6 = (f32[1,1536]{1,0:T(1,128)S(1)}, f32[1,1536]{1,0:T(1,128)S(1)}, u32[]{:S(2)}, u32[]{:S(2)}) collective-permute-start(f32[1,1536]{1,0:T(1,128)S(1)} %get-tuple-element.36), channel_id=1, source_target_pairs={{0,5},{1,4},{2,7},{3,6},{4,1},{5,0},{6,3},{7,2},{8,13},{9,12},{10,... | collective-permute-start | bytes 18440 | tf_op jit(solution)/shard_map/ppermute | solution.py:442
  16.6 4.9 %collective-permute-start.7 = (f32[1,1536]{1,0:T(1,128)S(1)}, f32[1,1536]{1,0:T(1,128)S(1)}, u32[]{:S(2)}, u32[]{:S(2)}) collective-permute-start(f32[1,1536]{1,0:T(1,128)S(1)} %get-tuple-element.37), channel_id=1, source_target_pairs={{0,7},{1,6},{2,5},{3,4},{4,3},{5,2},{6,1},{7,0},{8,15},{9,14},{10,... | collective-permute-start | bytes 18440 | tf_op jit(solution)/shard_map/ppermute | solution.py:442
  22.2 4.2 %collective-permute-start.11 = (f32[1,640]{1,0:T(1,128)S(1)}, f32[1,640]{1,0:T(1,128)S(1)}, u32[]{:S(2)}, u32[]{:S(2)}) collective-permute-start(f32[1,640]{1,0:T(1,128)S(1)} %get-tuple-element.39), channel_id=1, source_target_pairs={{0,1},{1,0},{2,3},{3,2},{4,5},{5,4},{6,7},{7,6},{8,9},{9,8},{10,11... | collective-permute-start | bytes 7688 | tf_op jit(solution)/shard_map/ppermute | solution.py:442
  22.4 4.1 %collective-permute-start.12 = (f32[1,640]{1,0:T(1,128)S(1)}, f32[1,640]{1,0:T(1,128)S(1)}, u32[]{:S(2)}, u32[]{:S(2)}) collective-permute-start(f32[1,640]{1,0:T(1,128)S(1)} %get-tuple-element.40), channel_id=1, source_target_pairs={{0,3},{1,2},{2,1},{3,0},{4,7},{5,6},{6,5},{7,4},{8,11},{9,10},{10,... | collective-permute-start | bytes 7688 | tf_op jit(solution)/shard_map/ppermute | solution.py:442
  22.4 4.1 %collective-permute-start.13 = (f32[1,640]{1,0:T(1,128)S(1)}, f32[1,640]{1,0:T(1,128)S(1)}, u32[]{:S(2)}, u32[]{:S(2)}) collective-permute-start(f32[1,640]{1,0:T(1,128)S(1)} %get-tuple-element.41), channel_id=1, source_target_pairs={{0,5},{1,4},{2,7},{3,6},{4,1},{5,0},{6,3},{7,2},{8,13},{9,12},{10,... | collective-permute-start | bytes 7688 | tf_op jit(solution)/shard_map/ppermute | solution.py:442
  24.2 4.8 %collective-permute-start.14 = (f32[1,640]{1,0:T(1,128)S(1)}, f32[1,640]{1,0:T(1,128)S(1)}, u32[]{:S(2)}, u32[]{:S(2)}) collective-permute-start(f32[1,640]{1,0:T(1,128)S(1)} %get-tuple-element.42), channel_id=1, source_target_pairs={{0,7},{1,6},{2,5},{3,4},{4,3},{5,2},{6,1},{7,0},{8,15},{9,14},{10,... | collective-permute-start | bytes 7688 | tf_op jit(solution)/shard_map/ppermute | solution.py:442
  29.4 1.2 %collective-permute-start.15 = (f32[4,2176]{1,0:T(4,128)S(1)}, f32[4,2176]{1,0:T(4,128)S(1)}, u32[]{:S(2)}, u32[]{:S(2)}) collective-permute-start(f32[4,2176]{1,0:T(4,128)S(1)} %shard_map.259.a), channel_id=1, source_target_pairs={{0,1},{1,0},{2,3},{3,2},{4,5},{5,4},{6,7},{7,6},{8,9},{9,8},{10,11... | collective-permute-start | bytes 104456 | tf_op jit(solution)/shard_map/ppermute | solution.py:447
  30.7 6.7 %collective-permute-start.18 = (bf16[4,2048]{1,0:T(4,128)(2,1)S(1)}, bf16[4,2048]{1,0:T(4,128)(2,1)S(1)}, u32[]{:S(2)}, u32[]{:S(2)}) collective-permute-start(bf16[4,2048]{1,0:T(4,128)(2,1)S(1)} %get-tuple-element.43.refs_0_), channel_id=1, source_target_pairs={{0,7},{1,6},{2,5},{3,4},{4,3},{5,2},{6,1},{7,0},{8,15},{9,14},{10,... | collective-permute-start | bytes 49160 | tf_op jit(solution)/shard_map/ppermute | solution.py:442
  32.9 4.4 %collective-permute-start.17 = (bf16[4,2048]{1,0:T(4,128)(2,1)S(1)}, bf16[4,2048]{1,0:T(4,128)(2,1)S(1)}, u32[]{:S(2)}, u32[]{:S(2)}) collective-permute-start(bf16[4,2048]{1,0:T(4,128)(2,1)S(1)} %get-tuple-element.43.refs_0_), channel_id=1, source_target_pairs={{0,5},{1,4},{2,7},{3,6},{4,1},{5,0},{6,3},{7,2},{8,13},{9,12},{10,... | collective-permute-start | bytes 49160 | tf_op jit(solution)/shard_map/ppermute | solution.py:442
  32.9 4.4 %collective-permute-start.16 = (bf16[4,2048]{1,0:T(4,128)(2,1)S(1)}, bf16[4,2048]{1,0:T(4,128)(2,1)S(1)}, u32[]{:S(2)}, u32[]{:S(2)}) collective-permute-start(bf16[4,2048]{1,0:T(4,128)(2,1)S(1)} %get-tuple-element.43.refs_0_), channel_id=1, source_target_pairs={{0,3},{1,2},{2,1},{3,0},{4,7},{5,6},{6,5},{7,4},{8,11},{9,10},{10,... | collective-permute-start | bytes 49160 | tf_op jit(solution)/shard_map/ppermute | solution.py:442
  39.4 1.2 %collective-permute-start.19 = (f32[4,1024]{1,0:T(4,128)S(1)}, f32[4,1024]{1,0:T(4,128)S(1)}, u32[]{:S(2)}, u32[]{:S(2)}) collective-permute-start(f32[4,1024]{1,0:T(4,128)S(1)} %get-tuple-element.47), channel_id=1, source_target_pairs={{0,1},{1,0},{2,3},{3,2},{4,5},{5,4},{6,7},{7,6},{8,9},{9,8},{10,11... | collective-permute-start | bytes 49160 | tf_op jit(solution)/shard_map/ppermute | solution.py:447
  40.6 4.1 %collective-permute-start.20 = (f32[4,256]{1,0:T(4,128)S(1)}, f32[4,256]{1,0:T(4,128)S(1)}, u32[]{:S(2)}, u32[]{:S(2)}) collective-permute-start(f32[4,256]{1,0:T(4,128)S(1)} %get-tuple-element.49), channel_id=1, source_target_pairs={{0,3},{1,2},{2,1},{3,0},{4,7},{5,6},{6,5},{7,4},{8,11},{9,10},{10,... | collective-permute-start | bytes 12296 | tf_op jit(solution)/shard_map/ppermute | solution.py:442
  40.7 4.0 %collective-permute-start.21 = (f32[4,256]{1,0:T(4,128)S(1)}, f32[4,256]{1,0:T(4,128)S(1)}, u32[]{:S(2)}, u32[]{:S(2)}) collective-permute-start(f32[4,256]{1,0:T(4,128)S(1)} %get-tuple-element.50), channel_id=1, source_target_pairs={{0,5},{1,4},{2,7},{3,6},{4,1},{5,0},{6,3},{7,2},{8,13},{9,12},{10,... | collective-permute-start | bytes 12296 | tf_op jit(solution)/shard_map/ppermute | solution.py:442
  43.4 4.8 %collective-permute-start.22 = (f32[4,256]{1,0:T(4,128)S(1)}, f32[4,256]{1,0:T(4,128)S(1)}, u32[]{:S(2)}, u32[]{:S(2)}) collective-permute-start(f32[4,256]{1,0:T(4,128)S(1)} %get-tuple-element.51), channel_id=1, source_target_pairs={{0,7},{1,6},{2,5},{3,4},{4,3},{5,2},{6,1},{7,0},{8,15},{9,14},{10,... | collective-permute-start | bytes 12296 | tf_op jit(solution)/shard_map/ppermute | solution.py:442
  (16 other events, 52.9 us)
